TPU v7x, 256 devices: a whole 4x4x8 slice. The times are simulated.
256 devices in a mesh: sp: 64 (over z, x, core), tp: 4 (over y).
Axes of the slice: x: 4, y: 4, z: 8, core: 2. Of those that a mesh axis runs over, the one named last changes fastest.
Arguments:
- queries: bfloat16 [8192, 2048], P('sp', 'tp'), may hold values from -6 to 6
- keys: bfloat16 [8192, 512], P('sp', 'tp'), may hold values from -6 to 6
- values: bfloat16 [8192, 512], P('sp', 'tp'), may hold values from -6 to 6
- break_bias: float32 [16], P('tp'), as said below
- residual: bfloat16 [8192, 4096], P(('sp', 'tp')), may hold values from -6 to 6
- w_out: bfloat16 [2048, 4096], P('tp'), may hold values from -0.125 to 0.125
- ffn_gain: float32 [4096], replicated, may hold values from 0.1 to 1.9
- pick_ids: int32 [8192, 2], P('sp'), may hold values from 0 to 63, as said below
- pair_logit: float32 [8192], P('sp'), may hold values from -8 to 8
- w_gate: bfloat16 [64, 4096, 1024], P('sp', None, 'tp'), may hold values from -0.09375 to 0.09375
- w_up: bfloat16 [64, 4096, 1024], P('sp', None, 'tp'), may hold values from -0.09375 to 0.09375
- w_down: bfloat16 [64, 1024, 4096], P('sp', 'tp'), may hold values from -0.1875 to 0.1875
- out_gain: float32 [4096], replicated, may hold values from 0.1 to 1.9
Outputs:
- new_stream: bfloat16 [8192, 4096], P(('sp', 'tp'))
Inputs may be any that keep to these rules, and one draw needn't show every extreme that they name: `break_bias`: the logarithm of a break rate per position: between ln(0.02 / 8192) and ln(8 / 128). `pick_ids`: A row's 2 experts differ and lie in one group of 16 consecutive experts. In each aligned block of 32 rows no expert is named more than 2 times, and some expert exactly 2 times.
All inputs are finite; a program needn't handle non-finite values.
Results may differ from a plain program's by a relative error of at most 0.017.
Values may be sent and summed in bfloat16 or wider, within the bound.
No kernel may reach another device: no remote copies, remote signals or barrier semaphores. Data moves between devices by JAX's collectives and lax.ppermute only.
A program may use at most 64 MiB of HBM per device.

v0:
```python
import functools

import jax
import jax.numpy as jnp
from jax import lax
from jax.experimental import pallas as pl
from jax.experimental.pallas import tpu as pltpu
from jax.sharding import PartitionSpec as P


HEAD = 128
TOP = 2
Z_SIZE = 8
X_SIZE = 4
CORES = 2
Z_PLANE = X_SIZE * CORES

epsilon = 1e-06


def split_up(shard, dim, peers):
    before, after = (shard.shape[:dim], shard.shape[dim + 1 :])
    return jnp.moveaxis(shard.reshape(*before, peers, -1, *after), dim, 0)


LOG2E = 1.4426950408889634
KEY_BLOCK = 256
PICK_ROWS = 8


def causal_visit(state, query_ref, kv_ref, bias_ref, later, block, first_query):
    outputs, used = state
    rows = query_ref.shape[0] // bias_ref.shape[0]
    heads = bias_ref.shape[0]
    factor = HEAD ** (-0.5) * LOG2E
    at_block = pl.ds(pl.multiple_of(block * KEY_BLOCK, KEY_BLOCK), KEY_BLOCK)
    keys = kv_ref[at_block, :HEAD]
    values = kv_ref[at_block, HEAD:]
    scores = lax.dot_general(
        query_ref[...], keys, (((1,), (1,)), ((), ())), preferred_element_type=jnp.float32
    )
    if first_query is not None:
        query_pos = first_query + lax.broadcasted_iota(jnp.int32, (rows, KEY_BLOCK), 0)
        key_pos = block * KEY_BLOCK + lax.broadcasted_iota(jnp.int32, (rows, KEY_BLOCK), 1)
        before = key_pos < query_pos
    breaks, leads = [], []
    for head in range(heads):
        z = scores[head * rows : (head + 1) * rows] * factor + bias_ref[head] * LOG2E
        log_term = jnp.log2(1.0 + jnp.exp2(-jnp.abs(z)))
        softplus = jnp.maximum(z, 0.0) + log_term
        leads.append(z - softplus)
        breaks.append(softplus if first_query is None else jnp.where(before, softplus, 0.0))
    behind = jnp.dot(
        jnp.concatenate([b.astype(jnp.bfloat16) for b in breaks], axis=0),
        later,
        preferred_element_type=jnp.float32,
    )
    weights = []
    for head in range(heads):
        at = slice(head * rows, (head + 1) * rows)
        past = behind[at]
        gone = used[at]
        weight = jnp.exp2(leads[head] - past - jnp.concatenate([gone, gone], axis=1))
        if first_query is not None:
            weight = jnp.where(before, weight, 0.0)
        weights.append(weight.astype(jnp.bfloat16))
        used[at] = gone + jnp.broadcast_to(past[:, :1] + breaks[head][:, :1], gone.shape)
    outputs[...] += jnp.dot(
        jnp.concatenate(weights, axis=0), values, preferred_element_type=jnp.float32
    )


def later_keys():
    return (
        lax.broadcasted_iota(jnp.int32, (KEY_BLOCK, KEY_BLOCK), 0)
        > lax.broadcasted_iota(jnp.int32, (KEY_BLOCK, KEY_BLOCK), 1)
    ).astype(jnp.float32).astype(jnp.bfloat16)


def lay_out(own_ref, twin_ref, plane, place):
    lanes = (place // CORES) % X_SIZE
    core = place % CORES
    length = own_ref.shape[1] - PICK_ROWS
    for shift in range(X_SIZE):
        source = ((lanes + X_SIZE - shift) % X_SIZE) * CORES
        plane[pl.ds(pl.multiple_of((source + core) * length, length), length)] = own_ref[shift, :length]
        plane[pl.ds(pl.multiple_of((source + 1 - core) * length, length), length)] = twin_ref[shift, :length]


def tally(counts, *pieces):
    expert = lax.broadcasted_iota(jnp.int32, counts.shape, 0).astype(jnp.float32)
    found = counts[...]
    for piece in pieces:
        length = piece.shape[1] - PICK_ROWS
        for shift in range(X_SIZE):
            picks = piece[shift, length:].astype(jnp.float32)[0:1]
            found = found + (picks == expert).astype(jnp.float32)
    counts[...] = found


def own_plane_kernel(place_ref, bias_ref, query_ref, own_ref, twin_ref, near, near_used, far, counts, plane):
    place = place_ref[0]
    lay_out(own_ref, twin_ref, plane, place)
    for ref in (near, near_used, far, counts):
        ref[...] = jnp.zeros_like(ref)
    tally(counts, own_ref, twin_ref)
    later = later_keys()
    rows = query_ref.shape[0] // bias_ref.shape[0]
    first_query = (place % (X_SIZE * CORES)) * rows
    last = (first_query + rows - 1) // KEY_BLOCK

    def step(index, carried):
        causal_visit((near, near_used), query_ref, plane, bias_ref, later, last - index, first_query)
        return carried

    lax.fori_loop(0, last + 1, step, 0)


def whole_plane(state, query_ref, plane, bias_ref):
    later = later_keys()
    blocks = plane.shape[0] // KEY_BLOCK

    def step(index, carried):
        causal_visit(state, query_ref, plane, bias_ref, later, blocks - 1 - 2 * index, None)
        causal_visit(state, query_ref, plane, bias_ref, later, blocks - 2 - 2 * index, None)
        return carried

    lax.fori_loop(0, blocks // 2, step, 0)


def two_planes_kernel(distance, place_ref, bias_ref, query_ref, below, below_twin, above, above_twin,
                      near_in, near_used_in, far_in, counts_in, near, near_used, far, counts,
                      planes, found, found_used):
    place = place_ref[0]
    tally(counts, below, below_twin, above, above_twin)
    level = place // (X_SIZE * CORES)
    lay_out(below, below_twin, planes.at[0], place)
    lay_out(above, above_twin, planes.at[1], place)

    def visit(side, carried):
        found[...] = jnp.zeros_like(found)
        found_used[...] = jnp.zeros_like(found_used)
        whole_plane((found, found_used), query_ref, planes.at[side], bias_ref)

        @pl.when(side == 0)
        def _():
            near[...] += jnp.exp2(-near_used[...]) * found[...]
            near_used[...] += found_used[...]

        @pl.when(side == 1)
        def _():
            far[...] = found[...] + jnp.exp2(-found_used[...]) * far[...]

        return carried

    first = jnp.where(level >= distance, 0, 1)
    past = jnp.where(level + distance >= Z_SIZE, 2, 1)
    lax.fori_loop(first, past, visit, 0)


def last_plane_kernel(distance, place_ref, bias_ref, query_ref, below, below_twin,
                      near_in, near_used_in, far_in, counts_in, out_ref, most_ref, plane, near, near_used, counts):
    place = place_ref[0]
    counts[...] = counts_in[...]
    tally(counts, below, below_twin)
    quarter = counts.shape[1] // 4
    lane = lax.broadcasted_iota(jnp.int32, counts.shape, 1) // quarter
    most = jnp.zeros((counts.shape[0], 1), jnp.float32)
    for member in range(4):
        named = jnp.sum(jnp.where(lane == member, counts[...], 0.0), axis=1, keepdims=True)
        most = jnp.maximum(most, named)
    most_ref[0] = jnp.max(most).astype(jnp.int32)
    near[...] = near_in[...]
    near_used[...] = near_used_in[...]

    @pl.when(place // (X_SIZE * CORES) >= distance)
    def _():
        lay_out(below, below_twin, plane, place)
        whole_plane((near, near_used), query_ref, plane, bias_ref)

    rows = out_ref.shape[0]
    for head in range(bias_ref.shape[0]):
        at = slice(head * rows, (head + 1) * rows)
        output = near[at] + jnp.exp2(-near_used[at]) * far_in[at]
        scaled = output * lax.rsqrt(jnp.mean(output * output, axis=-1, keepdims=True) + epsilon)
        out_ref[:, head * HEAD : (head + 1) * HEAD] = scaled.astype(jnp.bfloat16)


def attention_call(kernel, name, planes, position, break_bias, stacked, key_values, state, rows):
    stack = stacked.shape[0]
    in_vmem = pl.BlockSpec(memory_space=pltpu.VMEM)
    in_smem = pl.BlockSpec(memory_space=pltpu.SMEM)
    plane = (Z_PLANE * rows, 2 * HEAD)
    running = pltpu.VMEM((stack, HEAD), jnp.float32)
    kept = jax.ShapeDtypeStruct((stack, HEAD), jnp.float32)
    counts = (Z_SIZE * Z_PLANE, rows * TOP)
    last = name == "attend_last"
    keys = planes * Z_PLANE * rows
    first_state = 3 + len(key_values)
    heads = jax.ShapeDtypeStruct((rows, stack // rows * HEAD), jnp.bfloat16)
    return pl.pallas_call(
        kernel,
        out_shape=(heads, jax.ShapeDtypeStruct((1,), jnp.int32))
        if last
        else (kept,) * 3 + (jax.ShapeDtypeStruct(counts, jnp.float32),),
        in_specs=[in_smem, in_smem] + [in_vmem] * (1 + len(key_values) + len(state)),
        out_specs=(in_vmem, in_smem) if last else (in_vmem,) * 4,
        scratch_shapes=[pltpu.VMEM(plane if planes == 1 else (planes, *plane), jnp.bfloat16)]
        + ([running, running] if state else [])
        + ([pltpu.VMEM(counts, jnp.float32)] if last else []),
        input_output_aliases={} if last or not state else {first_state + i: i for i in range(4)},
        cost_estimate=pl.CostEstimate(
            flops=2 * stack * keys * (2 * HEAD + KEY_BLOCK), transcendentals=3 * stack * keys, bytes_accessed=0
        ),
        compiler_params=pltpu.CompilerParams(vmem_limit_bytes=24 * 1024 * 1024),
    )(position, break_bias, stacked, *key_values, *state)


def moved(shard, step_z, step_x, swap):
    pairs = []
    for place in range(Z_SIZE * Z_PLANE):
        z, x, core = place // Z_PLANE, place // CORES % X_SIZE, place % CORES
        target = ((z + step_z) % Z_SIZE * X_SIZE + (x + step_x) % X_SIZE) * CORES + (core ^ swap)
        pairs.append((place, target))
    return lax.ppermute(shard, "sp", pairs)


def attend(queries, keys, values, break_bias, pick_ids, position):
    rows = queries.shape[0]
    heads = queries.shape[1] // HEAD
    stacked = jnp.concatenate([queries[:, h * HEAD : (h + 1) * HEAD] for h in range(heads)], axis=0)
    picks = pick_ids.astype(jnp.bfloat16).reshape(1, rows * TOP)
    picks = jnp.concatenate([picks, jnp.zeros((PICK_ROWS - 1, rows * TOP), jnp.bfloat16)], axis=0)
    block = jnp.concatenate([jnp.concatenate([keys, values], axis=1), picks], axis=0)
    own = jnp.stack([block] + [moved(block, 0, step, 0) for step in range(1, X_SIZE)])
    twin = moved(own, 0, 0, 1)
    common = (position, break_bias, stacked)
    below, above = own, own
    arrived = []
    for distance in range(1, Z_SIZE // 2 + 1):
        below = moved(below, 1, 0, 0)
        pieces = [below, moved(below, 0, 0, 1)]
        if distance < Z_SIZE // 2:
            above = moved(above, -1, 0, 0)
            pieces += [above, moved(above, 0, 0, 1)]
        arrived.append(pieces)
    state = attention_call(own_plane_kernel, "attend_0", 1, *common, (own, twin), (), rows)
    for distance in range(1, Z_SIZE // 2):
        kernel = functools.partial(two_planes_kernel, distance)
        name = f"attend_{distance}"
        state = attention_call(kernel, name, 2, *common, arrived[distance - 1], state, rows)
    kernel = functools.partial(last_plane_kernel, Z_SIZE // 2)
    return attention_call(kernel, "attend_last", 1, *common, arrived[-1], state, rows)


COLUMNS = 1024
PACKED = 48


def in_kernel(kernel, out_shapes, megabytes, flops, *operands, scratch=()):
    spec = pl.BlockSpec(memory_space=pltpu.VMEM)
    several = isinstance(out_shapes, tuple)
    return pl.pallas_call(
        kernel,
        out_shape=out_shapes,
        in_specs=[spec] * len(operands),
        out_specs=(spec,) * len(out_shapes) if several else spec,
        scratch_shapes=list(scratch),
        cost_estimate=pl.CostEstimate(flops=flops, transcendentals=0, bytes_accessed=0),
        compiler_params=pltpu.CompilerParams(vmem_limit_bytes=megabytes * 1024 * 1024),
    )(*operands)


def over_columns(width, step, carried):
    def at_column(index, carried):
        return step(pl.ds(pl.multiple_of(index * COLUMNS, COLUMNS), COLUMNS), carried)

    return lax.fori_loop(0, width // COLUMNS, at_column, carried)


def dispatch_kernel(mixed_ref, residual_ref, gain_ref, targets_ref, stream_ref, outgoing_ref):
    rows, width = residual_ref.shape
    experts, capacity = outgoing_ref.shape[:2]

    def add(at, total):
        mixed = mixed_ref[0, :, at].astype(jnp.float32)
        for member in range(1, mixed_ref.shape[0]):
            mixed = mixed + mixed_ref[member, :, at].astype(jnp.float32)
        stream = (residual_ref[:, at].astype(jnp.float32) + mixed).astype(jnp.bfloat16)
        stream_ref[:, at] = stream
        wide = stream.astype(jnp.float32)
        return total + jnp.sum(wide * wide, axis=1, keepdims=True)

    total = over_columns(width, add, jnp.zeros((rows, 1), jnp.float32))
    scale = lax.rsqrt(total / width + epsilon)
    slot = lax.broadcasted_iota(jnp.int32, (experts * capacity, rows), 0)
    chosen = (slot == targets_ref[0:1, :]) | (slot == targets_ref[1:2, :])
    chosen = chosen.astype(jnp.float32).astype(jnp.bfloat16)

    def send(at, carried):
        normed = (stream_ref[:, at].astype(jnp.float32) * scale * gain_ref[:, at]).astype(jnp.bfloat16)
        sent = jnp.dot(chosen, normed, preferred_element_type=jnp.float32).astype(jnp.bfloat16)
        outgoing_ref[:, :, at] = sent.reshape(experts, capacity, COLUMNS)
        return carried

    over_columns(width, send, 0)


def pack_kernel(arrived_ref, first_ref, second_ref, rest_ref, back_ref, entries):
    slots = arrived_ref.shape[0] * arrived_ref.shape[1]
    width = arrived_ref.shape[2]

    def read(at, largest):
        part = arrived_ref[:, :, at].reshape(slots, COLUMNS)
        entries[:, at] = part
        size = jnp.abs(part.astype(jnp.float32))
        for lane in range(0, COLUMNS, 128):
            largest = jnp.maximum(largest, size[:, lane : lane + 128])
        return largest

    largest = over_columns(width, read, jnp.zeros((slots, 128), jnp.float32))
    held = (jnp.max(largest, axis=1, keepdims=True) > 0).astype(jnp.float32)
    row = lax.broadcasted_iota(jnp.int32, (slots, slots), 0)
    column = lax.broadcasted_iota(jnp.int32, (slots, slots), 1)

    def product(left, right):
        left, right = left.astype(jnp.float32), right.astype(jnp.float32)
        return jnp.dot(
            left.astype(jnp.bfloat16), right.astype(jnp.bfloat16), preferred_element_type=jnp.float32
        )

    held_rows = jnp.broadcast_to(held, (slots, slots))
    held_columns = product(jnp.ones((slots, slots), jnp.float32), jnp.where(row == column, held_rows, 0.0))
    place_rows = product(column < row, held_rows)
    place_columns = product(held_columns, row < column)
    back = ((place_rows == column.astype(jnp.float32)) & (held_rows > 0)).astype(jnp.float32)
    back_ref[...] = back.astype(jnp.bfloat16)
    forth = ((place_columns == row.astype(jnp.float32)) & (held_columns > 0)).astype(jnp.float32)
    forth = forth.astype(jnp.bfloat16)
    half = first_ref.shape[0]

    def write(at, carried):
        packed = jnp.dot(forth, entries[:, at], preferred_element_type=jnp.float32).astype(jnp.bfloat16)
        first_ref[:, at] = packed[:half]
        second_ref[:, at] = packed[half : 2 * half]
        rest_ref[:, at] = packed[2 * half :]
        return carried

    over_columns(width, write, 0)


def expert_kernel(*refs):
    count = (len(refs) - 6) // 2
    inputs, outs = refs[:count], refs[count + 3 : -3]
    gate_ref, up_ref, down_ref = refs[count : count + 3]
    entries, gate, up = refs[-3:]
    half, width = inputs[0].shape
    for index, source in enumerate(inputs):
        entries[index * half : (index + 1) * half] = source[...]
    gate[...] = jnp.zeros_like(gate)
    up[...] = jnp.zeros_like(up)

    def rise(index, carried):
        at = pl.ds(pl.multiple_of(index * COLUMNS, COLUMNS), COLUMNS)
        part = entries[:, at]
        gate[...] += jnp.dot(part, gate_ref[at, :], preferred_element_type=jnp.float32)
        up[...] += jnp.dot(part, up_ref[at, :], preferred_element_type=jnp.float32)
        return carried

    lax.fori_loop(0, width // COLUMNS, rise, 0)
    hidden = (gate[...] / (1.0 + jnp.exp(-gate[...])) * up[...]).astype(jnp.bfloat16)

    def fall(index, carried):
        at = pl.ds(pl.multiple_of(index * COLUMNS, COLUMNS), COLUMNS)
        share = jnp.dot(hidden, down_ref[:, at], preferred_element_type=jnp.float32).astype(jnp.bfloat16)
        for place, out in enumerate(outs):
            out[:, at] = share[place * half : (place + 1) * half]
        return carried

    lax.fori_loop(0, width // COLUMNS, fall, 0)


def run_experts(pieces, weights):
    shapes = tuple(jax.ShapeDtypeStruct(piece.shape, jnp.bfloat16) for piece in pieces)
    slots = sum(piece.shape[0] for piece in pieces)
    width, units = weights[0].shape
    flops = 6 * slots * width * units
    scratch = [pltpu.VMEM((slots, width), jnp.bfloat16)] + [pltpu.VMEM((slots, units), jnp.float32)] * 2
    return in_kernel(expert_kernel, shapes, 32, flops, *pieces, *weights, scratch=scratch)


def final_kernel(returned_ref, targets_ref, logits_ref, stream_ref, gain_ref, out_ref, blended):
    rows, width = stream_ref.shape
    slots = returned_ref.shape[0] * returned_ref.shape[1]
    slot = lax.broadcasted_iota(jnp.int32, (rows, slots), 1)
    picks = [
        (slot == targets_ref[:, pick : pick + 1]).astype(jnp.float32).astype(jnp.bfloat16) for pick in range(TOP)
    ]
    logits = logits_ref[...]
    shares = (1.0 / (1.0 + jnp.exp(-logits)), 1.0 / (1.0 + jnp.exp(logits)))

    def mix(at, total):
        entries = returned_ref[:, :, at].reshape(slots, COLUMNS)
        both = shares[0] * jnp.dot(picks[0], entries, preferred_element_type=jnp.float32)
        both = both + shares[1] * jnp.dot(picks[1], entries, preferred_element_type=jnp.float32)
        blended[:, at] = both
        return total + jnp.sum(both * both, axis=1, keepdims=True)

    total = over_columns(width, mix, jnp.zeros((rows, 1), jnp.float32))
    scale = lax.rsqrt(total / width + epsilon)

    def add(at, carried):
        wide = stream_ref[:, at].astype(jnp.float32)
        out_ref[:, at] = (wide + blended[:, at] * scale * gain_ref[:, at]).astype(jnp.bfloat16)
        return carried

    over_columns(width, add, 0)


def along_tp(shard, step):
    size = lax.axis_size("tp")
    return lax.ppermute(shard, "tp", [(member, (member + step) % size) for member in range(size)])


def relay_kernel(own_up, far_up, own_down, far_down, up_ref, down_ref):
    for own, far, out in ((own_up, far_up, up_ref), (own_down, far_down, down_ref)):

        def step(index, carried):
            at = pl.ds(pl.multiple_of(index * COLUMNS, COLUMNS), COLUMNS)
            out[:, at] = (own[:, at].astype(jnp.float32) + far[:, at].astype(jnp.float32)).astype(jnp.bfloat16)
            return carried

        lax.fori_loop(0, out.shape[1] // COLUMNS, step, 0)


def unpack_kernel(back_ref, rest_ref, *refs):
    firsts, seconds, results_ref = refs[:3], refs[3:6], refs[6]
    _, width = firsts[0].shape

    def step(index, carried):
        at = pl.ds(pl.multiple_of(index * COLUMNS, COLUMNS), COLUMNS)
        sums = []
        for parts in (firsts, seconds):
            total = parts[0][:, at].astype(jnp.float32)
            for part in parts[1:]:
                total = total + part[:, at].astype(jnp.float32)
            sums.append(total.astype(jnp.bfloat16))
        packed = jnp.concatenate(sums + [rest_ref[:, at]], axis=0)
        spread = jnp.dot(back_ref[...], packed, preferred_element_type=jnp.float32).astype(jnp.bfloat16)
        results_ref[:, :, at] = spread.reshape(results_ref.shape[0], results_ref.shape[1], COLUMNS)
        return carried

    lax.fori_loop(0, width // COLUMNS, step, 0)


def rest_outputs(rest, weights):
    half = rest.shape[0] // 2
    members = lax.axis_size("tp")
    gathered = [
        lax.all_gather(rest[start : start + half], "tp", axis=0, tiled=False) for start in (0, half)
    ]
    rows = jnp.concatenate(gathered, axis=1).reshape(members * rest.shape[0], rest.shape[1])
    (share,) = run_experts((rows,), weights)
    parts = lax.all_to_all(split_up(share, 0, members), "tp", split_axis=0, concat_axis=0, tiled=True)
    return jnp.sum(parts.astype(jnp.float32), axis=0).astype(jnp.bfloat16)


def expert_outputs(arrived, most, weights):
    experts, capacity, width = arrived.shape
    slots = experts * capacity
    half = jax.ShapeDtypeStruct((PACKED, width), jnp.bfloat16)
    rest_shape = jax.ShapeDtypeStruct((slots - 2 * PACKED, width), jnp.bfloat16)
    square = jax.ShapeDtypeStruct((slots, slots), jnp.bfloat16)
    first, second, rest, back = in_kernel(
        pack_kernel, (half, half, rest_shape, square), 16, 2 * slots * slots * width, arrived,
        scratch=[pltpu.VMEM((slots, width), jnp.bfloat16)],
    )
    below_first = along_tp(first, 1)
    above_second = along_tp(second, -1)
    below_second = along_tp(second, 1)
    above_first = along_tp(first, -1)
    far_first = along_tp(below_first, 1)
    far_second = along_tp(above_second, -1)
    own = run_experts((first, second), weights)
    near = run_experts((below_first, below_second, above_first, above_second), weights)
    direct_up = along_tp(near[3], 1)
    direct_down = along_tp(near[0], -1)
    far = run_experts((far_first, far_second), weights)
    relay_up = along_tp(far[0], 1)
    relay_down = along_tp(far[1], -1)
    both_up, both_down = in_kernel(
        relay_kernel, (half, half), 8, 4 * PACKED * width, near[2], relay_up, near[1], relay_down
    )
    both_up = along_tp(both_up, 1)
    both_down = along_tp(both_down, -1)
    rest_out = lax.cond(most > 2 * PACKED, lambda: rest_outputs(rest, weights), lambda: jnp.zeros_like(rest))
    return in_kernel(
        unpack_kernel, jax.ShapeDtypeStruct(arrived.shape, jnp.bfloat16), 16,
        2 * slots * slots * width, back, rest_out, own[0], both_up, direct_down, own[1], direct_up, both_down,
    )


def on_device(
    queries,
    keys,
    values,
    break_bias,
    residual,
    w_out,
    ffn_gain,
    pick_ids,
    pair_logit,
    w_gate,
    w_up,
    w_down,
    out_gain,
):
    position = lax.axis_index("sp")
    quarters = lax.axis_size("tp")
    quarter = lax.axis_index("tp")
    slice_rows = queries.shape[0] // quarters
    width = w_out.shape[1]
    experts = lax.axis_size("sp")
    capacity = max(2, (3 * slice_rows + experts - 1) // experts)
    routed = lax.dynamic_slice_in_dim(pick_ids, quarter * slice_rows, slice_rows, 0)
    flat_ids = routed.reshape(slice_rows * TOP)
    places = jnp.arange(slice_rows * TOP, dtype=jnp.int32)
    matches = (flat_ids[:, None] == flat_ids[None, :]) & (places[None, :] < places[:, None])
    ranks = jnp.sum(matches.astype(jnp.int32), axis=1)
    targets = (flat_ids * capacity + ranks).reshape(slice_rows, TOP)
    logits = lax.dynamic_slice_in_dim(pair_logit, quarter * slice_rows, slice_rows, 0)[:, None]

    place = position.reshape(1).astype(jnp.int32)
    head_out, most = attend(queries, keys, values, break_bias, pick_ids, place)
    partial = jnp.dot(head_out, w_out, preferred_element_type=jnp.float32).astype(jnp.bfloat16)
    parts = split_up(partial, 0, quarters)
    mixed = lax.all_to_all(parts, "tp", split_axis=0, concat_axis=0, tiled=True)
    slots = jax.ShapeDtypeStruct((experts, capacity, width), jnp.bfloat16)
    rows = jax.ShapeDtypeStruct((slice_rows, width), jnp.bfloat16)
    dispatch_flops = 2 * experts * capacity * slice_rows * width
    stream, outgoing = in_kernel(
        dispatch_kernel, (rows, slots), 16, dispatch_flops,
        mixed, residual, ffn_gain[None], targets.T,
    )
    arrived = lax.all_to_all(outgoing, "sp", split_axis=0, concat_axis=0, tiled=True)
    results = expert_outputs(arrived, most[0], (w_gate[0], w_up[0], w_down[0]))
    returned = lax.all_to_all(results, "sp", split_axis=0, concat_axis=0, tiled=True)
    return in_kernel(
        final_kernel, rows, 16, 2 * dispatch_flops,
        returned, targets, logits, stream, out_gain[None],
        scratch=[pltpu.VMEM((slice_rows, width), jnp.float32)],
    )


def solution(mesh):
    placed = (
        P("sp", "tp"),
        P("sp", "tp"),
        P("sp", "tp"),
        P("tp"),
        P(("sp", "tp"), None),
        P("tp", None),
        P(),
        P("sp", None),
        P("sp"),
        P("sp", None, "tp"),
        P("sp", None, "tp"),
        P("sp", "tp", None),
        P(),
    )

    return jax.shard_map(on_device, mesh=mesh, in_specs=placed, out_specs=P(("sp", "tp"), None), check_vma=False)
```

profile of v0, /device:TPU:1, one launch (start us, length us, event | category | flops | bytes accessed | tf_op | source)
XLA Modules:
  0.0 221.6 jit_solution(10792069239137128626)
XLA Ops:
  12.0 4.0 %collective-permute-start.9 = (bf16[4,136,256]{2,1,0:T(8,128)(2,1)S(1)}, bf16[4,136,256]{2,1,0:T(8,128)(2,1)S(1)}, u32[]{:S(2)}, u32[]{:S(2)}) collective-permute-start(bf16[4,136,256]{2,1,0:T(8,128)(2,1)S(1)} %pad_maximum_fusion.1.own_ref), channel_id=1, source_target_pairs={{0,224},{4,228},{8,232},{12,236},{16,240},{20,244},{24,248},{28,25... | collective-permute-start | bytes 835592 | tf_op jit(solution)/shard_map/ppermute | solution.py:225
  16.0 5.1 %collective-permute-done.3.below = bf16[4,136,256]{2,1,0:T(8,128)(2,1)S(1)} collective-permute-done((bf16[4,136,256]{2,1,0:T(8,128)(2,1)S(1)}, bf16[4,136,256]{2,1,0:T(8,128)(2,1)S(1)}, u32[]{:S(2)}, u32[]{:S(2)}) %collective-permute-start.3) | collective-permute-done | bytes 278560 | tf_op jit(solution)/shard_map/ppermute | solution.py:225
  21.2 2.7 %collective-permute-start.10 = (bf16[4,136,256]{2,1,0:T(8,128)(2,1)S(1)}, bf16[4,136,256]{2,1,0:T(8,128)(2,1)S(1)}, u32[]{:S(2)}, u32[]{:S(2)}) collective-permute-start(bf16[4,136,256]{2,1,0:T(8,128)(2,1)S(1)} %collective-permute-done.9.above), channel_id=1, source_target_pairs={{0,224},{4,228},{8,232},{12,236},{16,240},{20,244},{24,248},{28,25... | collective-permute-start | bytes 835592 | tf_op jit(solution)/shard_map/ppermute | solution.py:225
  23.8 2.9 %collective-permute-start.17 = (bf16[4,136,256]{2,1,0:T(8,128)(2,1)S(1)}, bf16[4,136,256]{2,1,0:T(8,128)(2,1)S(1)}, u32[]{:S(2)}, u32[]{:S(2)}) collective-permute-start(bf16[4,136,256]{2,1,0:T(8,128)(2,1)S(1)} %pad_maximum_fusion.1.own_ref), channel_id=1, source_target_pairs={{0,4},{4,0},{8,12},{12,8},{16,20},{20,16},{24,28},{28,24},{32,36},... | collective-permute-start | bytes 835592 | tf_op jit(solution)/shard_map/ppermute | solution.py:225
  28.2 3.2 %collective-permute-start.16 = (bf16[4,136,256]{2,1,0:T(8,128)(2,1)S(1)}, bf16[4,136,256]{2,1,0:T(8,128)(2,1)S(1)}, u32[]{:S(2)}, u32[]{:S(2)}) collective-permute-start(bf16[4,136,256]{2,1,0:T(8,128)(2,1)S(1)} %collective-permute-done.9.above), channel_id=1, source_target_pairs={{0,4},{4,0},{8,12},{12,8},{16,20},{20,16},{24,28},{28,24},{32,36},... | collective-permute-start | bytes 835592 | tf_op jit(solution)/shard_map/ppermute | solution.py:225
  31.5 3.0 %collective-permute-start.11 = (bf16[4,136,256]{2,1,0:T(8,128)(2,1)S(1)}, bf16[4,136,256]{2,1,0:T(8,128)(2,1)S(1)}, u32[]{:S(2)}, u32[]{:S(2)}) collective-permute-start(bf16[4,136,256]{2,1,0:T(8,128)(2,1)S(1)} %collective-permute-done.10.above), channel_id=1, source_target_pairs={{0,224},{4,228},{8,232},{12,236},{16,240},{20,244},{24,248},{28,25... | collective-permute-start | bytes 835592 | tf_op jit(solution)/shard_map/ppermute | solution.py:225
  36.5 3.7 %collective-permute-start.8 = (bf16[4,136,256]{2,1,0:T(8,128)(2,1)S(1)}, bf16[4,136,256]{2,1,0:T(8,128)(2,1)}, u32[]{:S(2)}, u32[]{:S(2)}) collective-permute-start(bf16[4,136,256]{2,1,0:T(8,128)(2,1)S(1)} %collective-permute-done.5.below), channel_id=1, source_target_pairs={{0,4},{4,0},{8,12},{12,8},{16,20},{20,16},{24,28},{28,24},{32,36},... | collective-permute-start | bytes 835592 | tf_op jit(solution)/shard_map/ppermute | solution.py:225
  53.1 4.3 %all-to-all-start.1 = ((bf16[4,32,4096]{2,1,0:T(8,128)(2,1)}), bf16[4,32,4096]{2,1,0:T(8,128)(2,1)S(1)}, u32[]{:S(2)}, u32[]{:S(2)}) async-start(bf16[4,32,4096]{2,1,0:T(8,128)(2,1)} %bitcast.9), calls=%async_computation.1 | async-start | bytes 2097152 | tf_op jit(solution)/shard_map/all_to_all | solution.py:537
  58.1 14.2 %all-to-all-done.1.mixed_ref = bf16[4,32,4096]{2,1,0:T(8,128)(2,1)S(1)} async-done(((bf16[4,32,4096]{2,1,0:T(8,128)(2,1)}), bf16[4,32,4096]{2,1,0:T(8,128)(2,1)S(1)}, u32[]{:S(2)}, u32[]{:S(2)}) %all-to-all-start.1) | async-done | bytes 1048608 | tf_op jit(solution)/shard_map/all_to_all | solution.py:537
  73.7 49.3 %all_to_all.20.arrived_ref = bf16[64,2,4096]{2,1,0:T(2,128)(2,1)S(1)} all-to-all(bf16[64,2,4096]{2,1,0:T(2,128)(2,1)S(1)} %get-tuple-element.71), channel_id=1, replica_groups=mesh['sp'=64,'tp'=4] {'sp'}, dimensions={0} | all-to-all | bytes 2097152 | tf_op jit(solution)/shard_map/all_to_all | solution.py:545
  123.1 2.7 %shard_map.133 = (bf16[48,4096]{1,0:T(8,128)(2,1)S(1)}, bf16[48,4096]{1,0:T(8,128)(2,1)S(1)}, bf16[32,4096]{1,0:T(8,128)(2,1)}, bf16[128,128]{1,0:T(8,128)(2,1)S(1)}) custom-call(bf16[64,2,4096]{2,1,0:T(2,128)(2,1)S(1)} %all_to_all.20.arrived_ref), custom_call_target="tpu_custom_call" | custom-call | flops 134217728 | tf_op jit(solution)/shard_map/pallas_call | solution.py:263
  128.5 8.1 %collective-permute-done.18.refs_0_ = bf16[48,4096]{1,0:T(8,128)(2,1)S(1)} collective-permute-done((bf16[48,4096]{1,0:T(8,128)(2,1)S(1)}, bf16[48,4096]{1,0:T(8,128)(2,1)S(1)}, u32[]{:S(2)}, u32[]{:S(2)}) %collective-permute-start.18) | collective-permute-done | bytes 393248 | tf_op jit(solution)/shard_map/ppermute | solution.py:422
  136.6 2.7 %collective-permute-start.23 = (bf16[48,4096]{1,0:T(8,128)(2,1)S(1)}, bf16[48,4096]{1,0:T(8,128)(2,1)S(1)}, u32[]{:S(2)}, u32[]{:S(2)}) collective-permute-start(bf16[48,4096]{1,0:T(8,128)(2,1)S(1)} %collective-permute-done.21.refs_3_), channel_id=1, source_target_pairs={{0,3},{1,0},{2,1},{3,2},{4,7},{5,4},{6,5},{7,6},{8,11},{9,8},{10,9... | collective-permute-start | bytes 1179656 | tf_op jit(solution)/shard_map/ppermute | solution.py:422
  139.2 2.7 %collective-permute-start.20 = (bf16[48,4096]{1,0:T(8,128)(2,1)S(1)}, bf16[48,4096]{1,0:T(8,128)(2,1)S(1)}, u32[]{:S(2)}, u32[]{:S(2)}) collective-permute-start(bf16[48,4096]{1,0:T(8,128)(2,1)S(1)} %get-tuple-element.75.refs_0_), channel_id=1, source_target_pairs={{0,3},{1,0},{2,1},{3,2},{4,7},{5,4},{6,5},{7,6},{8,11},{9,8},{10,9... | collective-permute-start | bytes 1179656 | tf_op jit(solution)/shard_map/ppermute | solution.py:422
  141.9 4.5 %collective-permute-done.22.refs_0_ = bf16[48,4096]{1,0:T(8,128)(2,1)S(1)} collective-permute-done((bf16[48,4096]{1,0:T(8,128)(2,1)S(1)}, bf16[48,4096]{1,0:T(8,128)(2,1)S(1)}, u32[]{:S(2)}, u32[]{:S(2)}) %collective-permute-start.22) | collective-permute-done | bytes 393248 | tf_op jit(solution)/shard_map/ppermute | solution.py:422
  146.5 4.0 %shard_map.136 = (bf16[48,4096]{1,0:T(8,128)(2,1)S(1)}, bf16[48,4096]{1,0:T(8,128)(2,1)S(1)}) custom-call(bf16[48,4096]{1,0:T(8,128)(2,1)S(1)} %collective-permute-done.22.refs_0_, bf16[48,4096]{1,0:T(8,128)(2,1)S(1)} %collective-permute-done.23.refs_1_, bf16[4096,256]{1,0:T(8,128)(2,1)S(1)} %bitcast.28, bf16[4096,256]{1,0:T(8,128)(2,1)S(1)} %bitcast.32, ...), custom_call_target="tpu_custom_call" | custom-call | flops 603979776 | tf_op jit(solution)/shard_map/pallas_call | solution.py:263
  150.5 2.7 %collective-permute-start.25 = (bf16[48,4096]{1,0:T(8,128)(2,1)S(1)}, bf16[48,4096]{1,0:T(8,128)(2,1)S(1)}, u32[]{:S(2)}, u32[]{:S(2)}) collective-permute-start(bf16[48,4096]{1,0:T(8,128)(2,1)S(1)} %get-tuple-element.81), channel_id=1, source_target_pairs={{0,3},{1,0},{2,1},{3,2},{4,7},{5,4},{6,5},{7,6},{8,11},{9,8},{10,9... | collective-permute-start | bytes 1179656 | tf_op jit(solution)/shard_map/ppermute | solution.py:422
  154.9 2.8 %shard_map.135 = (bf16[48,4096]{1,0:T(8,128)(2,1)S(1)}, bf16[48,4096]{1,0:T(8,128)(2,1)S(1)}, bf16[48,4096]{1,0:T(8,128)(2,1)S(1)}, bf16[48,4096]{1,0:T(8,128)(2,1)S(1)}) custom-call(bf16[48,4096]{1,0:T(8,128)(2,1)S(1)} %collective-permute-done.18.refs_0_, bf16[48,4096]{1,0:T(8,128)(2,1)S(1)} %collective-permute-done.19.refs_1_, ...), custom_call_target="tpu_custom_call" | custom-call | flops 1207959552 | tf_op jit(solution)/shard_map/pallas_call | solution.py:263
  160.1 2.7 %collective-permute-done.24.far_up = bf16[48,4096]{1,0:T(8,128)(2,1)S(1)} collective-permute-done((bf16[48,4096]{1,0:T(8,128)(2,1)S(1)}, bf16[48,4096]{1,0:T(8,128)(2,1)S(1)}, u32[]{:S(2)}, u32[]{:S(2)}) %collective-permute-start.24) | collective-permute-done | bytes 393248 | tf_op jit(solution)/shard_map/ppermute | solution.py:422
  164.0 2.7 %collective-permute-start.29 = (bf16[48,4096]{1,0:T(8,128)(2,1)}, bf16[48,4096]{1,0:T(8,128)(2,1)S(1)}, u32[]{:S(2)}, u32[]{:S(2)}) collective-permute-start(bf16[48,4096]{1,0:T(8,128)(2,1)} %get-tuple-element.86), channel_id=1, source_target_pairs={{0,3},{1,0},{2,1},{3,2},{4,7},{5,4},{6,5},{7,6},{8,11},{9,8},{10,9... | collective-permute-start | bytes 1179656 | tf_op jit(solution)/shard_map/ppermute | solution.py:422
  168.0 5.1 %shard_map.134 = (bf16[48,4096]{1,0:T(8,128)(2,1)S(1)}, bf16[48,4096]{1,0:T(8,128)(2,1)S(1)}) custom-call(bf16[48,4096]{1,0:T(8,128)(2,1)S(1)} %get-tuple-element.75.refs_0_, bf16[48,4096]{1,0:T(8,128)(2,1)S(1)} %get-tuple-element.76.refs_1_, bf16[4096,256]{1,0:T(8,128)(2,1)} %bitcast.27, bf16[4096,256]{1,0:T(8,128)(2,1)} %bitcast.31, bf16[256,4096]{1,0:T(8,128)(2,1)} %bitcast.36), custom_call_target="tpu_custom_call" | custom-call | flops 603979776 | tf_op jit(solution)/shard_map/pallas_call | solution.py:263
  173.1 4.6 %collective-permute-done.26.refs_1_ = bf16[48,4096]{1,0:T(8,128)(2,1)S(1)} collective-permute-done((bf16[48,4096]{1,0:T(8,128)(2,1)}, bf16[48,4096]{1,0:T(8,128)(2,1)S(1)}, u32[]{:S(2)}, u32[]{:S(2)}) %collective-permute-start.26) | collective-permute-done | bytes 393248 | tf_op jit(solution)/shard_map/ppermute | solution.py:422
  180.8 10.4 %all-to-all-start.3 = ((bf16[64,2,4096]{2,1,0:T(2,128)(2,1)}), bf16[64,2,4096]{2,1,0:T(2,128)(2,1)S(1)}, u32[]{:S(2)}, u32[]{:S(2)}) async-start(bf16[64,2,4096]{2,1,0:T(2,128)(2,1)} %shard_map.138), calls=%async_computation.3 | async-start | bytes 2097152 | tf_op jit(solution)/shard_map/all_to_all | solution.py:547
  191.4 28.0 %all-to-all-done.3.returned_ref = bf16[64,2,4096]{2,1,0:T(2,128)(2,1)S(1)} async-done(((bf16[64,2,4096]{2,1,0:T(2,128)(2,1)}), bf16[64,2,4096]{2,1,0:T(2,128)(2,1)S(1)}, u32[]{:S(2)}, u32[]{:S(2)}) %all-to-all-start.3) | async-done | bytes 1048608 | tf_op jit(solution)/shard_map/all_to_all | solution.py:547
  (102 shorter events, 45.3 us)
Async XLA Ops:
  10.0 11.2 %collective-permute-start.3 = (bf16[4,136,256]{2,1,0:T(8,128)(2,1)S(1)}, bf16[4,136,256]{2,1,0:T(8,128)(2,1)S(1)}, u32[]{:S(2)}, u32[]{:S(2)}) collective-permute-start(bf16[4,136,256]{2,1,0:T(8,128)(2,1)S(1)} %pad_maximum_fusion.1.own_ref), channel_id=1, source_target_pairs={{0,32},{4,36},{8,40},{12,44},{16,48},{20,52},{24,56},{28,60},{32,6... | collective-permute-start | bytes 835592 | tf_op jit(solution)/shard_map/ppermute | solution.py:225
  12.0 9.2 %collective-permute-start.9 = (bf16[4,136,256]{2,1,0:T(8,128)(2,1)S(1)}, bf16[4,136,256]{2,1,0:T(8,128)(2,1)S(1)}, u32[]{:S(2)}, u32[]{:S(2)}) collective-permute-start(bf16[4,136,256]{2,1,0:T(8,128)(2,1)S(1)} %pad_maximum_fusion.1.own_ref), channel_id=1, source_target_pairs={{0,224},{4,228},{8,232},{12,236},{16,240},{20,244},{24,248},{28,25... | collective-permute-start | bytes 835592 | tf_op jit(solution)/shard_map/ppermute | solution.py:225
  21.2 10.3 %collective-permute-start.10 = (bf16[4,136,256]{2,1,0:T(8,128)(2,1)S(1)}, bf16[4,136,256]{2,1,0:T(8,128)(2,1)S(1)}, u32[]{:S(2)}, u32[]{:S(2)}) collective-permute-start(bf16[4,136,256]{2,1,0:T(8,128)(2,1)S(1)} %collective-permute-done.9.above), channel_id=1, source_target_pairs={{0,224},{4,228},{8,232},{12,236},{16,240},{20,244},{24,248},{28,25... | collective-permute-start | bytes 835592 | tf_op jit(solution)/shard_map/ppermute | solution.py:225
  23.8 10.6 %collective-permute-start.17 = (bf16[4,136,256]{2,1,0:T(8,128)(2,1)S(1)}, bf16[4,136,256]{2,1,0:T(8,128)(2,1)S(1)}, u32[]{:S(2)}, u32[]{:S(2)}) collective-permute-start(bf16[4,136,256]{2,1,0:T(8,128)(2,1)S(1)} %pad_maximum_fusion.1.own_ref), channel_id=1, source_target_pairs={{0,4},{4,0},{8,12},{12,8},{16,20},{20,16},{24,28},{28,24},{32,36},... | collective-permute-start | bytes 835592 | tf_op jit(solution)/shard_map/ppermute | solution.py:225
  26.8 8.6 %collective-permute-start.15 = (bf16[4,136,256]{2,1,0:T(8,128)(2,1)S(1)}, bf16[4,136,256]{2,1,0:T(8,128)(2,1)S(1)}, u32[]{:S(2)}, u32[]{:S(2)}) collective-permute-start(bf16[4,136,256]{2,1,0:T(8,128)(2,1)S(1)} %collective-permute-done.3.below), channel_id=1, source_target_pairs={{0,4},{4,0},{8,12},{12,8},{16,20},{20,16},{24,28},{28,24},{32,36},... | collective-permute-start | bytes 835592 | tf_op jit(solution)/shard_map/ppermute | solution.py:225
  31.5 9.0 %collective-permute-start.11 = (bf16[4,136,256]{2,1,0:T(8,128)(2,1)S(1)}, bf16[4,136,256]{2,1,0:T(8,128)(2,1)S(1)}, u32[]{:S(2)}, u32[]{:S(2)}) collective-permute-start(bf16[4,136,256]{2,1,0:T(8,128)(2,1)S(1)} %collective-permute-done.10.above), channel_id=1, source_target_pairs={{0,224},{4,228},{8,232},{12,236},{16,240},{20,244},{24,248},{28,25... | collective-permute-start | bytes 835592 | tf_op jit(solution)/shard_map/ppermute | solution.py:225
  35.1 12.6 %collective-permute-start.13 = (bf16[4,136,256]{2,1,0:T(8,128)(2,1)S(1)}, bf16[4,136,256]{2,1,0:T(8,128)(2,1)S(1)}, u32[]{:S(2)}, u32[]{:S(2)}) collective-permute-start(bf16[4,136,256]{2,1,0:T(8,128)(2,1)S(1)} %collective-permute-done.4.below), channel_id=1, source_target_pairs={{0,4},{4,0},{8,12},{12,8},{16,20},{20,16},{24,28},{28,24},{32,36},... | collective-permute-start | bytes 835592 | tf_op jit(solution)/shard_map/ppermute | solution.py:225
  35.4 12.3 %collective-permute-start.14 = (bf16[4,136,256]{2,1,0:T(8,128)(2,1)S(1)}, bf16[4,136,256]{2,1,0:T(8,128)(2,1)S(1)}, u32[]{:S(2)}, u32[]{:S(2)}) collective-permute-start(bf16[4,136,256]{2,1,0:T(8,128)(2,1)S(1)} %collective-permute-done.10.above), channel_id=1, source_target_pairs={{0,4},{4,0},{8,12},{12,8},{16,20},{20,16},{24,28},{28,24},{32,36},... | collective-permute-start | bytes 835592 | tf_op jit(solution)/shard_map/ppermute | solution.py:225
  35.6 8.8 %collective-permute-start.6 = (bf16[4,136,256]{2,1,0:T(8,128)(2,1)S(1)}, bf16[4,136,256]{2,1,0:T(8,128)(2,1)S(1)}, u32[]{:S(2)}, u32[]{:S(2)}) collective-permute-start(bf16[4,136,256]{2,1,0:T(8,128)(2,1)S(1)} %collective-permute-done.5.below), channel_id=1, source_target_pairs={{0,32},{4,36},{8,40},{12,44},{16,48},{20,52},{24,56},{28,60},{32,6... | collective-permute-start | bytes 835592 | tf_op jit(solution)/shard_map/ppermute | solution.py:225
  36.5 12.0 %collective-permute-start.8 = (bf16[4,136,256]{2,1,0:T(8,128)(2,1)S(1)}, bf16[4,136,256]{2,1,0:T(8,128)(2,1)}, u32[]{:S(2)}, u32[]{:S(2)}) collective-permute-start(bf16[4,136,256]{2,1,0:T(8,128)(2,1)S(1)} %collective-permute-done.5.below), channel_id=1, source_target_pairs={{0,4},{4,0},{8,12},{12,8},{16,20},{20,16},{24,28},{28,24},{32,36},... | collective-permute-start | bytes 835592 | tf_op jit(solution)/shard_map/ppermute | solution.py:225
  53.1 19.2 %all-to-all-start.1 = ((bf16[4,32,4096]{2,1,0:T(8,128)(2,1)}), bf16[4,32,4096]{2,1,0:T(8,128)(2,1)S(1)}, u32[]{:S(2)}, u32[]{:S(2)}) async-start(bf16[4,32,4096]{2,1,0:T(8,128)(2,1)} %bitcast.9), calls=%async_computation.1 | async-start | bytes 2097152 | tf_op jit(solution)/shard_map/all_to_all | solution.py:537
  125.8 10.7 %collective-permute-start.18 = (bf16[48,4096]{1,0:T(8,128)(2,1)S(1)}, bf16[48,4096]{1,0:T(8,128)(2,1)S(1)}, u32[]{:S(2)}, u32[]{:S(2)}) collective-permute-start(bf16[48,4096]{1,0:T(8,128)(2,1)S(1)} %get-tuple-element.75.refs_0_), channel_id=1, source_target_pairs={{0,1},{1,2},{2,3},{3,0},{4,5},{5,6},{6,7},{7,4},{8,9},{9,10},{10,1... | collective-permute-start | bytes 1179656 | tf_op jit(solution)/shard_map/ppermute | solution.py:422
  126.1 10.5 %collective-permute-start.21 = (bf16[48,4096]{1,0:T(8,128)(2,1)S(1)}, bf16[48,4096]{1,0:T(8,128)(2,1)S(1)}, u32[]{:S(2)}, u32[]{:S(2)}) collective-permute-start(bf16[48,4096]{1,0:T(8,128)(2,1)S(1)} %get-tuple-element.76.refs_1_), channel_id=1, source_target_pairs={{0,3},{1,0},{2,1},{3,2},{4,7},{5,4},{6,5},{7,6},{8,11},{9,8},{10,9... | collective-permute-start | bytes 1179656 | tf_op jit(solution)/shard_map/ppermute | solution.py:422
  136.6 9.9 %collective-permute-start.22 = (bf16[48,4096]{1,0:T(8,128)(2,1)S(1)}, bf16[48,4096]{1,0:T(8,128)(2,1)S(1)}, u32[]{:S(2)}, u32[]{:S(2)}) collective-permute-start(bf16[48,4096]{1,0:T(8,128)(2,1)S(1)} %collective-permute-done.18.refs_0_), channel_id=1, source_target_pairs={{0,1},{1,2},{2,3},{3,0},{4,5},{5,6},{6,7},{7,4},{8,9},{9,10},{10,1... | collective-permute-start | bytes 1179656 | tf_op jit(solution)/shard_map/ppermute | solution.py:422
  136.6 9.9 %collective-permute-start.23 = (bf16[48,4096]{1,0:T(8,128)(2,1)S(1)}, bf16[48,4096]{1,0:T(8,128)(2,1)S(1)}, u32[]{:S(2)}, u32[]{:S(2)}) collective-permute-start(bf16[48,4096]{1,0:T(8,128)(2,1)S(1)} %collective-permute-done.21.refs_3_), channel_id=1, source_target_pairs={{0,3},{1,0},{2,1},{3,2},{4,7},{5,4},{6,5},{7,6},{8,11},{9,8},{10,9... | collective-permute-start | bytes 1179656 | tf_op jit(solution)/shard_map/ppermute | solution.py:422
  139.2 15.6 %collective-permute-start.19 = (bf16[48,4096]{1,0:T(8,128)(2,1)S(1)}, bf16[48,4096]{1,0:T(8,128)(2,1)S(1)}, u32[]{:S(2)}, u32[]{:S(2)}) collective-permute-start(bf16[48,4096]{1,0:T(8,128)(2,1)S(1)} %get-tuple-element.76.refs_1_), channel_id=1, source_target_pairs={{0,1},{1,2},{2,3},{3,0},{4,5},{5,6},{6,7},{7,4},{8,9},{9,10},{10,1... | collective-permute-start | bytes 1179656 | tf_op jit(solution)/shard_map/ppermute | solution.py:422
  139.2 15.6 %collective-permute-start.20 = (bf16[48,4096]{1,0:T(8,128)(2,1)S(1)}, bf16[48,4096]{1,0:T(8,128)(2,1)S(1)}, u32[]{:S(2)}, u32[]{:S(2)}) collective-permute-start(bf16[48,4096]{1,0:T(8,128)(2,1)S(1)} %get-tuple-element.75.refs_0_), channel_id=1, source_target_pairs={{0,3},{1,0},{2,1},{3,2},{4,7},{5,4},{6,5},{7,6},{8,11},{9,8},{10,9... | collective-permute-start | bytes 1179656 | tf_op jit(solution)/shard_map/ppermute | solution.py:422
  150.4 12.4 %collective-permute-start.24 = (bf16[48,4096]{1,0:T(8,128)(2,1)S(1)}, bf16[48,4096]{1,0:T(8,128)(2,1)S(1)}, u32[]{:S(2)}, u32[]{:S(2)}) collective-permute-start(bf16[48,4096]{1,0:T(8,128)(2,1)S(1)} %get-tuple-element.79), channel_id=1, source_target_pairs={{0,1},{1,2},{2,3},{3,0},{4,5},{5,6},{6,7},{7,4},{8,9},{9,10},{10,1... | collective-permute-start | bytes 1179656 | tf_op jit(solution)/shard_map/ppermute | solution.py:422
  150.5 12.3 %collective-permute-start.25 = (bf16[48,4096]{1,0:T(8,128)(2,1)S(1)}, bf16[48,4096]{1,0:T(8,128)(2,1)S(1)}, u32[]{:S(2)}, u32[]{:S(2)}) collective-permute-start(bf16[48,4096]{1,0:T(8,128)(2,1)S(1)} %get-tuple-element.81), channel_id=1, source_target_pairs={{0,3},{1,0},{2,1},{3,2},{4,7},{5,4},{6,5},{7,6},{8,11},{9,8},{10,9... | collective-permute-start | bytes 1179656 | tf_op jit(solution)/shard_map/ppermute | solution.py:422
  157.7 15.4 %collective-permute-start.27 = (bf16[48,4096]{1,0:T(8,128)(2,1)S(1)}, bf16[48,4096]{1,0:T(8,128)(2,1)S(1)}, u32[]{:S(2)}, u32[]{:S(2)}) collective-permute-start(bf16[48,4096]{1,0:T(8,128)(2,1)S(1)} %get-tuple-element.83), channel_id=1, source_target_pairs={{0,3},{1,0},{2,1},{3,2},{4,7},{5,4},{6,5},{7,6},{8,11},{9,8},{10,9... | collective-permute-start | bytes 1179656 | tf_op jit(solution)/shard_map/ppermute | solution.py:422
  160.1 13.0 %collective-permute-start.28 = (bf16[48,4096]{1,0:T(8,128)(2,1)S(1)}, bf16[48,4096]{1,0:T(8,128)(2,1)S(1)}, u32[]{:S(2)}, u32[]{:S(2)}) collective-permute-start(bf16[48,4096]{1,0:T(8,128)(2,1)S(1)} %get-tuple-element.85), channel_id=1, source_target_pairs={{0,1},{1,2},{2,3},{3,0},{4,5},{5,6},{6,7},{7,4},{8,9},{9,10},{10,1... | collective-permute-start | bytes 1179656 | tf_op jit(solution)/shard_map/ppermute | solution.py:422
  164.0 13.7 %collective-permute-start.26 = (bf16[48,4096]{1,0:T(8,128)(2,1)}, bf16[48,4096]{1,0:T(8,128)(2,1)S(1)}, u32[]{:S(2)}, u32[]{:S(2)}) collective-permute-start(bf16[48,4096]{1,0:T(8,128)(2,1)} %get-tuple-element.82), channel_id=1, source_target_pairs={{0,1},{1,2},{2,3},{3,0},{4,5},{5,6},{6,7},{7,4},{8,9},{9,10},{10,1... | collective-permute-start | bytes 1179656 | tf_op jit(solution)/shard_map/ppermute | solution.py:422
  164.0 14.8 %collective-permute-start.29 = (bf16[48,4096]{1,0:T(8,128)(2,1)}, bf16[48,4096]{1,0:T(8,128)(2,1)S(1)}, u32[]{:S(2)}, u32[]{:S(2)}) collective-permute-start(bf16[48,4096]{1,0:T(8,128)(2,1)} %get-tuple-element.86), channel_id=1, source_target_pairs={{0,3},{1,0},{2,1},{3,2},{4,7},{5,4},{6,5},{7,6},{8,11},{9,8},{10,9... | collective-permute-start | bytes 1179656 | tf_op jit(solution)/shard_map/ppermute | solution.py:422
  180.8 38.6 %all-to-all-start.3 = ((bf16[64,2,4096]{2,1,0:T(2,128)(2,1)}), bf16[64,2,4096]{2,1,0:T(2,128)(2,1)S(1)}, u32[]{:S(2)}, u32[]{:S(2)}) async-start(bf16[64,2,4096]{2,1,0:T(2,128)(2,1)} %shard_map.138), calls=%async_computation.3 | async-start | bytes 2097152 | tf_op jit(solution)/shard_map/all_to_all | solution.py:547
  (21 other events, 498.8 us)
where the time goes:
time: 222 us
  waiting for transfers between devices  73.2 us (33%)
  starting transfers between devices  61.8 us (28%)
  blocking collectives  49.3 us (22%)
  Pallas kernels  27.1 us (12%)
  local copies, waits for them, and re-layouts  4.88 us (2%)
  other arithmetic  2.64 us (1%)
    all_to_all x1, blocking collectives, on_device(): lax.all_to_all(outgoing, 'sp', split_axis=0, concat_axis=0, tiled=True)  49.3 us
    ppermute x18, starting transfers between devices, moved(): return lax.ppermute(shard, 'sp', pairs)  31.1 us
    all_to_all x1, waiting for transfers between devices, on_device(): lax.all_to_all(results, 'sp', split_axis=0, concat_axis=0, tiled=True)  28 us
    ppermute x12, waiting for transfers between devices, along_tp(): lax.ppermute(shard, 'tp', [(member, (member + step) % size) for member in...  22.6 us
    pallas_call x8, Pallas kernels, in_kernel(): pl.pallas_call(kernel, out_shape=out_shapes, in_specs=[spec] * len(operan...  21.3 us
    ppermute x12, starting transfers between devices, along_tp(): lax.ppermute(shard, 'tp', [(member, (member + step) % size) for member in...  15.9 us
    all_to_all x1, waiting for transfers between devices, on_device(): mixed = lax.all_to_all(parts, 'tp', split_axis=0, concat_axis=0, tiled=True)  14.2 us
    all_to_all x1, starting transfers between devices, on_device(): lax.all_to_all(results, 'sp', split_axis=0, concat_axis=0, tiled=True)  10.4 us
  transfers between devices with their start and end apart: 32, of which 13 were waited for; matrix products, arithmetic and copies ran while one was open for 1% of the time, Pallas kernels for 8%

commit v1 on v0

--- a/solution.py
+++ b/solution.py
@@ -1,4 +1,5 @@
 import functools
+import itertools
 
 import jax
 import jax.numpy as jnp
@@ -78,13 +79,12 @@
 
 
 def lay_out(own_ref, twin_ref, plane, place):
-    lanes = (place // CORES) % X_SIZE
     core = place % CORES
     length = own_ref.shape[1] - PICK_ROWS
-    for shift in range(X_SIZE):
-        source = ((lanes + X_SIZE - shift) % X_SIZE) * CORES
-        plane[pl.ds(pl.multiple_of((source + core) * length, length), length)] = own_ref[shift, :length]
-        plane[pl.ds(pl.multiple_of((source + 1 - core) * length, length), length)] = twin_ref[shift, :length]
+    for lane in range(X_SIZE):
+        first = lane * CORES * length
+        plane[pl.ds(pl.multiple_of(first + core * length, length), length)] = own_ref[lane, :length]
+        plane[pl.ds(pl.multiple_of(first + (1 - core) * length, length), length)] = twin_ref[lane, :length]
 
 
 def tally(counts, *pieces):
@@ -92,20 +92,21 @@
     found = counts[...]
     for piece in pieces:
         length = piece.shape[1] - PICK_ROWS
-        for shift in range(X_SIZE):
-            picks = piece[shift, length:].astype(jnp.float32)[0:1]
+        for block in range(piece.shape[0]):
+            picks = piece[block, length:].astype(jnp.float32)[0:1]
             found = found + (picks == expert).astype(jnp.float32)
     counts[...] = found
 
 
-def own_plane_kernel(place_ref, bias_ref, query_ref, own_ref, twin_ref, near, near_used, far, counts, plane):
+def own_plane_kernel(place_ref, bias_ref, query_ref, blocks_ref, near, near_used, far, counts, plane):
     place = place_ref[0]
-    lay_out(own_ref, twin_ref, plane, place)
+    rows = query_ref.shape[0] // bias_ref.shape[0]
+    for block in range(Z_PLANE):
+        plane[block * rows : (block + 1) * rows] = blocks_ref[block, :rows]
     for ref in (near, near_used, far, counts):
         ref[...] = jnp.zeros_like(ref)
-    tally(counts, own_ref, twin_ref)
+    tally(counts, blocks_ref)
     later = later_keys()
-    rows = query_ref.shape[0] // bias_ref.shape[0]
     first_query = (place % (X_SIZE * CORES)) * rows
     last = (first_query + rows - 1) // KEY_BLOCK
 
@@ -128,14 +129,14 @@
     lax.fori_loop(0, blocks // 2, step, 0)
 
 
-def two_planes_kernel(distance, place_ref, bias_ref, query_ref, below, below_twin, above, above_twin,
+def two_planes_kernel(distance, place_ref, bias_ref, query_ref, below, above, twins,
                       near_in, near_used_in, far_in, counts_in, near, near_used, far, counts,
                       planes, found, found_used):
     place = place_ref[0]
-    tally(counts, below, below_twin, above, above_twin)
+    tally(counts, below, above, twins)
     level = place // (X_SIZE * CORES)
-    lay_out(below, below_twin, planes.at[0], place)
-    lay_out(above, above_twin, planes.at[1], place)
+    lay_out(below, twins.at[:X_SIZE], planes.at[0], place)
+    lay_out(above, twins.at[X_SIZE:], planes.at[1], place)
 
     def visit(side, carried):
         found[...] = jnp.zeros_like(found)
@@ -232,19 +233,23 @@
     picks = pick_ids.astype(jnp.bfloat16).reshape(1, rows * TOP)
     picks = jnp.concatenate([picks, jnp.zeros((PICK_ROWS - 1, rows * TOP), jnp.bfloat16)], axis=0)
     block = jnp.concatenate([jnp.concatenate([keys, values], axis=1), picks], axis=0)
-    own = jnp.stack([block] + [moved(block, 0, step, 0) for step in range(1, X_SIZE)])
-    twin = moved(own, 0, 0, 1)
+    groups = [[z * Z_PLANE + w for w in range(Z_PLANE)] for z in range(Z_SIZE)]
+    copies = jnp.broadcast_to(block[None], (Z_PLANE, *block.shape))
+    blocks = lax.all_to_all(copies, "sp", 0, 0, axis_index_groups=groups, tiled=True)
+    by_core = blocks.reshape(X_SIZE, CORES, *block.shape)
+    own = lax.dynamic_index_in_dim(by_core, position[0] % CORES, 1, keepdims=False)
     common = (position, break_bias, stacked)
     below, above = own, own
     arrived = []
     for distance in range(1, Z_SIZE // 2 + 1):
         below = moved(below, 1, 0, 0)
-        pieces = [below, moved(below, 0, 0, 1)]
         if distance < Z_SIZE // 2:
             above = moved(above, -1, 0, 0)
-            pieces += [above, moved(above, 0, 0, 1)]
-        arrived.append(pieces)
-    state = attention_call(own_plane_kernel, "attend_0", 1, *common, (own, twin), (), rows)
+            both = jnp.concatenate([below, above], axis=0)
+            arrived.append((below, above, moved(both, 0, 0, 1)))
+        else:
+            arrived.append((below, moved(below, 0, 0, 1)))
+    state = attention_call(own_plane_kernel, "attend_0", 1, *common, (blocks,), (), rows)
     for distance in range(1, Z_SIZE // 2):
         kernel = functools.partial(two_planes_kernel, distance)
         name = f"attend_{distance}"
@@ -254,7 +259,7 @@
 
 
 COLUMNS = 1024
-PACKED = 48
+PACKED = (48, 40)
 
 
 def in_kernel(kernel, out_shapes, megabytes, flops, *operands, scratch=()):
@@ -271,7 +276,12 @@
     )(*operands)
 
 
-def over_columns(width, step, carried):
+def over_columns(width, step, carried, unrolled=False):
+    if unrolled:
+        for start in range(0, width, COLUMNS):
+            carried = step(slice(start, start + COLUMNS), carried)
+        return carried
+
     def at_column(index, carried):
         return step(pl.ds(pl.multiple_of(index * COLUMNS, COLUMNS), COLUMNS), carried)
 
@@ -291,7 +301,7 @@
         wide = stream.astype(jnp.float32)
         return total + jnp.sum(wide * wide, axis=1, keepdims=True)
 
-    total = over_columns(width, add, jnp.zeros((rows, 1), jnp.float32))
+    total = over_columns(width, add, jnp.zeros((rows, 1), jnp.float32), True)
     scale = lax.rsqrt(total / width + epsilon)
     slot = lax.broadcasted_iota(jnp.int32, (experts * capacity, rows), 0)
     chosen = (slot == targets_ref[0:1, :]) | (slot == targets_ref[1:2, :])
@@ -303,7 +313,7 @@
         outgoing_ref[:, :, at] = sent.reshape(experts, capacity, COLUMNS)
         return carried
 
-    over_columns(width, send, 0)
+    over_columns(width, send, 0, True)
 
 
 def pack_kernel(arrived_ref, first_ref, second_ref, rest_ref, back_ref, entries):
@@ -337,13 +347,13 @@
     back_ref[...] = back.astype(jnp.bfloat16)
     forth = ((place_columns == row.astype(jnp.float32)) & (held_columns > 0)).astype(jnp.float32)
     forth = forth.astype(jnp.bfloat16)
-    half = first_ref.shape[0]
+    half, both = first_ref.shape[0], first_ref.shape[0] + second_ref.shape[0]
 
     def write(at, carried):
         packed = jnp.dot(forth, entries[:, at], preferred_element_type=jnp.float32).astype(jnp.bfloat16)
         first_ref[:, at] = packed[:half]
-        second_ref[:, at] = packed[half : 2 * half]
-        rest_ref[:, at] = packed[2 * half :]
+        second_ref[:, at] = packed[half:both]
+        rest_ref[:, at] = packed[both:]
         return carried
 
     over_columns(width, write, 0)
@@ -354,9 +364,10 @@
     inputs, outs = refs[:count], refs[count + 3 : -3]
     gate_ref, up_ref, down_ref = refs[count : count + 3]
     entries, gate, up = refs[-3:]
-    half, width = inputs[0].shape
-    for index, source in enumerate(inputs):
-        entries[index * half : (index + 1) * half] = source[...]
+    width = inputs[0].shape[1]
+    ends = list(itertools.accumulate(source.shape[0] for source in inputs))
+    for source, end in zip(inputs, ends):
+        entries[end - source.shape[0] : end] = source[...]
     gate[...] = jnp.zeros_like(gate)
     up[...] = jnp.zeros_like(up)
 
@@ -373,8 +384,8 @@
     def fall(index, carried):
         at = pl.ds(pl.multiple_of(index * COLUMNS, COLUMNS), COLUMNS)
         share = jnp.dot(hidden, down_ref[:, at], preferred_element_type=jnp.float32).astype(jnp.bfloat16)
-        for place, out in enumerate(outs):
-            out[:, at] = share[place * half : (place + 1) * half]
+        for out, end in zip(outs, ends):
+            out[:, at] = share[end - out.shape[0] : end]
         return carried
 
     lax.fori_loop(0, width // COLUMNS, fall, 0)
@@ -406,7 +417,7 @@
         blended[:, at] = both
         return total + jnp.sum(both * both, axis=1, keepdims=True)
 
-    total = over_columns(width, mix, jnp.zeros((rows, 1), jnp.float32))
+    total = over_columns(width, mix, jnp.zeros((rows, 1), jnp.float32), True)
     scale = lax.rsqrt(total / width + epsilon)
 
     def add(at, carried):
@@ -414,7 +425,7 @@
         out_ref[:, at] = (wide + blended[:, at] * scale * gain_ref[:, at]).astype(jnp.bfloat16)
         return carried
 
-    over_columns(width, add, 0)
+    over_columns(width, add, 0, True)
 
 
 def along_tp(shard, step):
@@ -435,7 +446,7 @@
 
 def unpack_kernel(back_ref, rest_ref, *refs):
     firsts, seconds, results_ref = refs[:3], refs[3:6], refs[6]
-    _, width = firsts[0].shape
+    width = firsts[0].shape[1]
 
     def step(index, carried):
         at = pl.ds(pl.multiple_of(index * COLUMNS, COLUMNS), COLUMNS)
@@ -454,12 +465,9 @@
 
 
 def rest_outputs(rest, weights):
-    half = rest.shape[0] // 2
     members = lax.axis_size("tp")
-    gathered = [
-        lax.all_gather(rest[start : start + half], "tp", axis=0, tiled=False) for start in (0, half)
-    ]
-    rows = jnp.concatenate(gathered, axis=1).reshape(members * rest.shape[0], rest.shape[1])
+    copies = jnp.broadcast_to(rest[None], (members, *rest.shape))
+    rows = lax.all_to_all(copies, "tp", split_axis=0, concat_axis=0, tiled=True).reshape(-1, rest.shape[1])
     (share,) = run_experts((rows,), weights)
     parts = lax.all_to_all(split_up(share, 0, members), "tp", split_axis=0, concat_axis=0, tiled=True)
     return jnp.sum(parts.astype(jnp.float32), axis=0).astype(jnp.bfloat16)
@@ -468,11 +476,11 @@
 def expert_outputs(arrived, most, weights):
     experts, capacity, width = arrived.shape
     slots = experts * capacity
-    half = jax.ShapeDtypeStruct((PACKED, width), jnp.bfloat16)
-    rest_shape = jax.ShapeDtypeStruct((slots - 2 * PACKED, width), jnp.bfloat16)
+    half, other = (jax.ShapeDtypeStruct((count, width), jnp.bfloat16) for count in PACKED)
+    rest_shape = jax.ShapeDtypeStruct((slots - sum(PACKED), width), jnp.bfloat16)
     square = jax.ShapeDtypeStruct((slots, slots), jnp.bfloat16)
     first, second, rest, back = in_kernel(
-        pack_kernel, (half, half, rest_shape, square), 16, 2 * slots * slots * width, arrived,
+        pack_kernel, (half, other, rest_shape, square), 16, 2 * slots * slots * width, arrived,
         scratch=[pltpu.VMEM((slots, width), jnp.bfloat16)],
     )
     below_first = along_tp(first, 1)
@@ -489,11 +497,11 @@
     relay_up = along_tp(far[0], 1)
     relay_down = along_tp(far[1], -1)
     both_up, both_down = in_kernel(
-        relay_kernel, (half, half), 8, 4 * PACKED * width, near[2], relay_up, near[1], relay_down
+        relay_kernel, (half, other), 8, 2 * sum(PACKED) * width, near[2], relay_up, near[1], relay_down
     )
     both_up = along_tp(both_up, 1)
     both_down = along_tp(both_down, -1)
-    rest_out = lax.cond(most > 2 * PACKED, lambda: rest_outputs(rest, weights), lambda: jnp.zeros_like(rest))
+    rest_out = lax.cond(most > sum(PACKED), lambda: rest_outputs(rest, weights), lambda: jnp.zeros_like(rest))
     return in_kernel(
         unpack_kernel, jax.ShapeDtypeStruct(arrived.shape, jnp.bfloat16), 16,
         2 * slots * slots * width, back, rest_out, own[0], both_up, direct_down, own[1], direct_up, both_down,

time: 222 us -> 229 us (1.032)
  waiting for transfers between devices: 73.2 us -> 92.4 us
  starting transfers between devices: 61.8 us -> 55.9 us
    ppermute x18 -> x11, starting transfers between devices: 31.1 us -> 17.5 us  [moved(): return lax.ppermute(shard, 'sp', pairs)]
    ppermute x18 -> x11, waiting for transfers between devices: 8.31 us -> 20.5 us  [moved(): return lax.ppermute(shard, 'sp', pairs)]
    all_to_all x0 -> x1, waiting for transfers between devices: none -> 9.73 us  [attend(): lax.all_to_all(copies, 'sp', 0, 0, axis_index_groups=groups, tiled=True)]
    all_to_all x0 -> x1, starting transfers between devices: none -> 6.64 us  [attend(): lax.all_to_all(copies, 'sp', 0, 0, axis_index_groups=groups, tiled=True)]
    ppermute x12, waiting for transfers between devices: 22.6 us -> 19.9 us  [along_tp(): lax.ppermute(shard, 'tp', [(member, (member + step) % size) for member in...]
    all_to_all x1, starting transfers between devices: 10.4 us -> 12.8 us  [on_device(): lax.all_to_all(results, 'sp', split_axis=0, concat_axis=0, tiled=True)]
    unnamed x27 -> x25, local copies, waits for them, and re-layouts: 2.45 us -> 0.14 us
  transfers between devices with their start and end apart: 32 -> 26, of which waited for: 13 -> 14; matrix products, arithmetic and copies ran while one was open for 1% -> 1% of each run, Pallas kernels for 8% -> 7%
where the time goes in v1:
time: 229 us; the launch traced here: 228 us
  waiting for transfers between devices  92.4 us (40%)
  starting transfers between devices  55.9 us (24%)
  blocking collectives  47.1 us (21%)
  Pallas kernels  25.3 us (11%)
  local copies, waits for them, and re-layouts  2.68 us (1%)
    all_to_all x1, blocking collectives, on_device(): lax.all_to_all(outgoing, 'sp', split_axis=0, concat_axis=0, tiled=True)  47.1 us
    all_to_all x1, waiting for transfers between devices, on_device(): lax.all_to_all(results, 'sp', split_axis=0, concat_axis=0, tiled=True)  28 us
    ppermute x11, waiting for transfers between devices, moved(): return lax.ppermute(shard, 'sp', pairs)  20.5 us
    pallas_call x8, Pallas kernels, in_kernel(): pl.pallas_call(kernel, out_shape=out_shapes, in_specs=[spec] * len(operan...  20.3 us
    ppermute x12, waiting for transfers between devices, along_tp(): lax.ppermute(shard, 'tp', [(member, (member + step) % size) for member in...  19.9 us
    ppermute x11, starting transfers between devices, moved(): return lax.ppermute(shard, 'sp', pairs)  17.5 us
    ppermute x12, starting transfers between devices, along_tp(): lax.ppermute(shard, 'tp', [(member, (member + step) % size) for member in...  14.7 us
    all_to_all x1, waiting for transfers between devices, on_device(): mixed = lax.all_to_all(parts, 'tp', split_axis=0, concat_axis=0, tiled=True)  14.3 us
  transfers between devices with their start and end apart: 26, of which 14 were waited for; matrix products, arithmetic and copies ran while one was open for 1% of the time, Pallas kernels for 7%

profile of v1, /device:TPU:1, one launch (start us, length us, event | category | flops | bytes accessed | tf_op | source)
XLA Modules:
  0.0 228.1 jit_solution(16647700860924266077)
XLA Ops:
  2.8 6.6 %all-to-all-start.2 = ((bf16[8,136,256]{2,1,0:T(8,128)(2,1)}), bf16[8,136,256]{2,1,0:T(8,128)(2,1)S(1)}, u32[]{:S(2)}, u32[]{:S(2)}) async-start(bf16[8,136,256]{2,1,0:T(8,128)(2,1)} %broadcast_in_dim.17), calls=%async_computation.2 | async-start | bytes 1114112 | tf_op jit(solution)/shard_map/all_to_all | solution.py:238
  9.4 9.7 %all-to-all-done.2.blocks_ref = bf16[8,136,256]{2,1,0:T(8,128)(2,1)S(1)} async-done(((bf16[8,136,256]{2,1,0:T(8,128)(2,1)}), bf16[8,136,256]{2,1,0:T(8,128)(2,1)S(1)}, u32[]{:S(2)}, u32[]{:S(2)}) %all-to-all-start.2) | async-done | bytes 557088 | tf_op jit(solution)/shard_map/all_to_all | solution.py:238
  20.0 4.0 %collective-permute-start.5 = (bf16[4,136,256]{2,1,0:T(8,128)(2,1)S(1)}, bf16[4,136,256]{2,1,0:T(8,128)(2,1)S(1)}, u32[]{:S(2)}, u32[]{:S(2)}) collective-permute-start(bf16[4,136,256]{2,1,0:T(8,128)(2,1)S(1)} %dynamic-slice_bitcast_fusion), channel_id=1, source_target_pairs={{0,224},{4,228},{8,232},{12,236},{16,240},{20,244},{24,248},{28,25... | collective-permute-start | bytes 835592 | tf_op jit(solution)/shard_map/ppermute | solution.py:226
  24.0 6.0 %collective-permute-done.below = bf16[4,136,256]{2,1,0:T(8,128)(2,1)S(1)} collective-permute-done((bf16[4,136,256]{2,1,0:T(8,128)(2,1)S(1)}, bf16[4,136,256]{2,1,0:T(8,128)(2,1)S(1)}, u32[]{:S(2)}, u32[]{:S(2)}) %collective-permute-start) | collective-permute-done | bytes 278560 | tf_op jit(solution)/shard_map/ppermute | solution.py:226
  30.0 2.7 %collective-permute-start.6 = (bf16[4,136,256]{2,1,0:T(8,128)(2,1)S(1)}, bf16[4,136,256]{2,1,0:T(8,128)(2,1)S(1)}, u32[]{:S(2)}, u32[]{:S(2)}) collective-permute-start(bf16[4,136,256]{2,1,0:T(8,128)(2,1)S(1)} %collective-permute-done.5.above), channel_id=1, source_target_pairs={{0,224},{4,228},{8,232},{12,236},{16,240},{20,244},{24,248},{28,25... | collective-permute-start | bytes 835592 | tf_op jit(solution)/shard_map/ppermute | solution.py:226
  32.7 5.2 %collective-permute-done.1.below = bf16[4,136,256]{2,1,0:T(8,128)(2,1)S(1)} collective-permute-done((bf16[4,136,256]{2,1,0:T(8,128)(2,1)S(1)}, bf16[4,136,256]{2,1,0:T(8,128)(2,1)S(1)}, u32[]{:S(2)}, u32[]{:S(2)}) %collective-permute-start.1) | collective-permute-done | bytes 278560 | tf_op jit(solution)/shard_map/ppermute | solution.py:226
  37.9 2.7 %collective-permute-start.7 = (bf16[4,136,256]{2,1,0:T(8,128)(2,1)S(1)}, bf16[4,136,256]{2,1,0:T(8,128)(2,1)S(1)}, u32[]{:S(2)}, u32[]{:S(2)}) collective-permute-start(bf16[4,136,256]{2,1,0:T(8,128)(2,1)S(1)} %collective-permute-done.6.above), channel_id=1, source_target_pairs={{0,224},{4,228},{8,232},{12,236},{16,240},{20,244},{24,248},{28,25... | collective-permute-start | bytes 835592 | tf_op jit(solution)/shard_map/ppermute | solution.py:226
  40.6 3.0 %collective-permute-start.10 = (bf16[8,136,256]{2,1,0:T(8,128)(2,1)S(1)}, bf16[8,136,256]{2,1,0:T(8,128)(2,1)S(1)}, u32[]{:S(2)}, u32[]{:S(2)}) collective-permute-start(bf16[8,136,256]{2,1,0:T(8,128)(2,1)S(1)} %pad_maximum_fusion.2), channel_id=1, source_target_pairs={{0,4},{4,0},{8,12},{12,8},{16,20},{20,16},{24,28},{28,24},{32,36},... | collective-permute-start | bytes 1671176 | tf_op jit(solution)/shard_map/ppermute | solution.py:226
  45.0 3.3 %collective-permute-start.8 = (bf16[8,136,256]{2,1,0:T(8,128)(2,1)S(1)}, bf16[8,136,256]{2,1,0:T(8,128)(2,1)S(1)}, u32[]{:S(2)}, u32[]{:S(2)}) collective-permute-start(bf16[8,136,256]{2,1,0:T(8,128)(2,1)S(1)} %pad_maximum_fusion), channel_id=1, source_target_pairs={{0,4},{4,0},{8,12},{12,8},{16,20},{20,16},{24,28},{28,24},{32,36},... | collective-permute-start | bytes 1671176 | tf_op jit(solution)/shard_map/ppermute | solution.py:226
  49.7 8.3 %collective-permute-done.3.below = bf16[4,136,256]{2,1,0:T(8,128)(2,1)S(1)} collective-permute-done((bf16[4,136,256]{2,1,0:T(8,128)(2,1)S(1)}, bf16[4,136,256]{2,1,0:T(8,128)(2,1)S(1)}, u32[]{:S(2)}, u32[]{:S(2)}) %collective-permute-start.3) | collective-permute-done | bytes 278560 | tf_op jit(solution)/shard_map/ppermute | solution.py:226
  64.3 4.3 %all-to-all-start.3 = ((bf16[4,32,4096]{2,1,0:T(8,128)(2,1)}), bf16[4,32,4096]{2,1,0:T(8,128)(2,1)S(1)}, u32[]{:S(2)}, u32[]{:S(2)}) async-start(bf16[4,32,4096]{2,1,0:T(8,128)(2,1)} %bitcast.5), calls=%async_computation.3 | async-start | bytes 2097152 | tf_op jit(solution)/shard_map/all_to_all | solution.py:545
  69.2 14.3 %all-to-all-done.3.mixed_ref = bf16[4,32,4096]{2,1,0:T(8,128)(2,1)S(1)} async-done(((bf16[4,32,4096]{2,1,0:T(8,128)(2,1)}), bf16[4,32,4096]{2,1,0:T(8,128)(2,1)S(1)}, u32[]{:S(2)}, u32[]{:S(2)}) %all-to-all-start.3) | async-done | bytes 1048608 | tf_op jit(solution)/shard_map/all_to_all | solution.py:545
  84.2 47.1 %all_to_all.30.arrived_ref = bf16[64,2,4096]{2,1,0:T(2,128)(2,1)S(1)} all-to-all(bf16[64,2,4096]{2,1,0:T(2,128)(2,1)S(1)} %get-tuple-element.71), channel_id=1, replica_groups=mesh['sp'=64,'tp'=4] {'sp'}, dimensions={0} | all-to-all | bytes 2097152 | tf_op jit(solution)/shard_map/all_to_all | solution.py:553
  131.4 2.8 %shard_map.133 = (bf16[48,4096]{1,0:T(8,128)(2,1)S(1)}, bf16[40,4096]{1,0:T(8,128)(2,1)S(1)}, bf16[40,4096]{1,0:T(8,128)(2,1)}, bf16[128,128]{1,0:T(8,128)(2,1)S(1)}) custom-call(bf16[64,2,4096]{2,1,0:T(2,128)(2,1)S(1)} %all_to_all.30.arrived_ref), custom_call_target="tpu_custom_call" | custom-call | flops 134217728 | tf_op jit(solution)/shard_map/pallas_call | solution.py:268
  136.8 8.1 %collective-permute-done.11.refs_0_ = bf16[48,4096]{1,0:T(8,128)(2,1)S(1)} collective-permute-done((bf16[48,4096]{1,0:T(8,128)(2,1)S(1)}, bf16[48,4096]{1,0:T(8,128)(2,1)S(1)}, u32[]{:S(2)}, u32[]{:S(2)}) %collective-permute-start.11) | collective-permute-done | bytes 393248 | tf_op jit(solution)/shard_map/ppermute | solution.py:433
  144.9 2.7 %collective-permute-start.16 = (bf16[40,4096]{1,0:T(8,128)(2,1)S(1)}, bf16[40,4096]{1,0:T(8,128)(2,1)S(1)}, u32[]{:S(2)}, u32[]{:S(2)}) collective-permute-start(bf16[40,4096]{1,0:T(8,128)(2,1)S(1)} %collective-permute-done.14.refs_3_), channel_id=1, source_target_pairs={{0,3},{1,0},{2,1},{3,2},{4,7},{5,4},{6,5},{7,6},{8,11},{9,8},{10,9... | collective-permute-start | bytes 983048 | tf_op jit(solution)/shard_map/ppermute | solution.py:433
  149.0 3.3 %collective-permute-done.16.refs_1_ = bf16[40,4096]{1,0:T(8,128)(2,1)S(1)} collective-permute-done((bf16[40,4096]{1,0:T(8,128)(2,1)S(1)}, bf16[40,4096]{1,0:T(8,128)(2,1)S(1)}, u32[]{:S(2)}, u32[]{:S(2)}) %collective-permute-start.16) | collective-permute-done | bytes 327712 | tf_op jit(solution)/shard_map/ppermute | solution.py:433
  154.8 4.0 %shard_map.136 = (bf16[48,4096]{1,0:T(8,128)(2,1)S(1)}, bf16[40,4096]{1,0:T(8,128)(2,1)S(1)}) custom-call(bf16[48,4096]{1,0:T(8,128)(2,1)S(1)} %collective-permute-done.15.refs_0_, bf16[40,4096]{1,0:T(8,128)(2,1)S(1)} %collective-permute-done.16.refs_1_, bf16[4096,256]{1,0:T(8,128)(2,1)S(1)} %bitcast.27, bf16[4096,256]{1,0:T(8,128)(2,1)S(1)} %bitcast.31, ...), custom_call_target="tpu_custom_call" | custom-call | flops 553648128 | tf_op jit(solution)/shard_map/pallas_call | solution.py:268
  158.8 2.7 %collective-permute-start.18 = (bf16[40,4096]{1,0:T(8,128)(2,1)S(1)}, bf16[40,4096]{1,0:T(8,128)(2,1)S(1)}, u32[]{:S(2)}, u32[]{:S(2)}) collective-permute-start(bf16[40,4096]{1,0:T(8,128)(2,1)S(1)} %get-tuple-element.81), channel_id=1, source_target_pairs={{0,3},{1,0},{2,1},{3,2},{4,7},{5,4},{6,5},{7,6},{8,11},{9,8},{10,9... | collective-permute-start | bytes 983048 | tf_op jit(solution)/shard_map/ppermute | solution.py:433
  161.8 3.4 %shard_map.135 = (bf16[48,4096]{1,0:T(8,128)(2,1)S(1)}, bf16[40,4096]{1,0:T(8,128)(2,1)S(1)}, bf16[48,4096]{1,0:T(8,128)(2,1)S(1)}, bf16[40,4096]{1,0:T(8,128)(2,1)}) custom-call(bf16[48,4096]{1,0:T(8,128)(2,1)S(1)} %collective-permute-done.11.refs_0_, bf16[40,4096]{1,0:T(8,128)(2,1)S(1)} %collective-permute-done.12.refs_1_, ...), custom_call_target="tpu_custom_call" | custom-call | flops 1107296256 | tf_op jit(solution)/shard_map/pallas_call | solution.py:268
  173.3 5.1 %shard_map.134 = (bf16[48,4096]{1,0:T(8,128)(2,1)S(1)}, bf16[40,4096]{1,0:T(8,128)(2,1)S(1)}) custom-call(bf16[48,4096]{1,0:T(8,128)(2,1)S(1)} %get-tuple-element.75.refs_0_, bf16[40,4096]{1,0:T(8,128)(2,1)S(1)} %get-tuple-element.76.refs_1_, bf16[4096,256]{1,0:T(8,128)(2,1)} %bitcast.26, bf16[4096,256]{1,0:T(8,128)(2,1)} %bitcast.30, bf16[256,4096]{1,0:T(8,128)(2,1)} %bitcast.35), custom_call_target="tpu_custom_call" | custom-call | flops 553648128 | tf_op jit(solution)/shard_map/pallas_call | solution.py:268
  180.5 3.2 %collective-permute-done.22.refs_5_ = bf16[40,4096]{1,0:T(8,128)(2,1)S(1)} collective-permute-done((bf16[40,4096]{1,0:T(8,128)(2,1)}, bf16[40,4096]{1,0:T(8,128)(2,1)S(1)}, u32[]{:S(2)}, u32[]{:S(2)}) %collective-permute-start.22) | collective-permute-done | bytes 327712 | tf_op jit(solution)/shard_map/ppermute | solution.py:433
  185.7 12.8 %all-to-all-start.5 = ((bf16[64,2,4096]{2,1,0:T(2,128)(2,1)}), bf16[64,2,4096]{2,1,0:T(2,128)(2,1)S(1)}, u32[]{:S(2)}, u32[]{:S(2)}) async-start(bf16[64,2,4096]{2,1,0:T(2,128)(2,1)} %shard_map.138), calls=%async_computation.5 | async-start | bytes 2097152 | tf_op jit(solution)/shard_map/all_to_all | solution.py:555
  198.7 28.0 %all-to-all-done.5.returned_ref = bf16[64,2,4096]{2,1,0:T(2,128)(2,1)S(1)} async-done(((bf16[64,2,4096]{2,1,0:T(2,128)(2,1)}), bf16[64,2,4096]{2,1,0:T(2,128)(2,1)S(1)}, u32[]{:S(2)}, u32[]{:S(2)}) %all-to-all-start.5) | async-done | bytes 1048608 | tf_op jit(solution)/shard_map/all_to_all | solution.py:555
  (91 shorter events, 34.6 us)
Async XLA Ops:
  2.8 16.4 %all-to-all-start.2 = ((bf16[8,136,256]{2,1,0:T(8,128)(2,1)}), bf16[8,136,256]{2,1,0:T(8,128)(2,1)S(1)}, u32[]{:S(2)}, u32[]{:S(2)}) async-start(bf16[8,136,256]{2,1,0:T(8,128)(2,1)} %broadcast_in_dim.17), calls=%async_computation.2 | async-start | bytes 1114112 | tf_op jit(solution)/shard_map/all_to_all | solution.py:238
  19.2 10.8 %collective-permute-start = (bf16[4,136,256]{2,1,0:T(8,128)(2,1)S(1)}, bf16[4,136,256]{2,1,0:T(8,128)(2,1)S(1)}, u32[]{:S(2)}, u32[]{:S(2)}) collective-permute-start(bf16[4,136,256]{2,1,0:T(8,128)(2,1)S(1)} %dynamic-slice_bitcast_fusion), channel_id=1, source_target_pairs={{0,32},{4,36},{8,40},{12,44},{16,48},{20,52},{24,56},{28,60},{32,6... | collective-permute-start | bytes 835592 | tf_op jit(solution)/shard_map/ppermute | solution.py:226
  20.0 10.0 %collective-permute-start.5 = (bf16[4,136,256]{2,1,0:T(8,128)(2,1)S(1)}, bf16[4,136,256]{2,1,0:T(8,128)(2,1)S(1)}, u32[]{:S(2)}, u32[]{:S(2)}) collective-permute-start(bf16[4,136,256]{2,1,0:T(8,128)(2,1)S(1)} %dynamic-slice_bitcast_fusion), channel_id=1, source_target_pairs={{0,224},{4,228},{8,232},{12,236},{16,240},{20,244},{24,248},{28,25... | collective-permute-start | bytes 835592 | tf_op jit(solution)/shard_map/ppermute | solution.py:226
  30.0 7.9 %collective-permute-start.1 = (bf16[4,136,256]{2,1,0:T(8,128)(2,1)S(1)}, bf16[4,136,256]{2,1,0:T(8,128)(2,1)S(1)}, u32[]{:S(2)}, u32[]{:S(2)}) collective-permute-start(bf16[4,136,256]{2,1,0:T(8,128)(2,1)S(1)} %collective-permute-done.below), channel_id=1, source_target_pairs={{0,32},{4,36},{8,40},{12,44},{16,48},{20,52},{24,56},{28,60},{32,6... | collective-permute-start | bytes 835592 | tf_op jit(solution)/shard_map/ppermute | solution.py:226
  30.0 7.9 %collective-permute-start.6 = (bf16[4,136,256]{2,1,0:T(8,128)(2,1)S(1)}, bf16[4,136,256]{2,1,0:T(8,128)(2,1)S(1)}, u32[]{:S(2)}, u32[]{:S(2)}) collective-permute-start(bf16[4,136,256]{2,1,0:T(8,128)(2,1)S(1)} %collective-permute-done.5.above), channel_id=1, source_target_pairs={{0,224},{4,228},{8,232},{12,236},{16,240},{20,244},{24,248},{28,25... | collective-permute-start | bytes 835592 | tf_op jit(solution)/shard_map/ppermute | solution.py:226
  37.9 7.0 %collective-permute-start.2 = (bf16[4,136,256]{2,1,0:T(8,128)(2,1)S(1)}, bf16[4,136,256]{2,1,0:T(8,128)(2,1)S(1)}, u32[]{:S(2)}, u32[]{:S(2)}) collective-permute-start(bf16[4,136,256]{2,1,0:T(8,128)(2,1)S(1)} %collective-permute-done.1.below), channel_id=1, source_target_pairs={{0,32},{4,36},{8,40},{12,44},{16,48},{20,52},{24,56},{28,60},{32,6... | collective-permute-start | bytes 835592 | tf_op jit(solution)/shard_map/ppermute | solution.py:226
  40.6 18.1 %collective-permute-start.10 = (bf16[8,136,256]{2,1,0:T(8,128)(2,1)S(1)}, bf16[8,136,256]{2,1,0:T(8,128)(2,1)S(1)}, u32[]{:S(2)}, u32[]{:S(2)}) collective-permute-start(bf16[8,136,256]{2,1,0:T(8,128)(2,1)S(1)} %pad_maximum_fusion.2), channel_id=1, source_target_pairs={{0,4},{4,0},{8,12},{12,8},{16,20},{20,16},{24,28},{28,24},{32,36},... | collective-permute-start | bytes 1671176 | tf_op jit(solution)/shard_map/ppermute | solution.py:226
  43.7 15.8 %collective-permute-start.9 = (bf16[8,136,256]{2,1,0:T(8,128)(2,1)S(1)}, bf16[8,136,256]{2,1,0:T(8,128)(2,1)S(1)}, u32[]{:S(2)}, u32[]{:S(2)}) collective-permute-start(bf16[8,136,256]{2,1,0:T(8,128)(2,1)S(1)} %pad_maximum_fusion.1), channel_id=1, source_target_pairs={{0,4},{4,0},{8,12},{12,8},{16,20},{20,16},{24,28},{28,24},{32,36},... | collective-permute-start | bytes 1671176 | tf_op jit(solution)/shard_map/ppermute | solution.py:226
  45.0 15.3 %collective-permute-start.8 = (bf16[8,136,256]{2,1,0:T(8,128)(2,1)S(1)}, bf16[8,136,256]{2,1,0:T(8,128)(2,1)S(1)}, u32[]{:S(2)}, u32[]{:S(2)}) collective-permute-start(bf16[8,136,256]{2,1,0:T(8,128)(2,1)S(1)} %pad_maximum_fusion), channel_id=1, source_target_pairs={{0,4},{4,0},{8,12},{12,8},{16,20},{20,16},{24,28},{28,24},{32,36},... | collective-permute-start | bytes 1671176 | tf_op jit(solution)/shard_map/ppermute | solution.py:226
  48.3 9.7 %collective-permute-start.3 = (bf16[4,136,256]{2,1,0:T(8,128)(2,1)S(1)}, bf16[4,136,256]{2,1,0:T(8,128)(2,1)S(1)}, u32[]{:S(2)}, u32[]{:S(2)}) collective-permute-start(bf16[4,136,256]{2,1,0:T(8,128)(2,1)S(1)} %collective-permute-done.2.below), channel_id=1, source_target_pairs={{0,32},{4,36},{8,40},{12,44},{16,48},{20,52},{24,56},{28,60},{32,6... | collective-permute-start | bytes 835592 | tf_op jit(solution)/shard_map/ppermute | solution.py:226
  64.3 19.2 %all-to-all-start.3 = ((bf16[4,32,4096]{2,1,0:T(8,128)(2,1)}), bf16[4,32,4096]{2,1,0:T(8,128)(2,1)S(1)}, u32[]{:S(2)}, u32[]{:S(2)}) async-start(bf16[4,32,4096]{2,1,0:T(8,128)(2,1)} %bitcast.5), calls=%async_computation.3 | async-start | bytes 2097152 | tf_op jit(solution)/shard_map/all_to_all | solution.py:545
  134.2 10.7 %collective-permute-start.11 = (bf16[48,4096]{1,0:T(8,128)(2,1)S(1)}, bf16[48,4096]{1,0:T(8,128)(2,1)S(1)}, u32[]{:S(2)}, u32[]{:S(2)}) collective-permute-start(bf16[48,4096]{1,0:T(8,128)(2,1)S(1)} %get-tuple-element.75.refs_0_), channel_id=1, source_target_pairs={{0,1},{1,2},{2,3},{3,0},{4,5},{5,6},{6,7},{7,4},{8,9},{9,10},{10,1... | collective-permute-start | bytes 1179656 | tf_op jit(solution)/shard_map/ppermute | solution.py:433
  134.4 10.5 %collective-permute-start.14 = (bf16[40,4096]{1,0:T(8,128)(2,1)S(1)}, bf16[40,4096]{1,0:T(8,128)(2,1)S(1)}, u32[]{:S(2)}, u32[]{:S(2)}) collective-permute-start(bf16[40,4096]{1,0:T(8,128)(2,1)S(1)} %get-tuple-element.76.refs_1_), channel_id=1, source_target_pairs={{0,3},{1,0},{2,1},{3,2},{4,7},{5,4},{6,5},{7,6},{8,11},{9,8},{10,9... | collective-permute-start | bytes 983048 | tf_op jit(solution)/shard_map/ppermute | solution.py:433
  144.9 9.9 %collective-permute-start.15 = (bf16[48,4096]{1,0:T(8,128)(2,1)S(1)}, bf16[48,4096]{1,0:T(8,128)(2,1)S(1)}, u32[]{:S(2)}, u32[]{:S(2)}) collective-permute-start(bf16[48,4096]{1,0:T(8,128)(2,1)S(1)} %collective-permute-done.11.refs_0_), channel_id=1, source_target_pairs={{0,1},{1,2},{2,3},{3,0},{4,5},{5,6},{6,7},{7,4},{8,9},{9,10},{10,1... | collective-permute-start | bytes 1179656 | tf_op jit(solution)/shard_map/ppermute | solution.py:433
  144.9 7.5 %collective-permute-start.16 = (bf16[40,4096]{1,0:T(8,128)(2,1)S(1)}, bf16[40,4096]{1,0:T(8,128)(2,1)S(1)}, u32[]{:S(2)}, u32[]{:S(2)}) collective-permute-start(bf16[40,4096]{1,0:T(8,128)(2,1)S(1)} %collective-permute-done.14.refs_3_), channel_id=1, source_target_pairs={{0,3},{1,0},{2,1},{3,2},{4,7},{5,4},{6,5},{7,6},{8,11},{9,8},{10,9... | collective-permute-start | bytes 983048 | tf_op jit(solution)/shard_map/ppermute | solution.py:433
  147.6 14.2 %collective-permute-start.13 = (bf16[48,4096]{1,0:T(8,128)(2,1)S(1)}, bf16[48,4096]{1,0:T(8,128)(2,1)S(1)}, u32[]{:S(2)}, u32[]{:S(2)}) collective-permute-start(bf16[48,4096]{1,0:T(8,128)(2,1)S(1)} %get-tuple-element.75.refs_0_), channel_id=1, source_target_pairs={{0,3},{1,0},{2,1},{3,2},{4,7},{5,4},{6,5},{7,6},{8,11},{9,8},{10,9... | collective-permute-start | bytes 1179656 | tf_op jit(solution)/shard_map/ppermute | solution.py:433
  147.6 14.2 %collective-permute-start.12 = (bf16[40,4096]{1,0:T(8,128)(2,1)S(1)}, bf16[40,4096]{1,0:T(8,128)(2,1)S(1)}, u32[]{:S(2)}, u32[]{:S(2)}) collective-permute-start(bf16[40,4096]{1,0:T(8,128)(2,1)S(1)} %get-tuple-element.76.refs_1_), channel_id=1, source_target_pairs={{0,1},{1,2},{2,3},{3,0},{4,5},{5,6},{6,7},{7,4},{8,9},{9,10},{10,1... | collective-permute-start | bytes 983048 | tf_op jit(solution)/shard_map/ppermute | solution.py:433
  158.8 9.4 %collective-permute-start.17 = (bf16[48,4096]{1,0:T(8,128)(2,1)S(1)}, bf16[48,4096]{1,0:T(8,128)(2,1)S(1)}, u32[]{:S(2)}, u32[]{:S(2)}) collective-permute-start(bf16[48,4096]{1,0:T(8,128)(2,1)S(1)} %get-tuple-element.79), channel_id=1, source_target_pairs={{0,1},{1,2},{2,3},{3,0},{4,5},{5,6},{6,7},{7,4},{8,9},{9,10},{10,1... | collective-permute-start | bytes 1179656 | tf_op jit(solution)/shard_map/ppermute | solution.py:433
  158.8 8.8 %collective-permute-start.18 = (bf16[40,4096]{1,0:T(8,128)(2,1)S(1)}, bf16[40,4096]{1,0:T(8,128)(2,1)S(1)}, u32[]{:S(2)}, u32[]{:S(2)}) collective-permute-start(bf16[40,4096]{1,0:T(8,128)(2,1)S(1)} %get-tuple-element.81), channel_id=1, source_target_pairs={{0,3},{1,0},{2,1},{3,2},{4,7},{5,4},{6,5},{7,6},{8,11},{9,8},{10,9... | collective-permute-start | bytes 983048 | tf_op jit(solution)/shard_map/ppermute | solution.py:433
  165.2 15.2 %collective-permute-start.20 = (bf16[48,4096]{1,0:T(8,128)(2,1)S(1)}, bf16[48,4096]{1,0:T(8,128)(2,1)S(1)}, u32[]{:S(2)}, u32[]{:S(2)}) collective-permute-start(bf16[48,4096]{1,0:T(8,128)(2,1)S(1)} %get-tuple-element.83), channel_id=1, source_target_pairs={{0,3},{1,0},{2,1},{3,2},{4,7},{5,4},{6,5},{7,6},{8,11},{9,8},{10,9... | collective-permute-start | bytes 1179656 | tf_op jit(solution)/shard_map/ppermute | solution.py:433
  169.1 14.6 %collective-permute-start.19 = (bf16[48,4096]{1,0:T(8,128)(2,1)S(1)}, bf16[48,4096]{1,0:T(8,128)(2,1)S(1)}, u32[]{:S(2)}, u32[]{:S(2)}) collective-permute-start(bf16[48,4096]{1,0:T(8,128)(2,1)S(1)} %get-tuple-element.82), channel_id=1, source_target_pairs={{0,1},{1,2},{2,3},{3,0},{4,5},{5,6},{6,7},{7,4},{8,9},{9,10},{10,1... | collective-permute-start | bytes 1179656 | tf_op jit(solution)/shard_map/ppermute | solution.py:433
  169.1 11.3 %collective-permute-start.21 = (bf16[40,4096]{1,0:T(8,128)(2,1)}, bf16[40,4096]{1,0:T(8,128)(2,1)S(1)}, u32[]{:S(2)}, u32[]{:S(2)}) collective-permute-start(bf16[40,4096]{1,0:T(8,128)(2,1)} %get-tuple-element.85), channel_id=1, source_target_pairs={{0,1},{1,2},{2,3},{3,0},{4,5},{5,6},{6,7},{7,4},{8,9},{9,10},{10,1... | collective-permute-start | bytes 983048 | tf_op jit(solution)/shard_map/ppermute | solution.py:433
  169.6 14.1 %collective-permute-start.22 = (bf16[40,4096]{1,0:T(8,128)(2,1)}, bf16[40,4096]{1,0:T(8,128)(2,1)S(1)}, u32[]{:S(2)}, u32[]{:S(2)}) collective-permute-start(bf16[40,4096]{1,0:T(8,128)(2,1)} %get-tuple-element.86), channel_id=1, source_target_pairs={{0,3},{1,0},{2,1},{3,2},{4,7},{5,4},{6,5},{7,6},{8,11},{9,8},{10,9... | collective-permute-start | bytes 983048 | tf_op jit(solution)/shard_map/ppermute | solution.py:433
  185.7 41.0 %all-to-all-start.5 = ((bf16[64,2,4096]{2,1,0:T(2,128)(2,1)}), bf16[64,2,4096]{2,1,0:T(2,128)(2,1)S(1)}, u32[]{:S(2)}, u32[]{:S(2)}) async-start(bf16[64,2,4096]{2,1,0:T(2,128)(2,1)} %shard_map.138), calls=%async_computation.5 | async-start | bytes 2097152 | tf_op jit(solution)/shard_map/all_to_all | solution.py:555
  (14 other events, 524.9 us)

commit v2 on v1

--- a/solution.py
+++ b/solution.py
@@ -26,6 +26,7 @@
 
 LOG2E = 1.4426950408889634
 KEY_BLOCK = 256
+MOST = 100.0
 PICK_ROWS = 8
 
 
@@ -47,8 +48,7 @@
     breaks, leads = [], []
     for head in range(heads):
         z = scores[head * rows : (head + 1) * rows] * factor + bias_ref[head] * LOG2E
-        log_term = jnp.log2(1.0 + jnp.exp2(-jnp.abs(z)))
-        softplus = jnp.maximum(z, 0.0) + log_term
+        softplus = jnp.maximum(jnp.log2(1.0 + jnp.exp2(jnp.minimum(z, MOST))), z)
         leads.append(z - softplus)
         breaks.append(softplus if first_query is None else jnp.where(before, softplus, 0.0))
     behind = jnp.dot(
@@ -79,12 +79,13 @@
 
 
 def lay_out(own_ref, twin_ref, plane, place):
+    lanes = (place // CORES) % X_SIZE
     core = place % CORES
     length = own_ref.shape[1] - PICK_ROWS
-    for lane in range(X_SIZE):
-        first = lane * CORES * length
-        plane[pl.ds(pl.multiple_of(first + core * length, length), length)] = own_ref[lane, :length]
-        plane[pl.ds(pl.multiple_of(first + (1 - core) * length, length), length)] = twin_ref[lane, :length]
+    for shift in range(X_SIZE):
+        source = ((lanes + X_SIZE - shift) % X_SIZE) * CORES
+        plane[pl.ds(pl.multiple_of((source + core) * length, length), length)] = own_ref[shift, :length]
+        plane[pl.ds(pl.multiple_of((source + 1 - core) * length, length), length)] = twin_ref[shift, :length]
 
 
 def tally(counts, *pieces):
@@ -98,15 +99,14 @@
     counts[...] = found
 
 
-def own_plane_kernel(place_ref, bias_ref, query_ref, blocks_ref, near, near_used, far, counts, plane):
+def own_plane_kernel(place_ref, bias_ref, query_ref, own_ref, twin_ref, near, near_used, far, counts, plane):
     place = place_ref[0]
-    rows = query_ref.shape[0] // bias_ref.shape[0]
-    for block in range(Z_PLANE):
-        plane[block * rows : (block + 1) * rows] = blocks_ref[block, :rows]
+    lay_out(own_ref, twin_ref, plane, place)
     for ref in (near, near_used, far, counts):
         ref[...] = jnp.zeros_like(ref)
-    tally(counts, blocks_ref)
+    tally(counts, own_ref, twin_ref)
     later = later_keys()
+    rows = query_ref.shape[0] // bias_ref.shape[0]
     first_query = (place % (X_SIZE * CORES)) * rows
     last = (first_query + rows - 1) // KEY_BLOCK
 
@@ -233,11 +233,8 @@
     picks = pick_ids.astype(jnp.bfloat16).reshape(1, rows * TOP)
     picks = jnp.concatenate([picks, jnp.zeros((PICK_ROWS - 1, rows * TOP), jnp.bfloat16)], axis=0)
     block = jnp.concatenate([jnp.concatenate([keys, values], axis=1), picks], axis=0)
-    groups = [[z * Z_PLANE + w for w in range(Z_PLANE)] for z in range(Z_SIZE)]
-    copies = jnp.broadcast_to(block[None], (Z_PLANE, *block.shape))
-    blocks = lax.all_to_all(copies, "sp", 0, 0, axis_index_groups=groups, tiled=True)
-    by_core = blocks.reshape(X_SIZE, CORES, *block.shape)
-    own = lax.dynamic_index_in_dim(by_core, position[0] % CORES, 1, keepdims=False)
+    own = jnp.stack([block] + [moved(block, 0, step, 0) for step in range(1, X_SIZE)])
+    twin = moved(own, 0, 0, 1)
     common = (position, break_bias, stacked)
     below, above = own, own
     arrived = []
@@ -249,7 +246,7 @@
             arrived.append((below, above, moved(both, 0, 0, 1)))
         else:
             arrived.append((below, moved(below, 0, 0, 1)))
-    state = attention_call(own_plane_kernel, "attend_0", 1, *common, (blocks,), (), rows)
+    state = attention_call(own_plane_kernel, "attend_0", 1, *common, (own, twin), (), rows)
     for distance in range(1, Z_SIZE // 2):
         kernel = functools.partial(two_planes_kernel, distance)
         name = f"attend_{distance}"

time: 229 us -> 221 us (0.965)
  waiting for transfers between devices: 92.4 us -> 81.3 us
  other arithmetic: 1.9 us -> 5.22 us
    all_to_all x1 -> x0, waiting for transfers between devices: 9.73 us -> none  [attend(): lax.all_to_all(copies, 'sp', 0, 0, axis_index_groups=groups, tiled=True)]
    ppermute x11 -> x15, starting transfers between devices: 17.5 us -> 24.3 us  [moved(): return lax.ppermute(shard, 'sp', pairs)]
    all_to_all x1 -> x0, starting transfers between devices: 6.64 us -> none  [attend(): lax.all_to_all(copies, 'sp', 0, 0, axis_index_groups=groups, tiled=True)]
    concatenate x3, other arithmetic: 0.15 us -> 2.57 us  [attend(): both = jnp.concatenate([below, above], axis=0)]
    ppermute x11 -> x15, waiting for transfers between devices: 20.5 us -> 19.2 us  [moved(): return lax.ppermute(shard, 'sp', pairs)]
  transfers between devices with their start and end apart: 26 -> 29, of which waited for: 14 -> 14; matrix products, arithmetic and copies ran while one was open for 1% -> 2% of each run, Pallas kernels for 7% -> 8%
where the time goes in v2:
time: 221 us
  waiting for transfers between devices  81.3 us (37%)
  starting transfers between devices  56.1 us (25%)
  blocking collectives  47.1 us (21%)
  Pallas kernels  26.3 us (12%)
  other arithmetic  5.22 us (2%)
    all_to_all x1, blocking collectives, on_device(): lax.all_to_all(outgoing, 'sp', split_axis=0, concat_axis=0, tiled=True)  47.1 us
    all_to_all x1, waiting for transfers between devices, on_device(): lax.all_to_all(results, 'sp', split_axis=0, concat_axis=0, tiled=True)  28 us
    ppermute x15, starting transfers between devices, moved(): return lax.ppermute(shard, 'sp', pairs)  24.3 us
    pallas_call x8, Pallas kernels, in_kernel(): pl.pallas_call(kernel, out_shape=out_shapes, in_specs=[spec] * len(operan...  20.3 us
    ppermute x12, waiting for transfers between devices, along_tp(): lax.ppermute(shard, 'tp', [(member, (member + step) % size) for member in...  19.9 us
    ppermute x15, waiting for transfers between devices, moved(): return lax.ppermute(shard, 'sp', pairs)  19.2 us
    ppermute x12, starting transfers between devices, along_tp(): lax.ppermute(shard, 'tp', [(member, (member + step) % size) for member in...  14.7 us
    all_to_all x1, waiting for transfers between devices, on_device(): mixed = lax.all_to_all(parts, 'tp', split_axis=0, concat_axis=0, tiled=True)  14.2 us
  transfers between devices with their start and end apart: 29, of which 14 were waited for; matrix products, arithmetic and copies ran while one was open for 2% of the time, Pallas kernels for 8%

profile of v2, /device:TPU:1, one launch (start us, length us, event | category | flops | bytes accessed | tf_op | source)
XLA Modules:
  0.0 220.6 jit_solution(10601944549201611825)
XLA Ops:
  4.1 2.5 %collective-permute-start.1 = (bf16[136,256]{1,0:T(8,128)(2,1)S(1)}, bf16[136,256]{1,0:T(8,128)(2,1)S(1)}, u32[]{:S(2)}, u32[]{:S(2)}) collective-permute-start(bf16[136,256]{1,0:T(8,128)(2,1)S(1)} %maximum_maximum_fusion), channel_id=1, source_target_pairs={{0,16},{4,20},{8,24},{12,28},{16,0},{20,4},{24,8},{28,12},{32,48},... | collective-permute-start | bytes 208904 | tf_op jit(solution)/shard_map/ppermute | solution.py:226
  12.0 4.0 %collective-permute-start.8 = (bf16[4,136,256]{2,1,0:T(8,128)(2,1)S(1)}, bf16[4,136,256]{2,1,0:T(8,128)(2,1)S(1)}, u32[]{:S(2)}, u32[]{:S(2)}) collective-permute-start(bf16[4,136,256]{2,1,0:T(8,128)(2,1)S(1)} %pad_maximum_fusion.3.own_ref), channel_id=1, source_target_pairs={{0,224},{4,228},{8,232},{12,236},{16,240},{20,244},{24,248},{28,25... | collective-permute-start | bytes 835592 | tf_op jit(solution)/shard_map/ppermute | solution.py:226
  16.0 5.1 %collective-permute-done.3.below = bf16[4,136,256]{2,1,0:T(8,128)(2,1)S(1)} collective-permute-done((bf16[4,136,256]{2,1,0:T(8,128)(2,1)S(1)}, bf16[4,136,256]{2,1,0:T(8,128)(2,1)S(1)}, u32[]{:S(2)}, u32[]{:S(2)}) %collective-permute-start.3) | collective-permute-done | bytes 278560 | tf_op jit(solution)/shard_map/ppermute | solution.py:226
  21.2 2.7 %collective-permute-start.9 = (bf16[4,136,256]{2,1,0:T(8,128)(2,1)S(1)}, bf16[4,136,256]{2,1,0:T(8,128)(2,1)S(1)}, u32[]{:S(2)}, u32[]{:S(2)}) collective-permute-start(bf16[4,136,256]{2,1,0:T(8,128)(2,1)S(1)} %collective-permute-done.8.above), channel_id=1, source_target_pairs={{0,224},{4,228},{8,232},{12,236},{16,240},{20,244},{24,248},{28,25... | collective-permute-start | bytes 835592 | tf_op jit(solution)/shard_map/ppermute | solution.py:226
  23.9 4.4 %collective-permute-done.4.below = bf16[4,136,256]{2,1,0:T(8,128)(2,1)S(1)} collective-permute-done((bf16[4,136,256]{2,1,0:T(8,128)(2,1)S(1)}, bf16[4,136,256]{2,1,0:T(8,128)(2,1)S(1)}, u32[]{:S(2)}, u32[]{:S(2)}) %collective-permute-start.4) | collective-permute-done | bytes 278560 | tf_op jit(solution)/shard_map/ppermute | solution.py:226
  28.2 2.7 %collective-permute-start.10 = (bf16[4,136,256]{2,1,0:T(8,128)(2,1)S(1)}, bf16[4,136,256]{2,1,0:T(8,128)(2,1)S(1)}, u32[]{:S(2)}, u32[]{:S(2)}) collective-permute-start(bf16[4,136,256]{2,1,0:T(8,128)(2,1)S(1)} %collective-permute-done.9.above), channel_id=1, source_target_pairs={{0,224},{4,228},{8,232},{12,236},{16,240},{20,244},{24,248},{28,25... | collective-permute-start | bytes 835592 | tf_op jit(solution)/shard_map/ppermute | solution.py:226
  30.9 3.8 %collective-permute-start.14 = (bf16[4,136,256]{2,1,0:T(8,128)(2,1)S(1)}, bf16[4,136,256]{2,1,0:T(8,128)(2,1)}, u32[]{:S(2)}, u32[]{:S(2)}) collective-permute-start(bf16[4,136,256]{2,1,0:T(8,128)(2,1)S(1)} %pad_maximum_fusion.3.own_ref), channel_id=1, source_target_pairs={{0,4},{4,0},{8,12},{12,8},{16,20},{20,16},{24,28},{28,24},{32,36},... | collective-permute-start | bytes 835592 | tf_op jit(solution)/shard_map/ppermute | solution.py:226
  41.9 8.2 %collective-permute-done.6.below = bf16[4,136,256]{2,1,0:T(8,128)(2,1)S(1)} collective-permute-done((bf16[4,136,256]{2,1,0:T(8,128)(2,1)S(1)}, bf16[4,136,256]{2,1,0:T(8,128)(2,1)S(1)}, u32[]{:S(2)}, u32[]{:S(2)}) %collective-permute-start.6) | collective-permute-done | bytes 278560 | tf_op jit(solution)/shard_map/ppermute | solution.py:226
  56.8 4.3 %all-to-all-start.2 = ((bf16[4,32,4096]{2,1,0:T(8,128)(2,1)}), bf16[4,32,4096]{2,1,0:T(8,128)(2,1)S(1)}, u32[]{:S(2)}, u32[]{:S(2)}) async-start(bf16[4,32,4096]{2,1,0:T(8,128)(2,1)} %bitcast.7), calls=%async_computation.2 | async-start | bytes 2097152 | tf_op jit(solution)/shard_map/all_to_all | solution.py:542
  61.8 14.2 %all-to-all-done.2.mixed_ref = bf16[4,32,4096]{2,1,0:T(8,128)(2,1)S(1)} async-done(((bf16[4,32,4096]{2,1,0:T(8,128)(2,1)}), bf16[4,32,4096]{2,1,0:T(8,128)(2,1)S(1)}, u32[]{:S(2)}, u32[]{:S(2)}) %all-to-all-start.2) | async-done | bytes 1048608 | tf_op jit(solution)/shard_map/all_to_all | solution.py:542
  76.8 47.1 %all_to_all.25.arrived_ref = bf16[64,2,4096]{2,1,0:T(2,128)(2,1)S(1)} all-to-all(bf16[64,2,4096]{2,1,0:T(2,128)(2,1)S(1)} %get-tuple-element.71), channel_id=1, replica_groups=mesh['sp'=64,'tp'=4] {'sp'}, dimensions={0} | all-to-all | bytes 2097152 | tf_op jit(solution)/shard_map/all_to_all | solution.py:550
  123.9 2.8 %shard_map.133 = (bf16[48,4096]{1,0:T(8,128)(2,1)S(1)}, bf16[40,4096]{1,0:T(8,128)(2,1)S(1)}, bf16[40,4096]{1,0:T(8,128)(2,1)}, bf16[128,128]{1,0:T(8,128)(2,1)S(1)}) custom-call(bf16[64,2,4096]{2,1,0:T(2,128)(2,1)S(1)} %all_to_all.25.arrived_ref), custom_call_target="tpu_custom_call" | custom-call | flops 134217728 | tf_op jit(solution)/shard_map/pallas_call | solution.py:265
  126.9 2.4 %collective-permute-start.18 = (bf16[40,4096]{1,0:T(8,128)(2,1)S(1)}, bf16[40,4096]{1,0:T(8,128)(2,1)S(1)}, u32[]{:S(2)}, u32[]{:S(2)}) collective-permute-start(bf16[40,4096]{1,0:T(8,128)(2,1)S(1)} %get-tuple-element.76.refs_1_), channel_id=1, source_target_pairs={{0,3},{1,0},{2,1},{3,2},{4,7},{5,4},{6,5},{7,6},{8,11},{9,8},{10,9... | collective-permute-start | bytes 983048 | tf_op jit(solution)/shard_map/ppermute | solution.py:430
  129.3 8.1 %collective-permute-done.15.refs_0_ = bf16[48,4096]{1,0:T(8,128)(2,1)S(1)} collective-permute-done((bf16[48,4096]{1,0:T(8,128)(2,1)S(1)}, bf16[48,4096]{1,0:T(8,128)(2,1)S(1)}, u32[]{:S(2)}, u32[]{:S(2)}) %collective-permute-start.15) | collective-permute-done | bytes 393248 | tf_op jit(solution)/shard_map/ppermute | solution.py:430
  137.4 2.7 %collective-permute-start.20 = (bf16[40,4096]{1,0:T(8,128)(2,1)S(1)}, bf16[40,4096]{1,0:T(8,128)(2,1)S(1)}, u32[]{:S(2)}, u32[]{:S(2)}) collective-permute-start(bf16[40,4096]{1,0:T(8,128)(2,1)S(1)} %collective-permute-done.18.refs_3_), channel_id=1, source_target_pairs={{0,3},{1,0},{2,1},{3,2},{4,7},{5,4},{6,5},{7,6},{8,11},{9,8},{10,9... | collective-permute-start | bytes 983048 | tf_op jit(solution)/shard_map/ppermute | solution.py:430
  141.5 3.3 %collective-permute-done.20.refs_1_ = bf16[40,4096]{1,0:T(8,128)(2,1)S(1)} collective-permute-done((bf16[40,4096]{1,0:T(8,128)(2,1)S(1)}, bf16[40,4096]{1,0:T(8,128)(2,1)S(1)}, u32[]{:S(2)}, u32[]{:S(2)}) %collective-permute-start.20) | collective-permute-done | bytes 327712 | tf_op jit(solution)/shard_map/ppermute | solution.py:430
  144.8 2.4 %collective-permute-done.19.refs_0_ = bf16[48,4096]{1,0:T(8,128)(2,1)S(1)} collective-permute-done((bf16[48,4096]{1,0:T(8,128)(2,1)S(1)}, bf16[48,4096]{1,0:T(8,128)(2,1)S(1)}, u32[]{:S(2)}, u32[]{:S(2)}) %collective-permute-start.19) | collective-permute-done | bytes 393248 | tf_op jit(solution)/shard_map/ppermute | solution.py:430
  147.3 4.0 %shard_map.136 = (bf16[48,4096]{1,0:T(8,128)(2,1)S(1)}, bf16[40,4096]{1,0:T(8,128)(2,1)S(1)}) custom-call(bf16[48,4096]{1,0:T(8,128)(2,1)S(1)} %collective-permute-done.19.refs_0_, bf16[40,4096]{1,0:T(8,128)(2,1)S(1)} %collective-permute-done.20.refs_1_, bf16[4096,256]{1,0:T(8,128)(2,1)S(1)} %bitcast.26, bf16[4096,256]{1,0:T(8,128)(2,1)S(1)} %bitcast.30, ...), custom_call_target="tpu_custom_call" | custom-call | flops 553648128 | tf_op jit(solution)/shard_map/pallas_call | solution.py:265
  151.3 2.7 %collective-permute-start.22 = (bf16[40,4096]{1,0:T(8,128)(2,1)S(1)}, bf16[40,4096]{1,0:T(8,128)(2,1)S(1)}, u32[]{:S(2)}, u32[]{:S(2)}) collective-permute-start(bf16[40,4096]{1,0:T(8,128)(2,1)S(1)} %get-tuple-element.81), channel_id=1, source_target_pairs={{0,3},{1,0},{2,1},{3,2},{4,7},{5,4},{6,5},{7,6},{8,11},{9,8},{10,9... | collective-permute-start | bytes 983048 | tf_op jit(solution)/shard_map/ppermute | solution.py:430
  154.3 3.4 %shard_map.135 = (bf16[48,4096]{1,0:T(8,128)(2,1)S(1)}, bf16[40,4096]{1,0:T(8,128)(2,1)S(1)}, bf16[48,4096]{1,0:T(8,128)(2,1)S(1)}, bf16[40,4096]{1,0:T(8,128)(2,1)}) custom-call(bf16[48,4096]{1,0:T(8,128)(2,1)S(1)} %collective-permute-done.15.refs_0_, bf16[40,4096]{1,0:T(8,128)(2,1)S(1)} %collective-permute-done.16.refs_1_, ...), custom_call_target="tpu_custom_call" | custom-call | flops 1107296256 | tf_op jit(solution)/shard_map/pallas_call | solution.py:265
  165.7 5.1 %shard_map.134 = (bf16[48,4096]{1,0:T(8,128)(2,1)S(1)}, bf16[40,4096]{1,0:T(8,128)(2,1)S(1)}) custom-call(bf16[48,4096]{1,0:T(8,128)(2,1)S(1)} %get-tuple-element.75.refs_0_, bf16[40,4096]{1,0:T(8,128)(2,1)S(1)} %get-tuple-element.76.refs_1_, bf16[4096,256]{1,0:T(8,128)(2,1)} %bitcast.25, bf16[4096,256]{1,0:T(8,128)(2,1)} %bitcast.29, bf16[256,4096]{1,0:T(8,128)(2,1)} %bitcast.34), custom_call_target="tpu_custom_call" | custom-call | flops 553648128 | tf_op jit(solution)/shard_map/pallas_call | solution.py:265
  173.0 3.2 %collective-permute-done.26.refs_5_ = bf16[40,4096]{1,0:T(8,128)(2,1)S(1)} collective-permute-done((bf16[40,4096]{1,0:T(8,128)(2,1)}, bf16[40,4096]{1,0:T(8,128)(2,1)S(1)}, u32[]{:S(2)}, u32[]{:S(2)}) %collective-permute-start.26) | collective-permute-done | bytes 327712 | tf_op jit(solution)/shard_map/ppermute | solution.py:430
  178.1 12.9 %all-to-all-start.4 = ((bf16[64,2,4096]{2,1,0:T(2,128)(2,1)}), bf16[64,2,4096]{2,1,0:T(2,128)(2,1)S(1)}, u32[]{:S(2)}, u32[]{:S(2)}) async-start(bf16[64,2,4096]{2,1,0:T(2,128)(2,1)} %shard_map.138), calls=%async_computation.4 | async-start | bytes 2097152 | tf_op jit(solution)/shard_map/all_to_all | solution.py:552
  191.2 28.0 %all-to-all-done.4.returned_ref = bf16[64,2,4096]{2,1,0:T(2,128)(2,1)S(1)} async-done(((bf16[64,2,4096]{2,1,0:T(2,128)(2,1)}), bf16[64,2,4096]{2,1,0:T(2,128)(2,1)S(1)}, u32[]{:S(2)}, u32[]{:S(2)}) %all-to-all-start.4) | async-done | bytes 1048608 | tf_op jit(solution)/shard_map/all_to_all | solution.py:552
  (97 shorter events, 40.6 us)
Async XLA Ops:
  10.0 11.2 %collective-permute-start.3 = (bf16[4,136,256]{2,1,0:T(8,128)(2,1)S(1)}, bf16[4,136,256]{2,1,0:T(8,128)(2,1)S(1)}, u32[]{:S(2)}, u32[]{:S(2)}) collective-permute-start(bf16[4,136,256]{2,1,0:T(8,128)(2,1)S(1)} %pad_maximum_fusion.3.own_ref), channel_id=1, source_target_pairs={{0,32},{4,36},{8,40},{12,44},{16,48},{20,52},{24,56},{28,60},{32,6... | collective-permute-start | bytes 835592 | tf_op jit(solution)/shard_map/ppermute | solution.py:226
  12.0 9.2 %collective-permute-start.8 = (bf16[4,136,256]{2,1,0:T(8,128)(2,1)S(1)}, bf16[4,136,256]{2,1,0:T(8,128)(2,1)S(1)}, u32[]{:S(2)}, u32[]{:S(2)}) collective-permute-start(bf16[4,136,256]{2,1,0:T(8,128)(2,1)S(1)} %pad_maximum_fusion.3.own_ref), channel_id=1, source_target_pairs={{0,224},{4,228},{8,232},{12,236},{16,240},{20,244},{24,248},{28,25... | collective-permute-start | bytes 835592 | tf_op jit(solution)/shard_map/ppermute | solution.py:226
  21.2 7.0 %collective-permute-start.4 = (bf16[4,136,256]{2,1,0:T(8,128)(2,1)S(1)}, bf16[4,136,256]{2,1,0:T(8,128)(2,1)S(1)}, u32[]{:S(2)}, u32[]{:S(2)}) collective-permute-start(bf16[4,136,256]{2,1,0:T(8,128)(2,1)S(1)} %collective-permute-done.3.below), channel_id=1, source_target_pairs={{0,32},{4,36},{8,40},{12,44},{16,48},{20,52},{24,56},{28,60},{32,6... | collective-permute-start | bytes 835592 | tf_op jit(solution)/shard_map/ppermute | solution.py:226
  28.2 8.7 %collective-permute-start.5 = (bf16[4,136,256]{2,1,0:T(8,128)(2,1)S(1)}, bf16[4,136,256]{2,1,0:T(8,128)(2,1)S(1)}, u32[]{:S(2)}, u32[]{:S(2)}) collective-permute-start(bf16[4,136,256]{2,1,0:T(8,128)(2,1)S(1)} %collective-permute-done.4.below), channel_id=1, source_target_pairs={{0,32},{4,36},{8,40},{12,44},{16,48},{20,52},{24,56},{28,60},{32,6... | collective-permute-start | bytes 835592 | tf_op jit(solution)/shard_map/ppermute | solution.py:226
  28.2 8.7 %collective-permute-start.10 = (bf16[4,136,256]{2,1,0:T(8,128)(2,1)S(1)}, bf16[4,136,256]{2,1,0:T(8,128)(2,1)S(1)}, u32[]{:S(2)}, u32[]{:S(2)}) collective-permute-start(bf16[4,136,256]{2,1,0:T(8,128)(2,1)S(1)} %collective-permute-done.9.above), channel_id=1, source_target_pairs={{0,224},{4,228},{8,232},{12,236},{16,240},{20,244},{24,248},{28,25... | collective-permute-start | bytes 835592 | tf_op jit(solution)/shard_map/ppermute | solution.py:226
  30.9 9.2 %collective-permute-start.14 = (bf16[4,136,256]{2,1,0:T(8,128)(2,1)S(1)}, bf16[4,136,256]{2,1,0:T(8,128)(2,1)}, u32[]{:S(2)}, u32[]{:S(2)}) collective-permute-start(bf16[4,136,256]{2,1,0:T(8,128)(2,1)S(1)} %pad_maximum_fusion.3.own_ref), channel_id=1, source_target_pairs={{0,4},{4,0},{8,12},{12,8},{16,20},{20,16},{24,28},{28,24},{32,36},... | collective-permute-start | bytes 835592 | tf_op jit(solution)/shard_map/ppermute | solution.py:226
  35.6 15.1 %collective-permute-start.13 = (bf16[8,136,256]{2,1,0:T(8,128)(2,1)}, bf16[8,136,256]{2,1,0:T(8,128)(2,1)}, u32[]{:S(2)}, u32[]{:S(2)}) collective-permute-start(bf16[8,136,256]{2,1,0:T(8,128)(2,1)} %pad_maximum_fusion.2), channel_id=1, source_target_pairs={{0,4},{4,0},{8,12},{12,8},{16,20},{20,16},{24,28},{28,24},{32,36},... | collective-permute-start | bytes 1671176 | tf_op jit(solution)/shard_map/ppermute | solution.py:226
  36.4 15.7 %collective-permute-start.12 = (bf16[8,136,256]{2,1,0:T(8,128)(2,1)}, bf16[8,136,256]{2,1,0:T(8,128)(2,1)S(1)}, u32[]{:S(2)}, u32[]{:S(2)}) collective-permute-start(bf16[8,136,256]{2,1,0:T(8,128)(2,1)} %pad_maximum_fusion.1), channel_id=1, source_target_pairs={{0,4},{4,0},{8,12},{12,8},{16,20},{20,16},{24,28},{28,24},{32,36},... | collective-permute-start | bytes 1671176 | tf_op jit(solution)/shard_map/ppermute | solution.py:226
  37.8 15.1 %collective-permute-start.11 = (bf16[8,136,256]{2,1,0:T(8,128)(2,1)}, bf16[8,136,256]{2,1,0:T(8,128)(2,1)S(1)}, u32[]{:S(2)}, u32[]{:S(2)}) collective-permute-start(bf16[8,136,256]{2,1,0:T(8,128)(2,1)} %pad_maximum_fusion), channel_id=1, source_target_pairs={{0,4},{4,0},{8,12},{12,8},{16,20},{20,16},{24,28},{28,24},{32,36},... | collective-permute-start | bytes 1671176 | tf_op jit(solution)/shard_map/ppermute | solution.py:226
  40.1 10.0 %collective-permute-start.6 = (bf16[4,136,256]{2,1,0:T(8,128)(2,1)S(1)}, bf16[4,136,256]{2,1,0:T(8,128)(2,1)S(1)}, u32[]{:S(2)}, u32[]{:S(2)}) collective-permute-start(bf16[4,136,256]{2,1,0:T(8,128)(2,1)S(1)} %collective-permute-done.5.below), channel_id=1, source_target_pairs={{0,32},{4,36},{8,40},{12,44},{16,48},{20,52},{24,56},{28,60},{32,6... | collective-permute-start | bytes 835592 | tf_op jit(solution)/shard_map/ppermute | solution.py:226
  56.8 19.2 %all-to-all-start.2 = ((bf16[4,32,4096]{2,1,0:T(8,128)(2,1)}), bf16[4,32,4096]{2,1,0:T(8,128)(2,1)S(1)}, u32[]{:S(2)}, u32[]{:S(2)}) async-start(bf16[4,32,4096]{2,1,0:T(8,128)(2,1)} %bitcast.7), calls=%async_computation.2 | async-start | bytes 2097152 | tf_op jit(solution)/shard_map/all_to_all | solution.py:542
  126.7 10.7 %collective-permute-start.15 = (bf16[48,4096]{1,0:T(8,128)(2,1)S(1)}, bf16[48,4096]{1,0:T(8,128)(2,1)S(1)}, u32[]{:S(2)}, u32[]{:S(2)}) collective-permute-start(bf16[48,4096]{1,0:T(8,128)(2,1)S(1)} %get-tuple-element.75.refs_0_), channel_id=1, source_target_pairs={{0,1},{1,2},{2,3},{3,0},{4,5},{5,6},{6,7},{7,4},{8,9},{9,10},{10,1... | collective-permute-start | bytes 1179656 | tf_op jit(solution)/shard_map/ppermute | solution.py:430
  126.9 10.5 %collective-permute-start.18 = (bf16[40,4096]{1,0:T(8,128)(2,1)S(1)}, bf16[40,4096]{1,0:T(8,128)(2,1)S(1)}, u32[]{:S(2)}, u32[]{:S(2)}) collective-permute-start(bf16[40,4096]{1,0:T(8,128)(2,1)S(1)} %get-tuple-element.76.refs_1_), channel_id=1, source_target_pairs={{0,3},{1,0},{2,1},{3,2},{4,7},{5,4},{6,5},{7,6},{8,11},{9,8},{10,9... | collective-permute-start | bytes 983048 | tf_op jit(solution)/shard_map/ppermute | solution.py:430
  137.4 9.9 %collective-permute-start.19 = (bf16[48,4096]{1,0:T(8,128)(2,1)S(1)}, bf16[48,4096]{1,0:T(8,128)(2,1)S(1)}, u32[]{:S(2)}, u32[]{:S(2)}) collective-permute-start(bf16[48,4096]{1,0:T(8,128)(2,1)S(1)} %collective-permute-done.15.refs_0_), channel_id=1, source_target_pairs={{0,1},{1,2},{2,3},{3,0},{4,5},{5,6},{6,7},{7,4},{8,9},{9,10},{10,1... | collective-permute-start | bytes 1179656 | tf_op jit(solution)/shard_map/ppermute | solution.py:430
  137.4 7.5 %collective-permute-start.20 = (bf16[40,4096]{1,0:T(8,128)(2,1)S(1)}, bf16[40,4096]{1,0:T(8,128)(2,1)S(1)}, u32[]{:S(2)}, u32[]{:S(2)}) collective-permute-start(bf16[40,4096]{1,0:T(8,128)(2,1)S(1)} %collective-permute-done.18.refs_3_), channel_id=1, source_target_pairs={{0,3},{1,0},{2,1},{3,2},{4,7},{5,4},{6,5},{7,6},{8,11},{9,8},{10,9... | collective-permute-start | bytes 983048 | tf_op jit(solution)/shard_map/ppermute | solution.py:430
  140.1 14.2 %collective-permute-start.17 = (bf16[48,4096]{1,0:T(8,128)(2,1)S(1)}, bf16[48,4096]{1,0:T(8,128)(2,1)S(1)}, u32[]{:S(2)}, u32[]{:S(2)}) collective-permute-start(bf16[48,4096]{1,0:T(8,128)(2,1)S(1)} %get-tuple-element.75.refs_0_), channel_id=1, source_target_pairs={{0,3},{1,0},{2,1},{3,2},{4,7},{5,4},{6,5},{7,6},{8,11},{9,8},{10,9... | collective-permute-start | bytes 1179656 | tf_op jit(solution)/shard_map/ppermute | solution.py:430
  140.1 14.2 %collective-permute-start.16 = (bf16[40,4096]{1,0:T(8,128)(2,1)S(1)}, bf16[40,4096]{1,0:T(8,128)(2,1)S(1)}, u32[]{:S(2)}, u32[]{:S(2)}) collective-permute-start(bf16[40,4096]{1,0:T(8,128)(2,1)S(1)} %get-tuple-element.76.refs_1_), channel_id=1, source_target_pairs={{0,1},{1,2},{2,3},{3,0},{4,5},{5,6},{6,7},{7,4},{8,9},{9,10},{10,1... | collective-permute-start | bytes 983048 | tf_op jit(solution)/shard_map/ppermute | solution.py:430
  151.2 9.4 %collective-permute-start.21 = (bf16[48,4096]{1,0:T(8,128)(2,1)S(1)}, bf16[48,4096]{1,0:T(8,128)(2,1)S(1)}, u32[]{:S(2)}, u32[]{:S(2)}) collective-permute-start(bf16[48,4096]{1,0:T(8,128)(2,1)S(1)} %get-tuple-element.79), channel_id=1, source_target_pairs={{0,1},{1,2},{2,3},{3,0},{4,5},{5,6},{6,7},{7,4},{8,9},{9,10},{10,1... | collective-permute-start | bytes 1179656 | tf_op jit(solution)/shard_map/ppermute | solution.py:430
  151.3 8.7 %collective-permute-start.22 = (bf16[40,4096]{1,0:T(8,128)(2,1)S(1)}, bf16[40,4096]{1,0:T(8,128)(2,1)S(1)}, u32[]{:S(2)}, u32[]{:S(2)}) collective-permute-start(bf16[40,4096]{1,0:T(8,128)(2,1)S(1)} %get-tuple-element.81), channel_id=1, source_target_pairs={{0,3},{1,0},{2,1},{3,2},{4,7},{5,4},{6,5},{7,6},{8,11},{9,8},{10,9... | collective-permute-start | bytes 983048 | tf_op jit(solution)/shard_map/ppermute | solution.py:430
  157.7 15.3 %collective-permute-start.24 = (bf16[48,4096]{1,0:T(8,128)(2,1)S(1)}, bf16[48,4096]{1,0:T(8,128)(2,1)S(1)}, u32[]{:S(2)}, u32[]{:S(2)}) collective-permute-start(bf16[48,4096]{1,0:T(8,128)(2,1)S(1)} %get-tuple-element.83), channel_id=1, source_target_pairs={{0,3},{1,0},{2,1},{3,2},{4,7},{5,4},{6,5},{7,6},{8,11},{9,8},{10,9... | collective-permute-start | bytes 1179656 | tf_op jit(solution)/shard_map/ppermute | solution.py:430
  161.6 14.5 %collective-permute-start.23 = (bf16[48,4096]{1,0:T(8,128)(2,1)S(1)}, bf16[48,4096]{1,0:T(8,128)(2,1)S(1)}, u32[]{:S(2)}, u32[]{:S(2)}) collective-permute-start(bf16[48,4096]{1,0:T(8,128)(2,1)S(1)} %get-tuple-element.82), channel_id=1, source_target_pairs={{0,1},{1,2},{2,3},{3,0},{4,5},{5,6},{6,7},{7,4},{8,9},{9,10},{10,1... | collective-permute-start | bytes 1179656 | tf_op jit(solution)/shard_map/ppermute | solution.py:430
  161.6 11.3 %collective-permute-start.25 = (bf16[40,4096]{1,0:T(8,128)(2,1)}, bf16[40,4096]{1,0:T(8,128)(2,1)S(1)}, u32[]{:S(2)}, u32[]{:S(2)}) collective-permute-start(bf16[40,4096]{1,0:T(8,128)(2,1)} %get-tuple-element.85), channel_id=1, source_target_pairs={{0,1},{1,2},{2,3},{3,0},{4,5},{5,6},{6,7},{7,4},{8,9},{9,10},{10,1... | collective-permute-start | bytes 983048 | tf_op jit(solution)/shard_map/ppermute | solution.py:430
  162.1 14.1 %collective-permute-start.26 = (bf16[40,4096]{1,0:T(8,128)(2,1)}, bf16[40,4096]{1,0:T(8,128)(2,1)S(1)}, u32[]{:S(2)}, u32[]{:S(2)}) collective-permute-start(bf16[40,4096]{1,0:T(8,128)(2,1)} %get-tuple-element.86), channel_id=1, source_target_pairs={{0,3},{1,0},{2,1},{3,2},{4,7},{5,4},{6,5},{7,6},{8,11},{9,8},{10,9... | collective-permute-start | bytes 983048 | tf_op jit(solution)/shard_map/ppermute | solution.py:430
  178.1 41.0 %all-to-all-start.4 = ((bf16[64,2,4096]{2,1,0:T(2,128)(2,1)}), bf16[64,2,4096]{2,1,0:T(2,128)(2,1)S(1)}, u32[]{:S(2)}, u32[]{:S(2)}) async-start(bf16[64,2,4096]{2,1,0:T(2,128)(2,1)} %shard_map.138), calls=%async_computation.4 | async-start | bytes 2097152 | tf_op jit(solution)/shard_map/all_to_all | solution.py:552
  (17 other events, 534.1 us)

commit v3 on v2

--- a/solution.py
+++ b/solution.py
@@ -93,8 +93,8 @@
     found = counts[...]
     for piece in pieces:
         length = piece.shape[1] - PICK_ROWS
-        for block in range(piece.shape[0]):
-            picks = piece[block, length:].astype(jnp.float32)[0:1]
+        for shift in range(X_SIZE):
+            picks = piece[shift, length:].astype(jnp.float32)[0:1]
             found = found + (picks == expert).astype(jnp.float32)
     counts[...] = found
 
@@ -117,26 +117,27 @@
     lax.fori_loop(0, last + 1, step, 0)
 
 
-def whole_plane(state, query_ref, plane, bias_ref):
+def whole_plane(state, query_ref, plane, bias_ref, together=2):
     later = later_keys()
     blocks = plane.shape[0] // KEY_BLOCK
 
     def step(index, carried):
-        causal_visit(state, query_ref, plane, bias_ref, later, blocks - 1 - 2 * index, None)
-        causal_visit(state, query_ref, plane, bias_ref, later, blocks - 2 - 2 * index, None)
-        return carried
-
-    lax.fori_loop(0, blocks // 2, step, 0)
-
-
-def two_planes_kernel(distance, place_ref, bias_ref, query_ref, below, above, twins,
+        for offset in range(together):
+            block = blocks - 1 - offset - together * index
+            causal_visit(state, query_ref, plane, bias_ref, later, block, None)
+        return carried
+
+    lax.fori_loop(0, blocks // together, step, 0)
+
+
+def two_planes_kernel(distance, place_ref, bias_ref, query_ref, below, below_twin, above, above_twin,
                       near_in, near_used_in, far_in, counts_in, near, near_used, far, counts,
                       planes, found, found_used):
     place = place_ref[0]
-    tally(counts, below, above, twins)
+    tally(counts, below, below_twin, above, above_twin)
     level = place // (X_SIZE * CORES)
-    lay_out(below, twins.at[:X_SIZE], planes.at[0], place)
-    lay_out(above, twins.at[X_SIZE:], planes.at[1], place)
+    lay_out(below, below_twin, planes.at[0], place)
+    lay_out(above, above_twin, planes.at[1], place)
 
     def visit(side, carried):
         found[...] = jnp.zeros_like(found)
@@ -164,8 +165,8 @@
     place = place_ref[0]
     counts[...] = counts_in[...]
     tally(counts, below, below_twin)
-    quarter = counts.shape[1] // 4
-    lane = lax.broadcasted_iota(jnp.int32, counts.shape, 1) // quarter
+    rows = out_ref.shape[0]
+    lane = lax.broadcasted_iota(jnp.int32, counts.shape, 1) % rows // (rows // 4)
     most = jnp.zeros((counts.shape[0], 1), jnp.float32)
     for member in range(4):
         named = jnp.sum(jnp.where(lane == member, counts[...], 0.0), axis=1, keepdims=True)
@@ -177,7 +178,7 @@
     @pl.when(place // (X_SIZE * CORES) >= distance)
     def _():
         lay_out(below, below_twin, plane, place)
-        whole_plane((near, near_used), query_ref, plane, bias_ref)
+        whole_plane((near, near_used), query_ref, plane, bias_ref, 1)
 
     rows = out_ref.shape[0]
     for head in range(bias_ref.shape[0]):
@@ -230,7 +231,7 @@
     rows = queries.shape[0]
     heads = queries.shape[1] // HEAD
     stacked = jnp.concatenate([queries[:, h * HEAD : (h + 1) * HEAD] for h in range(heads)], axis=0)
-    picks = pick_ids.astype(jnp.bfloat16).reshape(1, rows * TOP)
+    picks = pick_ids.T.astype(jnp.bfloat16).reshape(1, TOP * rows)
     picks = jnp.concatenate([picks, jnp.zeros((PICK_ROWS - 1, rows * TOP), jnp.bfloat16)], axis=0)
     block = jnp.concatenate([jnp.concatenate([keys, values], axis=1), picks], axis=0)
     own = jnp.stack([block] + [moved(block, 0, step, 0) for step in range(1, X_SIZE)])
@@ -240,12 +241,11 @@
     arrived = []
     for distance in range(1, Z_SIZE // 2 + 1):
         below = moved(below, 1, 0, 0)
+        pieces = [below, moved(below, 0, 0, 1)]
         if distance < Z_SIZE // 2:
             above = moved(above, -1, 0, 0)
-            both = jnp.concatenate([below, above], axis=0)
-            arrived.append((below, above, moved(both, 0, 0, 1)))
-        else:
-            arrived.append((below, moved(below, 0, 0, 1)))
+            pieces += [above, moved(above, 0, 0, 1)]
+        arrived.append(pieces)
     state = attention_call(own_plane_kernel, "attend_0", 1, *common, (own, twin), (), rows)
     for distance in range(1, Z_SIZE // 2):
         kernel = functools.partial(two_planes_kernel, distance)
@@ -353,7 +353,7 @@
         rest_ref[:, at] = packed[both:]
         return carried
 
-    over_columns(width, write, 0)
+    over_columns(width, write, 0, True)
 
 
 def expert_kernel(*refs):
@@ -400,11 +400,17 @@
 def final_kernel(returned_ref, targets_ref, logits_ref, stream_ref, gain_ref, out_ref, blended):
     rows, width = stream_ref.shape
     slots = returned_ref.shape[0] * returned_ref.shape[1]
-    slot = lax.broadcasted_iota(jnp.int32, (rows, slots), 1)
+    slot = lax.broadcasted_iota(jnp.int32, (rows, slots), 1).astype(jnp.float32)
+    diagonal = lax.broadcasted_iota(jnp.int32, (rows, rows), 0) == lax.broadcasted_iota(jnp.int32, (rows, rows), 1)
+
+    def column(row):
+        return jnp.sum(jnp.where(diagonal, row.astype(jnp.float32), 0.0), axis=1, keepdims=True)
+
     picks = [
-        (slot == targets_ref[:, pick : pick + 1]).astype(jnp.float32).astype(jnp.bfloat16) for pick in range(TOP)
+        (slot == column(targets_ref[pick : pick + 1])).astype(jnp.float32).astype(jnp.bfloat16)
+        for pick in range(TOP)
     ]
-    logits = logits_ref[...]
+    logits = column(logits_ref[...])
     shares = (1.0 / (1.0 + jnp.exp(-logits)), 1.0 / (1.0 + jnp.exp(logits)))
 
     def mix(at, total):
@@ -445,8 +451,7 @@
     firsts, seconds, results_ref = refs[:3], refs[3:6], refs[6]
     width = firsts[0].shape[1]
 
-    def step(index, carried):
-        at = pl.ds(pl.multiple_of(index * COLUMNS, COLUMNS), COLUMNS)
+    def step(at, carried):
         sums = []
         for parts in (firsts, seconds):
             total = parts[0][:, at].astype(jnp.float32)
@@ -458,7 +463,7 @@
         results_ref[:, :, at] = spread.reshape(results_ref.shape[0], results_ref.shape[1], COLUMNS)
         return carried
 
-    lax.fori_loop(0, width // COLUMNS, step, 0)
+    over_columns(width, step, 0, True)
 
 
 def rest_outputs(rest, weights):
@@ -527,16 +532,17 @@
     width = w_out.shape[1]
     experts = lax.axis_size("sp")
     capacity = max(2, (3 * slice_rows + experts - 1) // experts)
-    routed = lax.dynamic_slice_in_dim(pick_ids, quarter * slice_rows, slice_rows, 0)
+    routed = lax.dynamic_slice_in_dim(pick_ids.T, quarter * slice_rows, slice_rows, 1)
     flat_ids = routed.reshape(slice_rows * TOP)
     places = jnp.arange(slice_rows * TOP, dtype=jnp.int32)
     matches = (flat_ids[:, None] == flat_ids[None, :]) & (places[None, :] < places[:, None])
     ranks = jnp.sum(matches.astype(jnp.int32), axis=1)
-    targets = (flat_ids * capacity + ranks).reshape(slice_rows, TOP)
-    logits = lax.dynamic_slice_in_dim(pair_logit, quarter * slice_rows, slice_rows, 0)[:, None]
+    targets = (flat_ids * capacity + ranks).reshape(TOP, slice_rows)
+    logits = lax.dynamic_slice_in_dim(pair_logit, quarter * slice_rows, slice_rows, 0)[None]
 
     place = position.reshape(1).astype(jnp.int32)
     head_out, most = attend(queries, keys, values, break_bias, pick_ids, place)
+    head_out, targets, logits = lax.optimization_barrier((head_out, targets, logits))
     partial = jnp.dot(head_out, w_out, preferred_element_type=jnp.float32).astype(jnp.bfloat16)
     parts = split_up(partial, 0, quarters)
     mixed = lax.all_to_all(parts, "tp", split_axis=0, concat_axis=0, tiled=True)
@@ -545,7 +551,7 @@
     dispatch_flops = 2 * experts * capacity * slice_rows * width
     stream, outgoing = in_kernel(
         dispatch_kernel, (rows, slots), 16, dispatch_flops,
-        mixed, residual, ffn_gain[None], targets.T,
+        mixed, residual, ffn_gain[None], targets,
     )
     arrived = lax.all_to_all(outgoing, "sp", split_axis=0, concat_axis=0, tiled=True)
     results = expert_outputs(arrived, most[0], (w_gate[0], w_up[0], w_down[0]))

time: 221 us -> 217 us (0.982)
  blocking collectives: 47.1 us -> 107 us
  waiting for transfers between devices: 81.3 us -> 31.3 us
  starting transfers between devices: 56.1 us -> 46.2 us
  Pallas kernels: 26.3 us -> 22.8 us
  local copies, waits for them, and re-layouts: 1.87 us -> 4.1 us
    all_to_all x0 -> x2, blocking collectives: none -> 58.9 us  [the longest x1 39.8 us: on_device(): lax.all_to_all(results, 'sp', split_axis=0, concat_axis=0, tiled=True)]
    all_to_all x2 -> x0, waiting for transfers between devices: 42.2 us -> none  [the longest x1 28 us: on_device(): lax.all_to_all(results, 'sp', split_axis=0, concat_axis=0, tiled=True)]
    all_to_all x2 -> x0, starting transfers between devices: 17.2 us -> none  [the longest x1 12.9 us: on_device(): lax.all_to_all(results, 'sp', split_axis=0, concat_axis=0, tiled=True)]
    ppermute x15 -> x18, waiting for transfers between devices: 19.2 us -> 6.93 us  [moved(): return lax.ppermute(shard, 'sp', pairs)]
    ppermute x15 -> x18, starting transfers between devices: 24.3 us -> 31.5 us  [moved(): return lax.ppermute(shard, 'sp', pairs)]
    ppermute x12, waiting for transfers between devices: 19.9 us -> 24.4 us  [along_tp(): lax.ppermute(shard, 'tp', [(member, (member + step) % size) for member in...]
    pallas_call x8, Pallas kernels: 20.3 us -> 16.7 us  [in_kernel(): pl.pallas_call(kernel, out_shape=out_shapes, in_specs=[spec] * len(operan...]
    concatenate x3 -> x0, other arithmetic: 2.57 us -> none  [attend(): both = jnp.concatenate([below, above], axis=0)]
  transfers between devices with their start and end apart: 29 -> 30, of which waited for: 14 -> 11; matrix products, arithmetic and copies ran while one was open for 2% -> 2% of each run, Pallas kernels for 8% -> 8%
where the time goes in v3:
time: 217 us
  blocking collectives  107 us (49%)
  starting transfers between devices  46.2 us (21%)
  waiting for transfers between devices  31.3 us (14%)
  Pallas kernels  22.8 us (11%)
  local copies, waits for them, and re-layouts  4.1 us (2%)
  other arithmetic  3.38 us (2%)
    all_to_all x1, blocking collectives, on_device(): lax.all_to_all(outgoing, 'sp', split_axis=0, concat_axis=0, tiled=True)  48.5 us
    all_to_all x1, blocking collectives, on_device(): lax.all_to_all(results, 'sp', split_axis=0, concat_axis=0, tiled=True)  39.8 us
    ppermute x18, starting transfers between devices, moved(): return lax.ppermute(shard, 'sp', pairs)  31.5 us
    ppermute x12, waiting for transfers between devices, along_tp(): lax.ppermute(shard, 'tp', [(member, (member + step) % size) for member in...  24.4 us
    all_to_all x1, blocking collectives, on_device(): mixed = lax.all_to_all(parts, 'tp', split_axis=0, concat_axis=0, tiled=True)  19 us
    pallas_call x8, Pallas kernels, in_kernel(): pl.pallas_call(kernel, out_shape=out_shapes, in_specs=[spec] * len(operan...  16.7 us
    ppermute x12, starting transfers between devices, along_tp(): lax.ppermute(shard, 'tp', [(member, (member + step) % size) for member in...  14.7 us
    ppermute x18, waiting for transfers between devices, moved(): return lax.ppermute(shard, 'sp', pairs)  6.93 us
  transfers between devices with their start and end apart: 30, of which 11 were waited for; matrix products, arithmetic and copies ran while one was open for 2% of the time, Pallas kernels for 8%

profile of v3, /device:TPU:1, one launch (start us, length us, event | category | flops | bytes accessed | tf_op | source)
XLA Modules:
  0.0 216.8 jit_solution(7992452038337641365)
XLA Ops:
  3.8 2.5 %collective-permute-start.1 = (bf16[136,256]{1,0:T(8,128)(2,1)S(1)}, bf16[136,256]{1,0:T(8,128)(2,1)S(1)}, u32[]{:S(2)}, u32[]{:S(2)}) collective-permute-start(bf16[136,256]{1,0:T(8,128)(2,1)S(1)} %maximum_maximum_fusion), channel_id=1, source_target_pairs={{0,16},{4,20},{8,24},{12,28},{16,0},{20,4},{24,8},{28,12},{32,48},... | collective-permute-start | bytes 208904 | tf_op jit(solution)/shard_map/ppermute | solution.py:227
  11.7 4.0 %collective-permute-start.9 = (bf16[4,136,256]{2,1,0:T(8,128)(2,1)S(1)}, bf16[4,136,256]{2,1,0:T(8,128)(2,1)S(1)}, u32[]{:S(2)}, u32[]{:S(2)}) collective-permute-start(bf16[4,136,256]{2,1,0:T(8,128)(2,1)S(1)} %pad_maximum_fusion.own_ref), channel_id=1, source_target_pairs={{0,224},{4,228},{8,232},{12,236},{16,240},{20,244},{24,248},{28,25... | collective-permute-start | bytes 835592 | tf_op jit(solution)/shard_map/ppermute | solution.py:227
  15.7 5.1 %collective-permute-done.3.below = bf16[4,136,256]{2,1,0:T(8,128)(2,1)S(1)} collective-permute-done((bf16[4,136,256]{2,1,0:T(8,128)(2,1)S(1)}, bf16[4,136,256]{2,1,0:T(8,128)(2,1)S(1)}, u32[]{:S(2)}, u32[]{:S(2)}) %collective-permute-start.3) | collective-permute-done | bytes 278560 | tf_op jit(solution)/shard_map/ppermute | solution.py:227
  21.7 2.7 %collective-permute-start.10 = (bf16[4,136,256]{2,1,0:T(8,128)(2,1)S(1)}, bf16[4,136,256]{2,1,0:T(8,128)(2,1)S(1)}, u32[]{:S(2)}, u32[]{:S(2)}) collective-permute-start(bf16[4,136,256]{2,1,0:T(8,128)(2,1)S(1)} %collective-permute-done.9.above), channel_id=1, source_target_pairs={{0,224},{4,228},{8,232},{12,236},{16,240},{20,244},{24,248},{28,25... | collective-permute-start | bytes 835592 | tf_op jit(solution)/shard_map/ppermute | solution.py:227
  25.2 3.0 %collective-permute-start.17 = (bf16[4,136,256]{2,1,0:T(8,128)(2,1)S(1)}, bf16[4,136,256]{2,1,0:T(8,128)(2,1)S(1)}, u32[]{:S(2)}, u32[]{:S(2)}) collective-permute-start(bf16[4,136,256]{2,1,0:T(8,128)(2,1)S(1)} %pad_maximum_fusion.own_ref), channel_id=1, source_target_pairs={{0,4},{4,0},{8,12},{12,8},{16,20},{20,16},{24,28},{28,24},{32,36},... | collective-permute-start | bytes 835592 | tf_op jit(solution)/shard_map/ppermute | solution.py:227
  28.6 2.8 %collective-permute-start.16 = (bf16[4,136,256]{2,1,0:T(8,128)(2,1)S(1)}, bf16[4,136,256]{2,1,0:T(8,128)(2,1)S(1)}, u32[]{:S(2)}, u32[]{:S(2)}) collective-permute-start(bf16[4,136,256]{2,1,0:T(8,128)(2,1)S(1)} %collective-permute-done.9.above), channel_id=1, source_target_pairs={{0,4},{4,0},{8,12},{12,8},{16,20},{20,16},{24,28},{28,24},{32,36},... | collective-permute-start | bytes 835592 | tf_op jit(solution)/shard_map/ppermute | solution.py:227
  31.4 3.0 %collective-permute-start.11 = (bf16[4,136,256]{2,1,0:T(8,128)(2,1)S(1)}, bf16[4,136,256]{2,1,0:T(8,128)(2,1)S(1)}, u32[]{:S(2)}, u32[]{:S(2)}) collective-permute-start(bf16[4,136,256]{2,1,0:T(8,128)(2,1)S(1)} %collective-permute-done.10.above), channel_id=1, source_target_pairs={{0,224},{4,228},{8,232},{12,236},{16,240},{20,244},{24,248},{28,25... | collective-permute-start | bytes 835592 | tf_op jit(solution)/shard_map/ppermute | solution.py:227
  35.9 3.1 %collective-permute-start.14 = (bf16[4,136,256]{2,1,0:T(8,128)(2,1)S(1)}, bf16[4,136,256]{2,1,0:T(8,128)(2,1)}, u32[]{:S(2)}, u32[]{:S(2)}) collective-permute-start(bf16[4,136,256]{2,1,0:T(8,128)(2,1)S(1)} %collective-permute-done.10.above), channel_id=1, source_target_pairs={{0,4},{4,0},{8,12},{12,8},{16,20},{20,16},{24,28},{28,24},{32,36},... | collective-permute-start | bytes 835592 | tf_op jit(solution)/shard_map/ppermute | solution.py:227
  43.5 3.2 %collective-permute-start.7 = (bf16[4,136,256]{2,1,0:T(8,128)(2,1)S(1)}, bf16[4,136,256]{2,1,0:T(8,128)(2,1)S(1)}, u32[]{:S(2)}, u32[]{:S(2)}) collective-permute-start(bf16[4,136,256]{2,1,0:T(8,128)(2,1)S(1)} %collective-permute-done.6.below), channel_id=1, source_target_pairs={{0,4},{4,0},{8,12},{12,8},{16,20},{20,16},{24,28},{28,24},{32,36},... | collective-permute-start | bytes 835592 | tf_op jit(solution)/shard_map/ppermute | solution.py:227
  52.2 19.0 %all_to_all.25.mixed_ref = bf16[4,32,4096]{2,1,0:T(8,128)(2,1)S(1)} all-to-all(bf16[4,32,4096]{2,1,0:T(8,128)(2,1)S(1)} %bitcast.46), channel_id=1, replica_groups=mesh['sp'=64,'tp'=4] {'tp'}, dimensions={0} | all-to-all | bytes 2097152 | tf_op jit(solution)/shard_map/all_to_all | solution.py:548
  72.0 48.5 %all_to_all.26.arrived_ref = bf16[64,2,4096]{2,1,0:T(2,128)(2,1)S(1)} all-to-all(bf16[64,2,4096]{2,1,0:T(2,128)(2,1)S(1)} %get-tuple-element.76), channel_id=1, replica_groups=mesh['sp'=64,'tp'=4] {'sp'}, dimensions={0} | all-to-all | bytes 2097152 | tf_op jit(solution)/shard_map/all_to_all | solution.py:556
  123.0 2.4 %collective-permute-start.21 = (bf16[40,4096]{1,0:T(8,128)(2,1)S(1)}, bf16[40,4096]{1,0:T(8,128)(2,1)S(1)}, u32[]{:S(2)}, u32[]{:S(2)}) collective-permute-start(bf16[40,4096]{1,0:T(8,128)(2,1)S(1)} %get-tuple-element.81.refs_1_), channel_id=1, source_target_pairs={{0,3},{1,0},{2,1},{3,2},{4,7},{5,4},{6,5},{7,6},{8,11},{9,8},{10,9... | collective-permute-start | bytes 983048 | tf_op jit(solution)/shard_map/ppermute | solution.py:436
  125.4 8.1 %collective-permute-done.18.refs_0_ = bf16[48,4096]{1,0:T(8,128)(2,1)S(1)} collective-permute-done((bf16[48,4096]{1,0:T(8,128)(2,1)S(1)}, bf16[48,4096]{1,0:T(8,128)(2,1)S(1)}, u32[]{:S(2)}, u32[]{:S(2)}) %collective-permute-start.18) | collective-permute-done | bytes 393248 | tf_op jit(solution)/shard_map/ppermute | solution.py:436
  133.5 2.7 %collective-permute-start.23 = (bf16[40,4096]{1,0:T(8,128)(2,1)S(1)}, bf16[40,4096]{1,0:T(8,128)(2,1)S(1)}, u32[]{:S(2)}, u32[]{:S(2)}) collective-permute-start(bf16[40,4096]{1,0:T(8,128)(2,1)S(1)} %collective-permute-done.21.refs_3_), channel_id=1, source_target_pairs={{0,3},{1,0},{2,1},{3,2},{4,7},{5,4},{6,5},{7,6},{8,11},{9,8},{10,9... | collective-permute-start | bytes 983048 | tf_op jit(solution)/shard_map/ppermute | solution.py:436
  137.6 3.3 %collective-permute-done.23.refs_1_ = bf16[40,4096]{1,0:T(8,128)(2,1)S(1)} collective-permute-done((bf16[40,4096]{1,0:T(8,128)(2,1)S(1)}, bf16[40,4096]{1,0:T(8,128)(2,1)S(1)}, u32[]{:S(2)}, u32[]{:S(2)}) %collective-permute-start.23) | collective-permute-done | bytes 327712 | tf_op jit(solution)/shard_map/ppermute | solution.py:436
  141.0 2.4 %collective-permute-done.22.refs_0_ = bf16[48,4096]{1,0:T(8,128)(2,1)S(1)} collective-permute-done((bf16[48,4096]{1,0:T(8,128)(2,1)S(1)}, bf16[48,4096]{1,0:T(8,128)(2,1)S(1)}, u32[]{:S(2)}, u32[]{:S(2)}) %collective-permute-start.22) | collective-permute-done | bytes 393248 | tf_op jit(solution)/shard_map/ppermute | solution.py:436
  145.7 2.7 %collective-permute-start.25 = (bf16[40,4096]{1,0:T(8,128)(2,1)S(1)}, bf16[40,4096]{1,0:T(8,128)(2,1)S(1)}, u32[]{:S(2)}, u32[]{:S(2)}) collective-permute-start(bf16[40,4096]{1,0:T(8,128)(2,1)S(1)} %get-tuple-element.86), channel_id=1, source_target_pairs={{0,3},{1,0},{2,1},{3,2},{4,7},{5,4},{6,5},{7,6},{8,11},{9,8},{10,9... | collective-permute-start | bytes 983048 | tf_op jit(solution)/shard_map/ppermute | solution.py:436
  150.4 3.4 %shard_map.135 = (bf16[48,4096]{1,0:T(8,128)(2,1)S(1)}, bf16[40,4096]{1,0:T(8,128)(2,1)S(1)}, bf16[48,4096]{1,0:T(8,128)(2,1)S(1)}, bf16[40,4096]{1,0:T(8,128)(2,1)}) custom-call(bf16[48,4096]{1,0:T(8,128)(2,1)S(1)} %collective-permute-done.18.refs_0_, bf16[40,4096]{1,0:T(8,128)(2,1)S(1)} %collective-permute-done.19.refs_1_, ...), custom_call_target="tpu_custom_call" | custom-call | flops 1107296256 | tf_op jit(solution)/shard_map/pallas_call | solution.py:265
  153.8 2.4 %collective-permute-start.27 = (bf16[48,4096]{1,0:T(8,128)(2,1)S(1)}, bf16[48,4096]{1,0:T(8,128)(2,1)S(1)}, u32[]{:S(2)}, u32[]{:S(2)}) collective-permute-start(bf16[48,4096]{1,0:T(8,128)(2,1)S(1)} %get-tuple-element.88), channel_id=1, source_target_pairs={{0,3},{1,0},{2,1},{3,2},{4,7},{5,4},{6,5},{7,6},{8,11},{9,8},{10,9... | collective-permute-start | bytes 1179656 | tf_op jit(solution)/shard_map/ppermute | solution.py:436
  156.3 2.4 %collective-permute-done.24.far_up = bf16[48,4096]{1,0:T(8,128)(2,1)S(1)} collective-permute-done((bf16[48,4096]{1,0:T(8,128)(2,1)S(1)}, bf16[48,4096]{1,0:T(8,128)(2,1)S(1)}, u32[]{:S(2)}, u32[]{:S(2)}) %collective-permute-start.24) | collective-permute-done | bytes 393248 | tf_op jit(solution)/shard_map/ppermute | solution.py:436
  159.7 2.7 %collective-permute-start.29 = (bf16[40,4096]{1,0:T(8,128)(2,1)}, bf16[40,4096]{1,0:T(8,128)(2,1)S(1)}, u32[]{:S(2)}, u32[]{:S(2)}) collective-permute-start(bf16[40,4096]{1,0:T(8,128)(2,1)} %get-tuple-element.91), channel_id=1, source_target_pairs={{0,3},{1,0},{2,1},{3,2},{4,7},{5,4},{6,5},{7,6},{8,11},{9,8},{10,9... | collective-permute-start | bytes 983048 | tf_op jit(solution)/shard_map/ppermute | solution.py:436
  163.8 5.1 %shard_map.134 = (bf16[48,4096]{1,0:T(8,128)(2,1)S(1)}, bf16[40,4096]{1,0:T(8,128)(2,1)S(1)}) custom-call(bf16[48,4096]{1,0:T(8,128)(2,1)S(1)} %get-tuple-element.80.refs_0_, bf16[40,4096]{1,0:T(8,128)(2,1)S(1)} %get-tuple-element.81.refs_1_, bf16[4096,256]{1,0:T(8,128)(2,1)} %bitcast.34, bf16[4096,256]{1,0:T(8,128)(2,1)} %bitcast.38, bf16[256,4096]{1,0:T(8,128)(2,1)} %bitcast.42), custom_call_target="tpu_custom_call" | custom-call | flops 553648128 | tf_op jit(solution)/shard_map/pallas_call | solution.py:265
  168.9 6.0 %collective-permute-done.28.refs_4_ = bf16[40,4096]{1,0:T(8,128)(2,1)S(1)} collective-permute-done((bf16[40,4096]{1,0:T(8,128)(2,1)}, bf16[40,4096]{1,0:T(8,128)(2,1)S(1)}, u32[]{:S(2)}, u32[]{:S(2)}) %collective-permute-start.28) | collective-permute-done | bytes 327712 | tf_op jit(solution)/shard_map/ppermute | solution.py:436
  175.5 39.8 %all_to_all.27.returned_ref = bf16[64,2,4096]{2,1,0:T(2,128)(2,1)S(1)} all-to-all(bf16[64,2,4096]{2,1,0:T(2,128)(2,1)S(1)} %shard_map.138), channel_id=1, replica_groups=mesh['sp'=64,'tp'=4] {'sp'}, dimensions={0} | all-to-all | bytes 2097152 | tf_op jit(solution)/shard_map/all_to_all | solution.py:558
  (94 shorter events, 36.5 us)
Async XLA Ops:
  9.7 11.2 %collective-permute-start.3 = (bf16[4,136,256]{2,1,0:T(8,128)(2,1)S(1)}, bf16[4,136,256]{2,1,0:T(8,128)(2,1)S(1)}, u32[]{:S(2)}, u32[]{:S(2)}) collective-permute-start(bf16[4,136,256]{2,1,0:T(8,128)(2,1)S(1)} %pad_maximum_fusion.own_ref), channel_id=1, source_target_pairs={{0,32},{4,36},{8,40},{12,44},{16,48},{20,52},{24,56},{28,60},{32,6... | collective-permute-start | bytes 835592 | tf_op jit(solution)/shard_map/ppermute | solution.py:227
  11.7 10.0 %collective-permute-start.9 = (bf16[4,136,256]{2,1,0:T(8,128)(2,1)S(1)}, bf16[4,136,256]{2,1,0:T(8,128)(2,1)S(1)}, u32[]{:S(2)}, u32[]{:S(2)}) collective-permute-start(bf16[4,136,256]{2,1,0:T(8,128)(2,1)S(1)} %pad_maximum_fusion.own_ref), channel_id=1, source_target_pairs={{0,224},{4,228},{8,232},{12,236},{16,240},{20,244},{24,248},{28,25... | collective-permute-start | bytes 835592 | tf_op jit(solution)/shard_map/ppermute | solution.py:227
  21.7 9.7 %collective-permute-start.10 = (bf16[4,136,256]{2,1,0:T(8,128)(2,1)S(1)}, bf16[4,136,256]{2,1,0:T(8,128)(2,1)S(1)}, u32[]{:S(2)}, u32[]{:S(2)}) collective-permute-start(bf16[4,136,256]{2,1,0:T(8,128)(2,1)S(1)} %collective-permute-done.9.above), channel_id=1, source_target_pairs={{0,224},{4,228},{8,232},{12,236},{16,240},{20,244},{24,248},{28,25... | collective-permute-start | bytes 835592 | tf_op jit(solution)/shard_map/ppermute | solution.py:227
  25.2 9.9 %collective-permute-start.17 = (bf16[4,136,256]{2,1,0:T(8,128)(2,1)S(1)}, bf16[4,136,256]{2,1,0:T(8,128)(2,1)S(1)}, u32[]{:S(2)}, u32[]{:S(2)}) collective-permute-start(bf16[4,136,256]{2,1,0:T(8,128)(2,1)S(1)} %pad_maximum_fusion.own_ref), channel_id=1, source_target_pairs={{0,4},{4,0},{8,12},{12,8},{16,20},{20,16},{24,28},{28,24},{32,36},... | collective-permute-start | bytes 835592 | tf_op jit(solution)/shard_map/ppermute | solution.py:227
  28.2 7.6 %collective-permute-start.15 = (bf16[4,136,256]{2,1,0:T(8,128)(2,1)S(1)}, bf16[4,136,256]{2,1,0:T(8,128)(2,1)S(1)}, u32[]{:S(2)}, u32[]{:S(2)}) collective-permute-start(bf16[4,136,256]{2,1,0:T(8,128)(2,1)S(1)} %collective-permute-done.3.below), channel_id=1, source_target_pairs={{0,4},{4,0},{8,12},{12,8},{16,20},{20,16},{24,28},{28,24},{32,36},... | collective-permute-start | bytes 835592 | tf_op jit(solution)/shard_map/ppermute | solution.py:227
  28.3 7.5 %collective-permute-start.5 = (bf16[4,136,256]{2,1,0:T(8,128)(2,1)S(1)}, bf16[4,136,256]{2,1,0:T(8,128)(2,1)S(1)}, u32[]{:S(2)}, u32[]{:S(2)}) collective-permute-start(bf16[4,136,256]{2,1,0:T(8,128)(2,1)S(1)} %collective-permute-done.4.below), channel_id=1, source_target_pairs={{0,32},{4,36},{8,40},{12,44},{16,48},{20,52},{24,56},{28,60},{32,6... | collective-permute-start | bytes 835592 | tf_op jit(solution)/shard_map/ppermute | solution.py:227
  28.6 10.3 %collective-permute-start.16 = (bf16[4,136,256]{2,1,0:T(8,128)(2,1)S(1)}, bf16[4,136,256]{2,1,0:T(8,128)(2,1)S(1)}, u32[]{:S(2)}, u32[]{:S(2)}) collective-permute-start(bf16[4,136,256]{2,1,0:T(8,128)(2,1)S(1)} %collective-permute-done.9.above), channel_id=1, source_target_pairs={{0,4},{4,0},{8,12},{12,8},{16,20},{20,16},{24,28},{28,24},{32,36},... | collective-permute-start | bytes 835592 | tf_op jit(solution)/shard_map/ppermute | solution.py:227
  31.4 8.6 %collective-permute-start.11 = (bf16[4,136,256]{2,1,0:T(8,128)(2,1)S(1)}, bf16[4,136,256]{2,1,0:T(8,128)(2,1)S(1)}, u32[]{:S(2)}, u32[]{:S(2)}) collective-permute-start(bf16[4,136,256]{2,1,0:T(8,128)(2,1)S(1)} %collective-permute-done.10.above), channel_id=1, source_target_pairs={{0,224},{4,228},{8,232},{12,236},{16,240},{20,244},{24,248},{28,25... | collective-permute-start | bytes 835592 | tf_op jit(solution)/shard_map/ppermute | solution.py:227
  35.2 12.3 %collective-permute-start.13 = (bf16[4,136,256]{2,1,0:T(8,128)(2,1)S(1)}, bf16[4,136,256]{2,1,0:T(8,128)(2,1)S(1)}, u32[]{:S(2)}, u32[]{:S(2)}) collective-permute-start(bf16[4,136,256]{2,1,0:T(8,128)(2,1)S(1)} %collective-permute-done.4.below), channel_id=1, source_target_pairs={{0,4},{4,0},{8,12},{12,8},{16,20},{20,16},{24,28},{28,24},{32,36},... | collective-permute-start | bytes 835592 | tf_op jit(solution)/shard_map/ppermute | solution.py:227
  35.9 7.6 %collective-permute-start.6 = (bf16[4,136,256]{2,1,0:T(8,128)(2,1)S(1)}, bf16[4,136,256]{2,1,0:T(8,128)(2,1)S(1)}, u32[]{:S(2)}, u32[]{:S(2)}) collective-permute-start(bf16[4,136,256]{2,1,0:T(8,128)(2,1)S(1)} %collective-permute-done.5.below), channel_id=1, source_target_pairs={{0,32},{4,36},{8,40},{12,44},{16,48},{20,52},{24,56},{28,60},{32,6... | collective-permute-start | bytes 835592 | tf_op jit(solution)/shard_map/ppermute | solution.py:227
  35.9 11.6 %collective-permute-start.14 = (bf16[4,136,256]{2,1,0:T(8,128)(2,1)S(1)}, bf16[4,136,256]{2,1,0:T(8,128)(2,1)}, u32[]{:S(2)}, u32[]{:S(2)}) collective-permute-start(bf16[4,136,256]{2,1,0:T(8,128)(2,1)S(1)} %collective-permute-done.10.above), channel_id=1, source_target_pairs={{0,4},{4,0},{8,12},{12,8},{16,20},{20,16},{24,28},{28,24},{32,36},... | collective-permute-start | bytes 835592 | tf_op jit(solution)/shard_map/ppermute | solution.py:227
  39.7 9.0 %collective-permute-start.8 = (bf16[4,136,256]{2,1,0:T(8,128)(2,1)S(1)}, bf16[4,136,256]{2,1,0:T(8,128)(2,1)}, u32[]{:S(2)}, u32[]{:S(2)}) collective-permute-start(bf16[4,136,256]{2,1,0:T(8,128)(2,1)S(1)} %collective-permute-done.5.below), channel_id=1, source_target_pairs={{0,4},{4,0},{8,12},{12,8},{16,20},{20,16},{24,28},{28,24},{32,36},... | collective-permute-start | bytes 835592 | tf_op jit(solution)/shard_map/ppermute | solution.py:227
  40.0 8.6 %collective-permute-start.12 = (bf16[4,136,256]{2,1,0:T(8,128)(2,1)S(1)}, bf16[4,136,256]{2,1,0:T(8,128)(2,1)}, u32[]{:S(2)}, u32[]{:S(2)}) collective-permute-start(bf16[4,136,256]{2,1,0:T(8,128)(2,1)S(1)} %collective-permute-done.11.above), channel_id=1, source_target_pairs={{0,4},{4,0},{8,12},{12,8},{16,20},{20,16},{24,28},{28,24},{32,36},... | collective-permute-start | bytes 835592 | tf_op jit(solution)/shard_map/ppermute | solution.py:227
  122.7 10.7 %collective-permute-start.18 = (bf16[48,4096]{1,0:T(8,128)(2,1)S(1)}, bf16[48,4096]{1,0:T(8,128)(2,1)S(1)}, u32[]{:S(2)}, u32[]{:S(2)}) collective-permute-start(bf16[48,4096]{1,0:T(8,128)(2,1)S(1)} %get-tuple-element.80.refs_0_), channel_id=1, source_target_pairs={{0,1},{1,2},{2,3},{3,0},{4,5},{5,6},{6,7},{7,4},{8,9},{9,10},{10,1... | collective-permute-start | bytes 1179656 | tf_op jit(solution)/shard_map/ppermute | solution.py:436
  123.0 10.5 %collective-permute-start.21 = (bf16[40,4096]{1,0:T(8,128)(2,1)S(1)}, bf16[40,4096]{1,0:T(8,128)(2,1)S(1)}, u32[]{:S(2)}, u32[]{:S(2)}) collective-permute-start(bf16[40,4096]{1,0:T(8,128)(2,1)S(1)} %get-tuple-element.81.refs_1_), channel_id=1, source_target_pairs={{0,3},{1,0},{2,1},{3,2},{4,7},{5,4},{6,5},{7,6},{8,11},{9,8},{10,9... | collective-permute-start | bytes 983048 | tf_op jit(solution)/shard_map/ppermute | solution.py:436
  133.5 9.9 %collective-permute-start.22 = (bf16[48,4096]{1,0:T(8,128)(2,1)S(1)}, bf16[48,4096]{1,0:T(8,128)(2,1)S(1)}, u32[]{:S(2)}, u32[]{:S(2)}) collective-permute-start(bf16[48,4096]{1,0:T(8,128)(2,1)S(1)} %collective-permute-done.18.refs_0_), channel_id=1, source_target_pairs={{0,1},{1,2},{2,3},{3,0},{4,5},{5,6},{6,7},{7,4},{8,9},{9,10},{10,1... | collective-permute-start | bytes 1179656 | tf_op jit(solution)/shard_map/ppermute | solution.py:436
  136.2 14.2 %collective-permute-start.20 = (bf16[48,4096]{1,0:T(8,128)(2,1)S(1)}, bf16[48,4096]{1,0:T(8,128)(2,1)S(1)}, u32[]{:S(2)}, u32[]{:S(2)}) collective-permute-start(bf16[48,4096]{1,0:T(8,128)(2,1)S(1)} %get-tuple-element.80.refs_0_), channel_id=1, source_target_pairs={{0,3},{1,0},{2,1},{3,2},{4,7},{5,4},{6,5},{7,6},{8,11},{9,8},{10,9... | collective-permute-start | bytes 1179656 | tf_op jit(solution)/shard_map/ppermute | solution.py:436
  136.2 14.2 %collective-permute-start.19 = (bf16[40,4096]{1,0:T(8,128)(2,1)S(1)}, bf16[40,4096]{1,0:T(8,128)(2,1)S(1)}, u32[]{:S(2)}, u32[]{:S(2)}) collective-permute-start(bf16[40,4096]{1,0:T(8,128)(2,1)S(1)} %get-tuple-element.81.refs_1_), channel_id=1, source_target_pairs={{0,1},{1,2},{2,3},{3,0},{4,5},{5,6},{6,7},{7,4},{8,9},{9,10},{10,1... | collective-permute-start | bytes 983048 | tf_op jit(solution)/shard_map/ppermute | solution.py:436
  145.6 13.1 %collective-permute-start.24 = (bf16[48,4096]{1,0:T(8,128)(2,1)S(1)}, bf16[48,4096]{1,0:T(8,128)(2,1)S(1)}, u32[]{:S(2)}, u32[]{:S(2)}) collective-permute-start(bf16[48,4096]{1,0:T(8,128)(2,1)S(1)} %get-tuple-element.84), channel_id=1, source_target_pairs={{0,1},{1,2},{2,3},{3,0},{4,5},{5,6},{6,7},{7,4},{8,9},{9,10},{10,1... | collective-permute-start | bytes 1179656 | tf_op jit(solution)/shard_map/ppermute | solution.py:436
  145.7 10.6 %collective-permute-start.25 = (bf16[40,4096]{1,0:T(8,128)(2,1)S(1)}, bf16[40,4096]{1,0:T(8,128)(2,1)S(1)}, u32[]{:S(2)}, u32[]{:S(2)}) collective-permute-start(bf16[40,4096]{1,0:T(8,128)(2,1)S(1)} %get-tuple-element.86), channel_id=1, source_target_pairs={{0,3},{1,0},{2,1},{3,2},{4,7},{5,4},{6,5},{7,6},{8,11},{9,8},{10,9... | collective-permute-start | bytes 983048 | tf_op jit(solution)/shard_map/ppermute | solution.py:436
  153.8 21.1 %collective-permute-start.27 = (bf16[48,4096]{1,0:T(8,128)(2,1)S(1)}, bf16[48,4096]{1,0:T(8,128)(2,1)S(1)}, u32[]{:S(2)}, u32[]{:S(2)}) collective-permute-start(bf16[48,4096]{1,0:T(8,128)(2,1)S(1)} %get-tuple-element.88), channel_id=1, source_target_pairs={{0,3},{1,0},{2,1},{3,2},{4,7},{5,4},{6,5},{7,6},{8,11},{9,8},{10,9... | collective-permute-start | bytes 1179656 | tf_op jit(solution)/shard_map/ppermute | solution.py:436
  159.7 15.2 %collective-permute-start.26 = (bf16[48,4096]{1,0:T(8,128)(2,1)S(1)}, bf16[48,4096]{1,0:T(8,128)(2,1)S(1)}, u32[]{:S(2)}, u32[]{:S(2)}) collective-permute-start(bf16[48,4096]{1,0:T(8,128)(2,1)S(1)} %get-tuple-element.87), channel_id=1, source_target_pairs={{0,1},{1,2},{2,3},{3,0},{4,5},{5,6},{6,7},{7,4},{8,9},{9,10},{10,1... | collective-permute-start | bytes 1179656 | tf_op jit(solution)/shard_map/ppermute | solution.py:436
  159.7 15.2 %collective-permute-start.28 = (bf16[40,4096]{1,0:T(8,128)(2,1)}, bf16[40,4096]{1,0:T(8,128)(2,1)S(1)}, u32[]{:S(2)}, u32[]{:S(2)}) collective-permute-start(bf16[40,4096]{1,0:T(8,128)(2,1)} %get-tuple-element.90), channel_id=1, source_target_pairs={{0,1},{1,2},{2,3},{3,0},{4,5},{5,6},{6,7},{7,4},{8,9},{9,10},{10,1... | collective-permute-start | bytes 983048 | tf_op jit(solution)/shard_map/ppermute | solution.py:436
  159.7 15.2 %collective-permute-start.29 = (bf16[40,4096]{1,0:T(8,128)(2,1)}, bf16[40,4096]{1,0:T(8,128)(2,1)S(1)}, u32[]{:S(2)}, u32[]{:S(2)}) collective-permute-start(bf16[40,4096]{1,0:T(8,128)(2,1)} %get-tuple-element.91), channel_id=1, source_target_pairs={{0,3},{1,0},{2,1},{3,2},{4,7},{5,4},{6,5},{7,6},{8,11},{9,8},{10,9... | collective-permute-start | bytes 983048 | tf_op jit(solution)/shard_map/ppermute | solution.py:436
  (18 other events, 412.7 us)

commit v4 on v3

--- a/solution.py
+++ b/solution.py
@@ -214,7 +214,7 @@
         cost_estimate=pl.CostEstimate(
             flops=2 * stack * keys * (2 * HEAD + KEY_BLOCK), transcendentals=3 * stack * keys, bytes_accessed=0
         ),
-        compiler_params=pltpu.CompilerParams(vmem_limit_bytes=24 * 1024 * 1024),
+        compiler_params=pltpu.CompilerParams(vmem_limit_bytes=8 * 1024 * 1024),
     )(position, break_bias, stacked, *key_values, *state)
 
 
@@ -227,7 +227,7 @@
     return lax.ppermute(shard, "sp", pairs)
 
 
-def attend(queries, keys, values, break_bias, pick_ids, position):
+def attend(queries, keys, values, break_bias, pick_ids, position, routing):
     rows = queries.shape[0]
     heads = queries.shape[1] // HEAD
     stacked = jnp.concatenate([queries[:, h * HEAD : (h + 1) * HEAD] for h in range(heads)], axis=0)
@@ -235,6 +235,7 @@
     picks = jnp.concatenate([picks, jnp.zeros((PICK_ROWS - 1, rows * TOP), jnp.bfloat16)], axis=0)
     block = jnp.concatenate([jnp.concatenate([keys, values], axis=1), picks], axis=0)
     own = jnp.stack([block] + [moved(block, 0, step, 0) for step in range(1, X_SIZE)])
+    own, stacked, routing = lax.optimization_barrier((own, stacked, routing))
     twin = moved(own, 0, 0, 1)
     common = (position, break_bias, stacked)
     below, above = own, own
@@ -252,7 +253,7 @@
         name = f"attend_{distance}"
         state = attention_call(kernel, name, 2, *common, arrived[distance - 1], state, rows)
     kernel = functools.partial(last_plane_kernel, Z_SIZE // 2)
-    return attention_call(kernel, "attend_last", 1, *common, arrived[-1], state, rows)
+    return *attention_call(kernel, "attend_last", 1, *common, arrived[-1], state, rows), routing
 
 
 COLUMNS = 1024
@@ -541,8 +542,9 @@
     logits = lax.dynamic_slice_in_dim(pair_logit, quarter * slice_rows, slice_rows, 0)[None]
 
     place = position.reshape(1).astype(jnp.int32)
-    head_out, most = attend(queries, keys, values, break_bias, pick_ids, place)
-    head_out, targets, logits = lax.optimization_barrier((head_out, targets, logits))
+    routing = (targets, logits)
+    head_out, most, routing = attend(queries, keys, values, break_bias, pick_ids, place, routing)
+    targets, logits = routing
     partial = jnp.dot(head_out, w_out, preferred_element_type=jnp.float32).astype(jnp.bfloat16)
     parts = split_up(partial, 0, quarters)
     mixed = lax.all_to_all(parts, "tp", split_axis=0, concat_axis=0, tiled=True)

time: 217 us -> 218 us (level)
  waiting for transfers between devices: 31.3 us -> 35.2 us
  starting transfers between devices: 46.2 us -> 42.8 us
    ppermute x18, waiting for transfers between devices: 6.93 us -> 10.8 us  [moved(): return lax.ppermute(shard, 'sp', pairs)]
    ppermute x18, starting transfers between devices: 31.5 us -> 28.1 us  [moved(): return lax.ppermute(shard, 'sp', pairs)]
where the time goes in v4:
time: 218 us
  blocking collectives  107 us (49%)
  starting transfers between devices  42.8 us (20%)
  waiting for transfers between devices  35.2 us (16%)
  Pallas kernels  22.8 us (10%)
  local copies, waits for them, and re-layouts  5.02 us (2%)
  other arithmetic  3.4 us (2%)
    all_to_all x1, blocking collectives, on_device(): lax.all_to_all(outgoing, 'sp', split_axis=0, concat_axis=0, tiled=True)  48.1 us
    all_to_all x1, blocking collectives, on_device(): lax.all_to_all(results, 'sp', split_axis=0, concat_axis=0, tiled=True)  39.9 us
    ppermute x18, starting transfers between devices, moved(): return lax.ppermute(shard, 'sp', pairs)  28.1 us
    ppermute x12, waiting for transfers between devices, along_tp(): lax.ppermute(shard, 'tp', [(member, (member + step) % size) for member in...  24.4 us
    all_to_all x1, blocking collectives, on_device(): mixed = lax.all_to_all(parts, 'tp', split_axis=0, concat_axis=0, tiled=True)  19 us
    pallas_call x8, Pallas kernels, in_kernel(): pl.pallas_call(kernel, out_shape=out_shapes, in_specs=[spec] * len(operan...  16.7 us
    ppermute x12, starting transfers between devices, along_tp(): lax.ppermute(shard, 'tp', [(member, (member + step) % size) for member in...  14.7 us
    ppermute x18, waiting for transfers between devices, moved(): return lax.ppermute(shard, 'sp', pairs)  10.8 us
  transfers between devices with their start and end apart: 30, of which 11 were waited for; matrix products, arithmetic and copies ran while one was open for 2% of the time, Pallas kernels for 8%

profile of v4, /device:TPU:1, one launch (start us, length us, event | category | flops | bytes accessed | tf_op | source)
XLA Modules:
  0.0 217.9 jit_solution(9745261877210283790)
XLA Ops:
  3.8 2.5 %collective-permute-start.1 = (bf16[136,256]{1,0:T(8,128)(2,1)S(1)}, bf16[136,256]{1,0:T(8,128)(2,1)S(1)}, u32[]{:S(2)}, u32[]{:S(2)}) collective-permute-start(bf16[136,256]{1,0:T(8,128)(2,1)S(1)} %maximum_maximum_fusion), channel_id=1, source_target_pairs={{0,16},{4,20},{8,24},{12,28},{16,0},{20,4},{24,8},{28,12},{32,48},... | collective-permute-start | bytes 208904 | tf_op jit(solution)/shard_map/ppermute | solution.py:227
  12.8 4.0 %collective-permute-start.9 = (bf16[4,136,256]{2,1,0:T(8,128)(2,1)S(1)}, bf16[4,136,256]{2,1,0:T(8,128)(2,1)S(1)}, u32[]{:S(2)}, u32[]{:S(2)}) collective-permute-start(bf16[4,136,256]{2,1,0:T(8,128)(2,1)S(1)} %pad_maximum_fusion.own_ref), channel_id=1, source_target_pairs={{0,224},{4,228},{8,232},{12,236},{16,240},{20,244},{24,248},{28,25... | collective-permute-start | bytes 835592 | tf_op jit(solution)/shard_map/ppermute | solution.py:227
  16.8 5.4 %collective-permute-done.3.below = bf16[4,136,256]{2,1,0:T(8,128)(2,1)S(1)} collective-permute-done((bf16[4,136,256]{2,1,0:T(8,128)(2,1)S(1)}, bf16[4,136,256]{2,1,0:T(8,128)(2,1)S(1)}, u32[]{:S(2)}, u32[]{:S(2)}) %collective-permute-start.3) | collective-permute-done | bytes 278560 | tf_op jit(solution)/shard_map/ppermute | solution.py:227
  22.3 2.7 %collective-permute-start.10 = (bf16[4,136,256]{2,1,0:T(8,128)(2,1)S(1)}, bf16[4,136,256]{2,1,0:T(8,128)(2,1)S(1)}, u32[]{:S(2)}, u32[]{:S(2)}) collective-permute-start(bf16[4,136,256]{2,1,0:T(8,128)(2,1)S(1)} %collective-permute-done.9.above), channel_id=1, source_target_pairs={{0,224},{4,228},{8,232},{12,236},{16,240},{20,244},{24,248},{28,25... | collective-permute-start | bytes 835592 | tf_op jit(solution)/shard_map/ppermute | solution.py:227
  24.9 4.7 %collective-permute-done.4.below = bf16[4,136,256]{2,1,0:T(8,128)(2,1)S(1)} collective-permute-done((bf16[4,136,256]{2,1,0:T(8,128)(2,1)S(1)}, bf16[4,136,256]{2,1,0:T(8,128)(2,1)S(1)}, u32[]{:S(2)}, u32[]{:S(2)}) %collective-permute-start.4) | collective-permute-done | bytes 278560 | tf_op jit(solution)/shard_map/ppermute | solution.py:227
  29.6 3.0 %collective-permute-start.17 = (bf16[4,136,256]{2,1,0:T(8,128)(2,1)S(1)}, bf16[4,136,256]{2,1,0:T(8,128)(2,1)S(1)}, u32[]{:S(2)}, u32[]{:S(2)}) collective-permute-start(bf16[4,136,256]{2,1,0:T(8,128)(2,1)S(1)} %pad_maximum_fusion.own_ref), channel_id=1, source_target_pairs={{0,4},{4,0},{8,12},{12,8},{16,20},{20,16},{24,28},{28,24},{32,36},... | collective-permute-start | bytes 835592 | tf_op jit(solution)/shard_map/ppermute | solution.py:227
  33.1 3.0 %collective-permute-start.11 = (bf16[4,136,256]{2,1,0:T(8,128)(2,1)S(1)}, bf16[4,136,256]{2,1,0:T(8,128)(2,1)S(1)}, u32[]{:S(2)}, u32[]{:S(2)}) collective-permute-start(bf16[4,136,256]{2,1,0:T(8,128)(2,1)S(1)} %collective-permute-done.10.above), channel_id=1, source_target_pairs={{0,224},{4,228},{8,232},{12,236},{16,240},{20,244},{24,248},{28,25... | collective-permute-start | bytes 835592 | tf_op jit(solution)/shard_map/ppermute | solution.py:227
  36.9 4.1 %collective-permute-start.13 = (bf16[4,136,256]{2,1,0:T(8,128)(2,1)S(1)}, bf16[4,136,256]{2,1,0:T(8,128)(2,1)}, u32[]{:S(2)}, u32[]{:S(2)}) collective-permute-start(bf16[4,136,256]{2,1,0:T(8,128)(2,1)S(1)} %collective-permute-done.4.below), channel_id=1, source_target_pairs={{0,4},{4,0},{8,12},{12,8},{16,20},{20,16},{24,28},{28,24},{32,36},... | collective-permute-start | bytes 835592 | tf_op jit(solution)/shard_map/ppermute | solution.py:227
  53.6 19.0 %all_to_all.25.mixed_ref = bf16[4,32,4096]{2,1,0:T(8,128)(2,1)S(1)} all-to-all(bf16[4,32,4096]{2,1,0:T(8,128)(2,1)S(1)} %bitcast.46), channel_id=1, replica_groups=mesh['sp'=64,'tp'=4] {'tp'}, dimensions={0} | all-to-all | bytes 2097152 | tf_op jit(solution)/shard_map/all_to_all | solution.py:550
  73.4 48.1 %all_to_all.26.arrived_ref = bf16[64,2,4096]{2,1,0:T(2,128)(2,1)S(1)} all-to-all(bf16[64,2,4096]{2,1,0:T(2,128)(2,1)S(1)} %get-tuple-element.78), channel_id=1, replica_groups=mesh['sp'=64,'tp'=4] {'sp'}, dimensions={0} | all-to-all | bytes 2097152 | tf_op jit(solution)/shard_map/all_to_all | solution.py:558
  121.6 2.3 %shard_map.133 = (bf16[48,4096]{1,0:T(8,128)(2,1)S(1)}, bf16[40,4096]{1,0:T(8,128)(2,1)S(1)}, bf16[40,4096]{1,0:T(8,128)(2,1)}, bf16[128,128]{1,0:T(8,128)(2,1)S(1)}) custom-call(bf16[64,2,4096]{2,1,0:T(2,128)(2,1)S(1)} %all_to_all.26.arrived_ref), custom_call_target="tpu_custom_call" | custom-call | flops 134217728 | tf_op jit(solution)/shard_map/pallas_call | solution.py:266
  124.2 2.4 %collective-permute-start.21 = (bf16[40,4096]{1,0:T(8,128)(2,1)S(1)}, bf16[40,4096]{1,0:T(8,128)(2,1)S(1)}, u32[]{:S(2)}, u32[]{:S(2)}) collective-permute-start(bf16[40,4096]{1,0:T(8,128)(2,1)S(1)} %get-tuple-element.83.refs_1_), channel_id=1, source_target_pairs={{0,3},{1,0},{2,1},{3,2},{4,7},{5,4},{6,5},{7,6},{8,11},{9,8},{10,9... | collective-permute-start | bytes 983048 | tf_op jit(solution)/shard_map/ppermute | solution.py:437
  126.5 8.1 %collective-permute-done.18.refs_0_ = bf16[48,4096]{1,0:T(8,128)(2,1)S(1)} collective-permute-done((bf16[48,4096]{1,0:T(8,128)(2,1)S(1)}, bf16[48,4096]{1,0:T(8,128)(2,1)S(1)}, u32[]{:S(2)}, u32[]{:S(2)}) %collective-permute-start.18) | collective-permute-done | bytes 393248 | tf_op jit(solution)/shard_map/ppermute | solution.py:437
  134.6 2.7 %collective-permute-start.23 = (bf16[40,4096]{1,0:T(8,128)(2,1)S(1)}, bf16[40,4096]{1,0:T(8,128)(2,1)S(1)}, u32[]{:S(2)}, u32[]{:S(2)}) collective-permute-start(bf16[40,4096]{1,0:T(8,128)(2,1)S(1)} %collective-permute-done.21.refs_3_), channel_id=1, source_target_pairs={{0,3},{1,0},{2,1},{3,2},{4,7},{5,4},{6,5},{7,6},{8,11},{9,8},{10,9... | collective-permute-start | bytes 983048 | tf_op jit(solution)/shard_map/ppermute | solution.py:437
  138.8 3.3 %collective-permute-done.23.refs_1_ = bf16[40,4096]{1,0:T(8,128)(2,1)S(1)} collective-permute-done((bf16[40,4096]{1,0:T(8,128)(2,1)S(1)}, bf16[40,4096]{1,0:T(8,128)(2,1)S(1)}, u32[]{:S(2)}, u32[]{:S(2)}) %collective-permute-start.23) | collective-permute-done | bytes 327712 | tf_op jit(solution)/shard_map/ppermute | solution.py:437
  142.1 2.4 %collective-permute-done.22.refs_0_ = bf16[48,4096]{1,0:T(8,128)(2,1)S(1)} collective-permute-done((bf16[48,4096]{1,0:T(8,128)(2,1)S(1)}, bf16[48,4096]{1,0:T(8,128)(2,1)S(1)}, u32[]{:S(2)}, u32[]{:S(2)}) %collective-permute-start.22) | collective-permute-done | bytes 393248 | tf_op jit(solution)/shard_map/ppermute | solution.py:437
  146.8 2.7 %collective-permute-start.25 = (bf16[40,4096]{1,0:T(8,128)(2,1)S(1)}, bf16[40,4096]{1,0:T(8,128)(2,1)S(1)}, u32[]{:S(2)}, u32[]{:S(2)}) collective-permute-start(bf16[40,4096]{1,0:T(8,128)(2,1)S(1)} %get-tuple-element.88), channel_id=1, source_target_pairs={{0,3},{1,0},{2,1},{3,2},{4,7},{5,4},{6,5},{7,6},{8,11},{9,8},{10,9... | collective-permute-start | bytes 983048 | tf_op jit(solution)/shard_map/ppermute | solution.py:437
  151.5 3.4 %shard_map.135 = (bf16[48,4096]{1,0:T(8,128)(2,1)S(1)}, bf16[40,4096]{1,0:T(8,128)(2,1)S(1)}, bf16[48,4096]{1,0:T(8,128)(2,1)S(1)}, bf16[40,4096]{1,0:T(8,128)(2,1)}) custom-call(bf16[48,4096]{1,0:T(8,128)(2,1)S(1)} %collective-permute-done.18.refs_0_, bf16[40,4096]{1,0:T(8,128)(2,1)S(1)} %collective-permute-done.19.refs_1_, ...), custom_call_target="tpu_custom_call" | custom-call | flops 1107296256 | tf_op jit(solution)/shard_map/pallas_call | solution.py:266
  154.9 2.4 %collective-permute-start.27 = (bf16[48,4096]{1,0:T(8,128)(2,1)S(1)}, bf16[48,4096]{1,0:T(8,128)(2,1)S(1)}, u32[]{:S(2)}, u32[]{:S(2)}) collective-permute-start(bf16[48,4096]{1,0:T(8,128)(2,1)S(1)} %get-tuple-element.90), channel_id=1, source_target_pairs={{0,3},{1,0},{2,1},{3,2},{4,7},{5,4},{6,5},{7,6},{8,11},{9,8},{10,9... | collective-permute-start | bytes 1179656 | tf_op jit(solution)/shard_map/ppermute | solution.py:437
  157.5 2.4 %collective-permute-done.24.far_up = bf16[48,4096]{1,0:T(8,128)(2,1)S(1)} collective-permute-done((bf16[48,4096]{1,0:T(8,128)(2,1)S(1)}, bf16[48,4096]{1,0:T(8,128)(2,1)S(1)}, u32[]{:S(2)}, u32[]{:S(2)}) %collective-permute-start.24) | collective-permute-done | bytes 393248 | tf_op jit(solution)/shard_map/ppermute | solution.py:437
  160.8 2.7 %collective-permute-start.29 = (bf16[40,4096]{1,0:T(8,128)(2,1)}, bf16[40,4096]{1,0:T(8,128)(2,1)S(1)}, u32[]{:S(2)}, u32[]{:S(2)}) collective-permute-start(bf16[40,4096]{1,0:T(8,128)(2,1)} %get-tuple-element.93), channel_id=1, source_target_pairs={{0,3},{1,0},{2,1},{3,2},{4,7},{5,4},{6,5},{7,6},{8,11},{9,8},{10,9... | collective-permute-start | bytes 983048 | tf_op jit(solution)/shard_map/ppermute | solution.py:437
  164.9 5.1 %shard_map.134 = (bf16[48,4096]{1,0:T(8,128)(2,1)S(1)}, bf16[40,4096]{1,0:T(8,128)(2,1)S(1)}) custom-call(bf16[48,4096]{1,0:T(8,128)(2,1)S(1)} %get-tuple-element.82.refs_0_, bf16[40,4096]{1,0:T(8,128)(2,1)S(1)} %get-tuple-element.83.refs_1_, bf16[4096,256]{1,0:T(8,128)(2,1)} %bitcast.34, bf16[4096,256]{1,0:T(8,128)(2,1)} %bitcast.38, bf16[256,4096]{1,0:T(8,128)(2,1)} %bitcast.42), custom_call_target="tpu_custom_call" | custom-call | flops 553648128 | tf_op jit(solution)/shard_map/pallas_call | solution.py:266
  170.0 6.0 %collective-permute-done.28.refs_4_ = bf16[40,4096]{1,0:T(8,128)(2,1)S(1)} collective-permute-done((bf16[40,4096]{1,0:T(8,128)(2,1)}, bf16[40,4096]{1,0:T(8,128)(2,1)S(1)}, u32[]{:S(2)}, u32[]{:S(2)}) %collective-permute-start.28) | collective-permute-done | bytes 327712 | tf_op jit(solution)/shard_map/ppermute | solution.py:437
  176.7 39.9 %all_to_all.27.returned_ref = bf16[64,2,4096]{2,1,0:T(2,128)(2,1)S(1)} all-to-all(bf16[64,2,4096]{2,1,0:T(2,128)(2,1)S(1)} %shard_map.138), channel_id=1, replica_groups=mesh['sp'=64,'tp'=4] {'sp'}, dimensions={0} | all-to-all | bytes 2097152 | tf_op jit(solution)/shard_map/all_to_all | solution.py:560
  (94 shorter events, 35.7 us)
Async XLA Ops:
  1.7 9.4 %collective-permute-start = (bf16[136,256]{1,0:T(8,128)(2,1)S(1)}, bf16[136,256]{1,0:T(8,128)(2,1)S(1)}, u32[]{:S(2)}, u32[]{:S(2)}) collective-permute-start(bf16[136,256]{1,0:T(8,128)(2,1)S(1)} %maximum_maximum_fusion), channel_id=1, source_target_pairs={{0,8},{4,12},{8,16},{12,20},{16,24},{20,28},{24,0},{28,4},{32,40},... | collective-permute-start | bytes 208904 | tf_op jit(solution)/shard_map/ppermute | solution.py:227
  11.1 11.2 %collective-permute-start.3 = (bf16[4,136,256]{2,1,0:T(8,128)(2,1)S(1)}, bf16[4,136,256]{2,1,0:T(8,128)(2,1)S(1)}, u32[]{:S(2)}, u32[]{:S(2)}) collective-permute-start(bf16[4,136,256]{2,1,0:T(8,128)(2,1)S(1)} %pad_maximum_fusion.own_ref), channel_id=1, source_target_pairs={{0,32},{4,36},{8,40},{12,44},{16,48},{20,52},{24,56},{28,60},{32,6... | collective-permute-start | bytes 835592 | tf_op jit(solution)/shard_map/ppermute | solution.py:227
  12.8 9.5 %collective-permute-start.9 = (bf16[4,136,256]{2,1,0:T(8,128)(2,1)S(1)}, bf16[4,136,256]{2,1,0:T(8,128)(2,1)S(1)}, u32[]{:S(2)}, u32[]{:S(2)}) collective-permute-start(bf16[4,136,256]{2,1,0:T(8,128)(2,1)S(1)} %pad_maximum_fusion.own_ref), channel_id=1, source_target_pairs={{0,224},{4,228},{8,232},{12,236},{16,240},{20,244},{24,248},{28,25... | collective-permute-start | bytes 835592 | tf_op jit(solution)/shard_map/ppermute | solution.py:227
  22.3 10.8 %collective-permute-start.10 = (bf16[4,136,256]{2,1,0:T(8,128)(2,1)S(1)}, bf16[4,136,256]{2,1,0:T(8,128)(2,1)S(1)}, u32[]{:S(2)}, u32[]{:S(2)}) collective-permute-start(bf16[4,136,256]{2,1,0:T(8,128)(2,1)S(1)} %collective-permute-done.9.above), channel_id=1, source_target_pairs={{0,224},{4,228},{8,232},{12,236},{16,240},{20,244},{24,248},{28,25... | collective-permute-start | bytes 835592 | tf_op jit(solution)/shard_map/ppermute | solution.py:227
  32.5 8.5 %collective-permute-start.15 = (bf16[4,136,256]{2,1,0:T(8,128)(2,1)S(1)}, bf16[4,136,256]{2,1,0:T(8,128)(2,1)S(1)}, u32[]{:S(2)}, u32[]{:S(2)}) collective-permute-start(bf16[4,136,256]{2,1,0:T(8,128)(2,1)S(1)} %collective-permute-done.3.below), channel_id=1, source_target_pairs={{0,4},{4,0},{8,12},{12,8},{16,20},{20,16},{24,28},{28,24},{32,36},... | collective-permute-start | bytes 835592 | tf_op jit(solution)/shard_map/ppermute | solution.py:227
  32.5 8.5 %collective-permute-start.16 = (bf16[4,136,256]{2,1,0:T(8,128)(2,1)S(1)}, bf16[4,136,256]{2,1,0:T(8,128)(2,1)S(1)}, u32[]{:S(2)}, u32[]{:S(2)}) collective-permute-start(bf16[4,136,256]{2,1,0:T(8,128)(2,1)S(1)} %collective-permute-done.9.above), channel_id=1, source_target_pairs={{0,4},{4,0},{8,12},{12,8},{16,20},{20,16},{24,28},{28,24},{32,36},... | collective-permute-start | bytes 835592 | tf_op jit(solution)/shard_map/ppermute | solution.py:227
  33.1 9.0 %collective-permute-start.11 = (bf16[4,136,256]{2,1,0:T(8,128)(2,1)S(1)}, bf16[4,136,256]{2,1,0:T(8,128)(2,1)S(1)}, u32[]{:S(2)}, u32[]{:S(2)}) collective-permute-start(bf16[4,136,256]{2,1,0:T(8,128)(2,1)S(1)} %collective-permute-done.10.above), channel_id=1, source_target_pairs={{0,224},{4,228},{8,232},{12,236},{16,240},{20,244},{24,248},{28,25... | collective-permute-start | bytes 835592 | tf_op jit(solution)/shard_map/ppermute | solution.py:227
  36.2 9.8 %collective-permute-start.6 = (bf16[4,136,256]{2,1,0:T(8,128)(2,1)S(1)}, bf16[4,136,256]{2,1,0:T(8,128)(2,1)S(1)}, u32[]{:S(2)}, u32[]{:S(2)}) collective-permute-start(bf16[4,136,256]{2,1,0:T(8,128)(2,1)S(1)} %collective-permute-done.5.below), channel_id=1, source_target_pairs={{0,32},{4,36},{8,40},{12,44},{16,48},{20,52},{24,56},{28,60},{32,6... | collective-permute-start | bytes 835592 | tf_op jit(solution)/shard_map/ppermute | solution.py:227
  36.9 11.9 %collective-permute-start.13 = (bf16[4,136,256]{2,1,0:T(8,128)(2,1)S(1)}, bf16[4,136,256]{2,1,0:T(8,128)(2,1)}, u32[]{:S(2)}, u32[]{:S(2)}) collective-permute-start(bf16[4,136,256]{2,1,0:T(8,128)(2,1)S(1)} %collective-permute-done.4.below), channel_id=1, source_target_pairs={{0,4},{4,0},{8,12},{12,8},{16,20},{20,16},{24,28},{28,24},{32,36},... | collective-permute-start | bytes 835592 | tf_op jit(solution)/shard_map/ppermute | solution.py:227
  41.0 7.8 %collective-permute-start.14 = (bf16[4,136,256]{2,1,0:T(8,128)(2,1)S(1)}, bf16[4,136,256]{2,1,0:T(8,128)(2,1)}, u32[]{:S(2)}, u32[]{:S(2)}) collective-permute-start(bf16[4,136,256]{2,1,0:T(8,128)(2,1)S(1)} %collective-permute-done.10.above), channel_id=1, source_target_pairs={{0,4},{4,0},{8,12},{12,8},{16,20},{20,16},{24,28},{28,24},{32,36},... | collective-permute-start | bytes 835592 | tf_op jit(solution)/shard_map/ppermute | solution.py:227
  41.0 9.1 %collective-permute-start.8 = (bf16[4,136,256]{2,1,0:T(8,128)(2,1)S(1)}, bf16[4,136,256]{2,1,0:T(8,128)(2,1)S(1)}, u32[]{:S(2)}, u32[]{:S(2)}) collective-permute-start(bf16[4,136,256]{2,1,0:T(8,128)(2,1)S(1)} %collective-permute-done.5.below), channel_id=1, source_target_pairs={{0,4},{4,0},{8,12},{12,8},{16,20},{20,16},{24,28},{28,24},{32,36},... | collective-permute-start | bytes 835592 | tf_op jit(solution)/shard_map/ppermute | solution.py:227
  42.0 8.1 %collective-permute-start.12 = (bf16[4,136,256]{2,1,0:T(8,128)(2,1)S(1)}, bf16[4,136,256]{2,1,0:T(8,128)(2,1)}, u32[]{:S(2)}, u32[]{:S(2)}) collective-permute-start(bf16[4,136,256]{2,1,0:T(8,128)(2,1)S(1)} %collective-permute-done.11.above), channel_id=1, source_target_pairs={{0,4},{4,0},{8,12},{12,8},{16,20},{20,16},{24,28},{28,24},{32,36},... | collective-permute-start | bytes 835592 | tf_op jit(solution)/shard_map/ppermute | solution.py:227
  123.9 10.7 %collective-permute-start.18 = (bf16[48,4096]{1,0:T(8,128)(2,1)S(1)}, bf16[48,4096]{1,0:T(8,128)(2,1)S(1)}, u32[]{:S(2)}, u32[]{:S(2)}) collective-permute-start(bf16[48,4096]{1,0:T(8,128)(2,1)S(1)} %get-tuple-element.82.refs_0_), channel_id=1, source_target_pairs={{0,1},{1,2},{2,3},{3,0},{4,5},{5,6},{6,7},{7,4},{8,9},{9,10},{10,1... | collective-permute-start | bytes 1179656 | tf_op jit(solution)/shard_map/ppermute | solution.py:437
  124.2 10.5 %collective-permute-start.21 = (bf16[40,4096]{1,0:T(8,128)(2,1)S(1)}, bf16[40,4096]{1,0:T(8,128)(2,1)S(1)}, u32[]{:S(2)}, u32[]{:S(2)}) collective-permute-start(bf16[40,4096]{1,0:T(8,128)(2,1)S(1)} %get-tuple-element.83.refs_1_), channel_id=1, source_target_pairs={{0,3},{1,0},{2,1},{3,2},{4,7},{5,4},{6,5},{7,6},{8,11},{9,8},{10,9... | collective-permute-start | bytes 983048 | tf_op jit(solution)/shard_map/ppermute | solution.py:437
  134.6 9.9 %collective-permute-start.22 = (bf16[48,4096]{1,0:T(8,128)(2,1)S(1)}, bf16[48,4096]{1,0:T(8,128)(2,1)S(1)}, u32[]{:S(2)}, u32[]{:S(2)}) collective-permute-start(bf16[48,4096]{1,0:T(8,128)(2,1)S(1)} %collective-permute-done.18.refs_0_), channel_id=1, source_target_pairs={{0,1},{1,2},{2,3},{3,0},{4,5},{5,6},{6,7},{7,4},{8,9},{9,10},{10,1... | collective-permute-start | bytes 1179656 | tf_op jit(solution)/shard_map/ppermute | solution.py:437
  134.6 7.5 %collective-permute-start.23 = (bf16[40,4096]{1,0:T(8,128)(2,1)S(1)}, bf16[40,4096]{1,0:T(8,128)(2,1)S(1)}, u32[]{:S(2)}, u32[]{:S(2)}) collective-permute-start(bf16[40,4096]{1,0:T(8,128)(2,1)S(1)} %collective-permute-done.21.refs_3_), channel_id=1, source_target_pairs={{0,3},{1,0},{2,1},{3,2},{4,7},{5,4},{6,5},{7,6},{8,11},{9,8},{10,9... | collective-permute-start | bytes 983048 | tf_op jit(solution)/shard_map/ppermute | solution.py:437
  137.3 14.2 %collective-permute-start.20 = (bf16[48,4096]{1,0:T(8,128)(2,1)S(1)}, bf16[48,4096]{1,0:T(8,128)(2,1)S(1)}, u32[]{:S(2)}, u32[]{:S(2)}) collective-permute-start(bf16[48,4096]{1,0:T(8,128)(2,1)S(1)} %get-tuple-element.82.refs_0_), channel_id=1, source_target_pairs={{0,3},{1,0},{2,1},{3,2},{4,7},{5,4},{6,5},{7,6},{8,11},{9,8},{10,9... | collective-permute-start | bytes 1179656 | tf_op jit(solution)/shard_map/ppermute | solution.py:437
  137.3 14.2 %collective-permute-start.19 = (bf16[40,4096]{1,0:T(8,128)(2,1)S(1)}, bf16[40,4096]{1,0:T(8,128)(2,1)S(1)}, u32[]{:S(2)}, u32[]{:S(2)}) collective-permute-start(bf16[40,4096]{1,0:T(8,128)(2,1)S(1)} %get-tuple-element.83.refs_1_), channel_id=1, source_target_pairs={{0,1},{1,2},{2,3},{3,0},{4,5},{5,6},{6,7},{7,4},{8,9},{9,10},{10,1... | collective-permute-start | bytes 983048 | tf_op jit(solution)/shard_map/ppermute | solution.py:437
  146.7 13.1 %collective-permute-start.24 = (bf16[48,4096]{1,0:T(8,128)(2,1)S(1)}, bf16[48,4096]{1,0:T(8,128)(2,1)S(1)}, u32[]{:S(2)}, u32[]{:S(2)}) collective-permute-start(bf16[48,4096]{1,0:T(8,128)(2,1)S(1)} %get-tuple-element.86), channel_id=1, source_target_pairs={{0,1},{1,2},{2,3},{3,0},{4,5},{5,6},{6,7},{7,4},{8,9},{9,10},{10,1... | collective-permute-start | bytes 1179656 | tf_op jit(solution)/shard_map/ppermute | solution.py:437
  146.8 10.6 %collective-permute-start.25 = (bf16[40,4096]{1,0:T(8,128)(2,1)S(1)}, bf16[40,4096]{1,0:T(8,128)(2,1)S(1)}, u32[]{:S(2)}, u32[]{:S(2)}) collective-permute-start(bf16[40,4096]{1,0:T(8,128)(2,1)S(1)} %get-tuple-element.88), channel_id=1, source_target_pairs={{0,3},{1,0},{2,1},{3,2},{4,7},{5,4},{6,5},{7,6},{8,11},{9,8},{10,9... | collective-permute-start | bytes 983048 | tf_op jit(solution)/shard_map/ppermute | solution.py:437
  154.9 21.1 %collective-permute-start.27 = (bf16[48,4096]{1,0:T(8,128)(2,1)S(1)}, bf16[48,4096]{1,0:T(8,128)(2,1)S(1)}, u32[]{:S(2)}, u32[]{:S(2)}) collective-permute-start(bf16[48,4096]{1,0:T(8,128)(2,1)S(1)} %get-tuple-element.90), channel_id=1, source_target_pairs={{0,3},{1,0},{2,1},{3,2},{4,7},{5,4},{6,5},{7,6},{8,11},{9,8},{10,9... | collective-permute-start | bytes 1179656 | tf_op jit(solution)/shard_map/ppermute | solution.py:437
  160.8 15.2 %collective-permute-start.26 = (bf16[48,4096]{1,0:T(8,128)(2,1)S(1)}, bf16[48,4096]{1,0:T(8,128)(2,1)S(1)}, u32[]{:S(2)}, u32[]{:S(2)}) collective-permute-start(bf16[48,4096]{1,0:T(8,128)(2,1)S(1)} %get-tuple-element.89), channel_id=1, source_target_pairs={{0,1},{1,2},{2,3},{3,0},{4,5},{5,6},{6,7},{7,4},{8,9},{9,10},{10,1... | collective-permute-start | bytes 1179656 | tf_op jit(solution)/shard_map/ppermute | solution.py:437
  160.8 15.2 %collective-permute-start.28 = (bf16[40,4096]{1,0:T(8,128)(2,1)}, bf16[40,4096]{1,0:T(8,128)(2,1)S(1)}, u32[]{:S(2)}, u32[]{:S(2)}) collective-permute-start(bf16[40,4096]{1,0:T(8,128)(2,1)} %get-tuple-element.92), channel_id=1, source_target_pairs={{0,1},{1,2},{2,3},{3,0},{4,5},{5,6},{6,7},{7,4},{8,9},{9,10},{10,1... | collective-permute-start | bytes 983048 | tf_op jit(solution)/shard_map/ppermute | solution.py:437
  160.8 15.2 %collective-permute-start.29 = (bf16[40,4096]{1,0:T(8,128)(2,1)}, bf16[40,4096]{1,0:T(8,128)(2,1)S(1)}, u32[]{:S(2)}, u32[]{:S(2)}) collective-permute-start(bf16[40,4096]{1,0:T(8,128)(2,1)} %get-tuple-element.93), channel_id=1, source_target_pairs={{0,3},{1,0},{2,1},{3,2},{4,7},{5,4},{6,5},{7,6},{8,11},{9,8},{10,9... | collective-permute-start | bytes 983048 | tf_op jit(solution)/shard_map/ppermute | solution.py:437
  (18 other events, 378.3 us)

commit v5 on v4

--- a/solution.py
+++ b/solution.py
@@ -28,6 +28,7 @@
 KEY_BLOCK = 256
 MOST = 100.0
 PICK_ROWS = 8
+TOGETHER = 2
 
 
 def causal_visit(state, query_ref, kv_ref, bias_ref, later, block, first_query):
@@ -117,17 +118,17 @@
     lax.fori_loop(0, last + 1, step, 0)
 
 
-def whole_plane(state, query_ref, plane, bias_ref, together=2):
+def whole_plane(state, query_ref, plane, bias_ref):
     later = later_keys()
     blocks = plane.shape[0] // KEY_BLOCK
 
     def step(index, carried):
-        for offset in range(together):
-            block = blocks - 1 - offset - together * index
+        for offset in range(TOGETHER):
+            block = blocks - 1 - offset - TOGETHER * index
             causal_visit(state, query_ref, plane, bias_ref, later, block, None)
         return carried
 
-    lax.fori_loop(0, blocks // together, step, 0)
+    lax.fori_loop(0, blocks // TOGETHER, step, 0)
 
 
 def two_planes_kernel(distance, place_ref, bias_ref, query_ref, below, below_twin, above, above_twin,
@@ -178,7 +179,7 @@
     @pl.when(place // (X_SIZE * CORES) >= distance)
     def _():
         lay_out(below, below_twin, plane, place)
-        whole_plane((near, near_used), query_ref, plane, bias_ref, 1)
+        whole_plane((near, near_used), query_ref, plane, bias_ref)
 
     rows = out_ref.shape[0]
     for head in range(bias_ref.shape[0]):

time: 218 us -> 218 us (level)
  no operation moved by 1% of the time
where the time goes in v5:
time: 218 us; the launch traced here: 217 us
  blocking collectives  106 us (49%)
  starting transfers between devices  42.8 us (20%)
  waiting for transfers between devices  35.2 us (16%)
  Pallas kernels  22.8 us (10%)
  local copies, waits for them, and re-layouts  5.02 us (2%)
  other arithmetic  3.4 us (2%)
    all_to_all x1, blocking collectives, on_device(): lax.all_to_all(outgoing, 'sp', split_axis=0, concat_axis=0, tiled=True)  47.5 us
    all_to_all x1, blocking collectives, on_device(): lax.all_to_all(results, 'sp', split_axis=0, concat_axis=0, tiled=True)  39.8 us
    ppermute x18, starting transfers between devices, moved(): return lax.ppermute(shard, 'sp', pairs)  28.1 us
    ppermute x12, waiting for transfers between devices, along_tp(): lax.ppermute(shard, 'tp', [(member, (member + step) % size) for member in...  24.4 us
    all_to_all x1, blocking collectives, on_device(): mixed = lax.all_to_all(parts, 'tp', split_axis=0, concat_axis=0, tiled=True)  19 us
    pallas_call x8, Pallas kernels, in_kernel(): pl.pallas_call(kernel, out_shape=out_shapes, in_specs=[spec] * len(operan...  16.7 us
    ppermute x12, starting transfers between devices, along_tp(): lax.ppermute(shard, 'tp', [(member, (member + step) % size) for member in...  14.7 us
    ppermute x18, waiting for transfers between devices, moved(): return lax.ppermute(shard, 'sp', pairs)  10.8 us
  transfers between devices with their start and end apart: 30, of which 11 were waited for; matrix products, arithmetic and copies ran while one was open for 2% of the time, Pallas kernels for 8%

profile of v5, /device:TPU:1, one launch (start us, length us, event | category | flops | bytes accessed | tf_op | source)
XLA Modules:
  0.0 217.2 jit_solution(10588993955312207101)
XLA Ops:
  3.8 2.5 %collective-permute-start.1 = (bf16[136,256]{1,0:T(8,128)(2,1)S(1)}, bf16[136,256]{1,0:T(8,128)(2,1)S(1)}, u32[]{:S(2)}, u32[]{:S(2)}) collective-permute-start(bf16[136,256]{1,0:T(8,128)(2,1)S(1)} %maximum_maximum_fusion), channel_id=1, source_target_pairs={{0,16},{4,20},{8,24},{12,28},{16,0},{20,4},{24,8},{28,12},{32,48},... | collective-permute-start | bytes 208904 | tf_op jit(solution)/shard_map/ppermute | solution.py:228
  12.8 4.0 %collective-permute-start.9 = (bf16[4,136,256]{2,1,0:T(8,128)(2,1)S(1)}, bf16[4,136,256]{2,1,0:T(8,128)(2,1)S(1)}, u32[]{:S(2)}, u32[]{:S(2)}) collective-permute-start(bf16[4,136,256]{2,1,0:T(8,128)(2,1)S(1)} %pad_maximum_fusion.own_ref), channel_id=1, source_target_pairs={{0,224},{4,228},{8,232},{12,236},{16,240},{20,244},{24,248},{28,25... | collective-permute-start | bytes 835592 | tf_op jit(solution)/shard_map/ppermute | solution.py:228
  16.8 5.4 %collective-permute-done.3.below = bf16[4,136,256]{2,1,0:T(8,128)(2,1)S(1)} collective-permute-done((bf16[4,136,256]{2,1,0:T(8,128)(2,1)S(1)}, bf16[4,136,256]{2,1,0:T(8,128)(2,1)S(1)}, u32[]{:S(2)}, u32[]{:S(2)}) %collective-permute-start.3) | collective-permute-done | bytes 278560 | tf_op jit(solution)/shard_map/ppermute | solution.py:228
  22.3 2.7 %collective-permute-start.10 = (bf16[4,136,256]{2,1,0:T(8,128)(2,1)S(1)}, bf16[4,136,256]{2,1,0:T(8,128)(2,1)S(1)}, u32[]{:S(2)}, u32[]{:S(2)}) collective-permute-start(bf16[4,136,256]{2,1,0:T(8,128)(2,1)S(1)} %collective-permute-done.9.above), channel_id=1, source_target_pairs={{0,224},{4,228},{8,232},{12,236},{16,240},{20,244},{24,248},{28,25... | collective-permute-start | bytes 835592 | tf_op jit(solution)/shard_map/ppermute | solution.py:228
  24.9 4.7 %collective-permute-done.4.below = bf16[4,136,256]{2,1,0:T(8,128)(2,1)S(1)} collective-permute-done((bf16[4,136,256]{2,1,0:T(8,128)(2,1)S(1)}, bf16[4,136,256]{2,1,0:T(8,128)(2,1)S(1)}, u32[]{:S(2)}, u32[]{:S(2)}) %collective-permute-start.4) | collective-permute-done | bytes 278560 | tf_op jit(solution)/shard_map/ppermute | solution.py:228
  29.6 3.0 %collective-permute-start.17 = (bf16[4,136,256]{2,1,0:T(8,128)(2,1)S(1)}, bf16[4,136,256]{2,1,0:T(8,128)(2,1)S(1)}, u32[]{:S(2)}, u32[]{:S(2)}) collective-permute-start(bf16[4,136,256]{2,1,0:T(8,128)(2,1)S(1)} %pad_maximum_fusion.own_ref), channel_id=1, source_target_pairs={{0,4},{4,0},{8,12},{12,8},{16,20},{20,16},{24,28},{28,24},{32,36},... | collective-permute-start | bytes 835592 | tf_op jit(solution)/shard_map/ppermute | solution.py:228
  33.1 3.0 %collective-permute-start.11 = (bf16[4,136,256]{2,1,0:T(8,128)(2,1)S(1)}, bf16[4,136,256]{2,1,0:T(8,128)(2,1)S(1)}, u32[]{:S(2)}, u32[]{:S(2)}) collective-permute-start(bf16[4,136,256]{2,1,0:T(8,128)(2,1)S(1)} %collective-permute-done.10.above), channel_id=1, source_target_pairs={{0,224},{4,228},{8,232},{12,236},{16,240},{20,244},{24,248},{28,25... | collective-permute-start | bytes 835592 | tf_op jit(solution)/shard_map/ppermute | solution.py:228
  36.9 4.1 %collective-permute-start.13 = (bf16[4,136,256]{2,1,0:T(8,128)(2,1)S(1)}, bf16[4,136,256]{2,1,0:T(8,128)(2,1)}, u32[]{:S(2)}, u32[]{:S(2)}) collective-permute-start(bf16[4,136,256]{2,1,0:T(8,128)(2,1)S(1)} %collective-permute-done.4.below), channel_id=1, source_target_pairs={{0,4},{4,0},{8,12},{12,8},{16,20},{20,16},{24,28},{28,24},{32,36},... | collective-permute-start | bytes 835592 | tf_op jit(solution)/shard_map/ppermute | solution.py:228
  53.6 19.0 %all_to_all.25.mixed_ref = bf16[4,32,4096]{2,1,0:T(8,128)(2,1)S(1)} all-to-all(bf16[4,32,4096]{2,1,0:T(8,128)(2,1)S(1)} %bitcast.46), channel_id=1, replica_groups=mesh['sp'=64,'tp'=4] {'tp'}, dimensions={0} | all-to-all | bytes 2097152 | tf_op jit(solution)/shard_map/all_to_all | solution.py:551
  73.4 47.5 %all_to_all.26.arrived_ref = bf16[64,2,4096]{2,1,0:T(2,128)(2,1)S(1)} all-to-all(bf16[64,2,4096]{2,1,0:T(2,128)(2,1)S(1)} %get-tuple-element.78), channel_id=1, replica_groups=mesh['sp'=64,'tp'=4] {'sp'}, dimensions={0} | all-to-all | bytes 2097152 | tf_op jit(solution)/shard_map/all_to_all | solution.py:559
  120.9 2.3 %shard_map.133 = (bf16[48,4096]{1,0:T(8,128)(2,1)S(1)}, bf16[40,4096]{1,0:T(8,128)(2,1)S(1)}, bf16[40,4096]{1,0:T(8,128)(2,1)}, bf16[128,128]{1,0:T(8,128)(2,1)S(1)}) custom-call(bf16[64,2,4096]{2,1,0:T(2,128)(2,1)S(1)} %all_to_all.26.arrived_ref), custom_call_target="tpu_custom_call" | custom-call | flops 134217728 | tf_op jit(solution)/shard_map/pallas_call | solution.py:267
  123.5 2.4 %collective-permute-start.21 = (bf16[40,4096]{1,0:T(8,128)(2,1)S(1)}, bf16[40,4096]{1,0:T(8,128)(2,1)S(1)}, u32[]{:S(2)}, u32[]{:S(2)}) collective-permute-start(bf16[40,4096]{1,0:T(8,128)(2,1)S(1)} %get-tuple-element.83.refs_1_), channel_id=1, source_target_pairs={{0,3},{1,0},{2,1},{3,2},{4,7},{5,4},{6,5},{7,6},{8,11},{9,8},{10,9... | collective-permute-start | bytes 983048 | tf_op jit(solution)/shard_map/ppermute | solution.py:438
  125.9 8.1 %collective-permute-done.18.refs_0_ = bf16[48,4096]{1,0:T(8,128)(2,1)S(1)} collective-permute-done((bf16[48,4096]{1,0:T(8,128)(2,1)S(1)}, bf16[48,4096]{1,0:T(8,128)(2,1)S(1)}, u32[]{:S(2)}, u32[]{:S(2)}) %collective-permute-start.18) | collective-permute-done | bytes 393248 | tf_op jit(solution)/shard_map/ppermute | solution.py:438
  134.0 2.7 %collective-permute-start.23 = (bf16[40,4096]{1,0:T(8,128)(2,1)S(1)}, bf16[40,4096]{1,0:T(8,128)(2,1)S(1)}, u32[]{:S(2)}, u32[]{:S(2)}) collective-permute-start(bf16[40,4096]{1,0:T(8,128)(2,1)S(1)} %collective-permute-done.21.refs_3_), channel_id=1, source_target_pairs={{0,3},{1,0},{2,1},{3,2},{4,7},{5,4},{6,5},{7,6},{8,11},{9,8},{10,9... | collective-permute-start | bytes 983048 | tf_op jit(solution)/shard_map/ppermute | solution.py:438
  138.1 3.3 %collective-permute-done.23.refs_1_ = bf16[40,4096]{1,0:T(8,128)(2,1)S(1)} collective-permute-done((bf16[40,4096]{1,0:T(8,128)(2,1)S(1)}, bf16[40,4096]{1,0:T(8,128)(2,1)S(1)}, u32[]{:S(2)}, u32[]{:S(2)}) %collective-permute-start.23) | collective-permute-done | bytes 327712 | tf_op jit(solution)/shard_map/ppermute | solution.py:438
  141.4 2.4 %collective-permute-done.22.refs_0_ = bf16[48,4096]{1,0:T(8,128)(2,1)S(1)} collective-permute-done((bf16[48,4096]{1,0:T(8,128)(2,1)S(1)}, bf16[48,4096]{1,0:T(8,128)(2,1)S(1)}, u32[]{:S(2)}, u32[]{:S(2)}) %collective-permute-start.22) | collective-permute-done | bytes 393248 | tf_op jit(solution)/shard_map/ppermute | solution.py:438
  146.2 2.7 %collective-permute-start.25 = (bf16[40,4096]{1,0:T(8,128)(2,1)S(1)}, bf16[40,4096]{1,0:T(8,128)(2,1)S(1)}, u32[]{:S(2)}, u32[]{:S(2)}) collective-permute-start(bf16[40,4096]{1,0:T(8,128)(2,1)S(1)} %get-tuple-element.88), channel_id=1, source_target_pairs={{0,3},{1,0},{2,1},{3,2},{4,7},{5,4},{6,5},{7,6},{8,11},{9,8},{10,9... | collective-permute-start | bytes 983048 | tf_op jit(solution)/shard_map/ppermute | solution.py:438
  150.9 3.4 %shard_map.135 = (bf16[48,4096]{1,0:T(8,128)(2,1)S(1)}, bf16[40,4096]{1,0:T(8,128)(2,1)S(1)}, bf16[48,4096]{1,0:T(8,128)(2,1)S(1)}, bf16[40,4096]{1,0:T(8,128)(2,1)}) custom-call(bf16[48,4096]{1,0:T(8,128)(2,1)S(1)} %collective-permute-done.18.refs_0_, bf16[40,4096]{1,0:T(8,128)(2,1)S(1)} %collective-permute-done.19.refs_1_, ...), custom_call_target="tpu_custom_call" | custom-call | flops 1107296256 | tf_op jit(solution)/shard_map/pallas_call | solution.py:267
  154.3 2.4 %collective-permute-start.27 = (bf16[48,4096]{1,0:T(8,128)(2,1)S(1)}, bf16[48,4096]{1,0:T(8,128)(2,1)S(1)}, u32[]{:S(2)}, u32[]{:S(2)}) collective-permute-start(bf16[48,4096]{1,0:T(8,128)(2,1)S(1)} %get-tuple-element.90), channel_id=1, source_target_pairs={{0,3},{1,0},{2,1},{3,2},{4,7},{5,4},{6,5},{7,6},{8,11},{9,8},{10,9... | collective-permute-start | bytes 1179656 | tf_op jit(solution)/shard_map/ppermute | solution.py:438
  156.8 2.4 %collective-permute-done.24.far_up = bf16[48,4096]{1,0:T(8,128)(2,1)S(1)} collective-permute-done((bf16[48,4096]{1,0:T(8,128)(2,1)S(1)}, bf16[48,4096]{1,0:T(8,128)(2,1)S(1)}, u32[]{:S(2)}, u32[]{:S(2)}) %collective-permute-start.24) | collective-permute-done | bytes 393248 | tf_op jit(solution)/shard_map/ppermute | solution.py:438
  160.2 2.7 %collective-permute-start.29 = (bf16[40,4096]{1,0:T(8,128)(2,1)}, bf16[40,4096]{1,0:T(8,128)(2,1)S(1)}, u32[]{:S(2)}, u32[]{:S(2)}) collective-permute-start(bf16[40,4096]{1,0:T(8,128)(2,1)} %get-tuple-element.93), channel_id=1, source_target_pairs={{0,3},{1,0},{2,1},{3,2},{4,7},{5,4},{6,5},{7,6},{8,11},{9,8},{10,9... | collective-permute-start | bytes 983048 | tf_op jit(solution)/shard_map/ppermute | solution.py:438
  164.3 5.1 %shard_map.134 = (bf16[48,4096]{1,0:T(8,128)(2,1)S(1)}, bf16[40,4096]{1,0:T(8,128)(2,1)S(1)}) custom-call(bf16[48,4096]{1,0:T(8,128)(2,1)S(1)} %get-tuple-element.82.refs_0_, bf16[40,4096]{1,0:T(8,128)(2,1)S(1)} %get-tuple-element.83.refs_1_, bf16[4096,256]{1,0:T(8,128)(2,1)} %bitcast.34, bf16[4096,256]{1,0:T(8,128)(2,1)} %bitcast.38, bf16[256,4096]{1,0:T(8,128)(2,1)} %bitcast.42), custom_call_target="tpu_custom_call" | custom-call | flops 553648128 | tf_op jit(solution)/shard_map/pallas_call | solution.py:267
  169.4 6.0 %collective-permute-done.28.refs_4_ = bf16[40,4096]{1,0:T(8,128)(2,1)S(1)} collective-permute-done((bf16[40,4096]{1,0:T(8,128)(2,1)}, bf16[40,4096]{1,0:T(8,128)(2,1)S(1)}, u32[]{:S(2)}, u32[]{:S(2)}) %collective-permute-start.28) | collective-permute-done | bytes 327712 | tf_op jit(solution)/shard_map/ppermute | solution.py:438
  176.0 39.8 %all_to_all.27.returned_ref = bf16[64,2,4096]{2,1,0:T(2,128)(2,1)S(1)} all-to-all(bf16[64,2,4096]{2,1,0:T(2,128)(2,1)S(1)} %shard_map.138), channel_id=1, replica_groups=mesh['sp'=64,'tp'=4] {'sp'}, dimensions={0} | all-to-all | bytes 2097152 | tf_op jit(solution)/shard_map/all_to_all | solution.py:561
  (94 shorter events, 35.7 us)
Async XLA Ops:
  1.7 9.4 %collective-permute-start = (bf16[136,256]{1,0:T(8,128)(2,1)S(1)}, bf16[136,256]{1,0:T(8,128)(2,1)S(1)}, u32[]{:S(2)}, u32[]{:S(2)}) collective-permute-start(bf16[136,256]{1,0:T(8,128)(2,1)S(1)} %maximum_maximum_fusion), channel_id=1, source_target_pairs={{0,8},{4,12},{8,16},{12,20},{16,24},{20,28},{24,0},{28,4},{32,40},... | collective-permute-start | bytes 208904 | tf_op jit(solution)/shard_map/ppermute | solution.py:228
  11.1 11.2 %collective-permute-start.3 = (bf16[4,136,256]{2,1,0:T(8,128)(2,1)S(1)}, bf16[4,136,256]{2,1,0:T(8,128)(2,1)S(1)}, u32[]{:S(2)}, u32[]{:S(2)}) collective-permute-start(bf16[4,136,256]{2,1,0:T(8,128)(2,1)S(1)} %pad_maximum_fusion.own_ref), channel_id=1, source_target_pairs={{0,32},{4,36},{8,40},{12,44},{16,48},{20,52},{24,56},{28,60},{32,6... | collective-permute-start | bytes 835592 | tf_op jit(solution)/shard_map/ppermute | solution.py:228
  12.8 9.5 %collective-permute-start.9 = (bf16[4,136,256]{2,1,0:T(8,128)(2,1)S(1)}, bf16[4,136,256]{2,1,0:T(8,128)(2,1)S(1)}, u32[]{:S(2)}, u32[]{:S(2)}) collective-permute-start(bf16[4,136,256]{2,1,0:T(8,128)(2,1)S(1)} %pad_maximum_fusion.own_ref), channel_id=1, source_target_pairs={{0,224},{4,228},{8,232},{12,236},{16,240},{20,244},{24,248},{28,25... | collective-permute-start | bytes 835592 | tf_op jit(solution)/shard_map/ppermute | solution.py:228
  22.3 10.8 %collective-permute-start.10 = (bf16[4,136,256]{2,1,0:T(8,128)(2,1)S(1)}, bf16[4,136,256]{2,1,0:T(8,128)(2,1)S(1)}, u32[]{:S(2)}, u32[]{:S(2)}) collective-permute-start(bf16[4,136,256]{2,1,0:T(8,128)(2,1)S(1)} %collective-permute-done.9.above), channel_id=1, source_target_pairs={{0,224},{4,228},{8,232},{12,236},{16,240},{20,244},{24,248},{28,25... | collective-permute-start | bytes 835592 | tf_op jit(solution)/shard_map/ppermute | solution.py:228
  32.5 8.5 %collective-permute-start.15 = (bf16[4,136,256]{2,1,0:T(8,128)(2,1)S(1)}, bf16[4,136,256]{2,1,0:T(8,128)(2,1)S(1)}, u32[]{:S(2)}, u32[]{:S(2)}) collective-permute-start(bf16[4,136,256]{2,1,0:T(8,128)(2,1)S(1)} %collective-permute-done.3.below), channel_id=1, source_target_pairs={{0,4},{4,0},{8,12},{12,8},{16,20},{20,16},{24,28},{28,24},{32,36},... | collective-permute-start | bytes 835592 | tf_op jit(solution)/shard_map/ppermute | solution.py:228
  32.5 8.5 %collective-permute-start.16 = (bf16[4,136,256]{2,1,0:T(8,128)(2,1)S(1)}, bf16[4,136,256]{2,1,0:T(8,128)(2,1)S(1)}, u32[]{:S(2)}, u32[]{:S(2)}) collective-permute-start(bf16[4,136,256]{2,1,0:T(8,128)(2,1)S(1)} %collective-permute-done.9.above), channel_id=1, source_target_pairs={{0,4},{4,0},{8,12},{12,8},{16,20},{20,16},{24,28},{28,24},{32,36},... | collective-permute-start | bytes 835592 | tf_op jit(solution)/shard_map/ppermute | solution.py:228
  33.1 9.0 %collective-permute-start.11 = (bf16[4,136,256]{2,1,0:T(8,128)(2,1)S(1)}, bf16[4,136,256]{2,1,0:T(8,128)(2,1)S(1)}, u32[]{:S(2)}, u32[]{:S(2)}) collective-permute-start(bf16[4,136,256]{2,1,0:T(8,128)(2,1)S(1)} %collective-permute-done.10.above), channel_id=1, source_target_pairs={{0,224},{4,228},{8,232},{12,236},{16,240},{20,244},{24,248},{28,25... | collective-permute-start | bytes 835592 | tf_op jit(solution)/shard_map/ppermute | solution.py:228
  36.2 9.8 %collective-permute-start.6 = (bf16[4,136,256]{2,1,0:T(8,128)(2,1)S(1)}, bf16[4,136,256]{2,1,0:T(8,128)(2,1)S(1)}, u32[]{:S(2)}, u32[]{:S(2)}) collective-permute-start(bf16[4,136,256]{2,1,0:T(8,128)(2,1)S(1)} %collective-permute-done.5.below), channel_id=1, source_target_pairs={{0,32},{4,36},{8,40},{12,44},{16,48},{20,52},{24,56},{28,60},{32,6... | collective-permute-start | bytes 835592 | tf_op jit(solution)/shard_map/ppermute | solution.py:228
  36.9 11.9 %collective-permute-start.13 = (bf16[4,136,256]{2,1,0:T(8,128)(2,1)S(1)}, bf16[4,136,256]{2,1,0:T(8,128)(2,1)}, u32[]{:S(2)}, u32[]{:S(2)}) collective-permute-start(bf16[4,136,256]{2,1,0:T(8,128)(2,1)S(1)} %collective-permute-done.4.below), channel_id=1, source_target_pairs={{0,4},{4,0},{8,12},{12,8},{16,20},{20,16},{24,28},{28,24},{32,36},... | collective-permute-start | bytes 835592 | tf_op jit(solution)/shard_map/ppermute | solution.py:228
  41.0 7.8 %collective-permute-start.14 = (bf16[4,136,256]{2,1,0:T(8,128)(2,1)S(1)}, bf16[4,136,256]{2,1,0:T(8,128)(2,1)}, u32[]{:S(2)}, u32[]{:S(2)}) collective-permute-start(bf16[4,136,256]{2,1,0:T(8,128)(2,1)S(1)} %collective-permute-done.10.above), channel_id=1, source_target_pairs={{0,4},{4,0},{8,12},{12,8},{16,20},{20,16},{24,28},{28,24},{32,36},... | collective-permute-start | bytes 835592 | tf_op jit(solution)/shard_map/ppermute | solution.py:228
  41.0 9.1 %collective-permute-start.8 = (bf16[4,136,256]{2,1,0:T(8,128)(2,1)S(1)}, bf16[4,136,256]{2,1,0:T(8,128)(2,1)S(1)}, u32[]{:S(2)}, u32[]{:S(2)}) collective-permute-start(bf16[4,136,256]{2,1,0:T(8,128)(2,1)S(1)} %collective-permute-done.5.below), channel_id=1, source_target_pairs={{0,4},{4,0},{8,12},{12,8},{16,20},{20,16},{24,28},{28,24},{32,36},... | collective-permute-start | bytes 835592 | tf_op jit(solution)/shard_map/ppermute | solution.py:228
  42.0 8.1 %collective-permute-start.12 = (bf16[4,136,256]{2,1,0:T(8,128)(2,1)S(1)}, bf16[4,136,256]{2,1,0:T(8,128)(2,1)}, u32[]{:S(2)}, u32[]{:S(2)}) collective-permute-start(bf16[4,136,256]{2,1,0:T(8,128)(2,1)S(1)} %collective-permute-done.11.above), channel_id=1, source_target_pairs={{0,4},{4,0},{8,12},{12,8},{16,20},{20,16},{24,28},{28,24},{32,36},... | collective-permute-start | bytes 835592 | tf_op jit(solution)/shard_map/ppermute | solution.py:228
  123.2 10.7 %collective-permute-start.18 = (bf16[48,4096]{1,0:T(8,128)(2,1)S(1)}, bf16[48,4096]{1,0:T(8,128)(2,1)S(1)}, u32[]{:S(2)}, u32[]{:S(2)}) collective-permute-start(bf16[48,4096]{1,0:T(8,128)(2,1)S(1)} %get-tuple-element.82.refs_0_), channel_id=1, source_target_pairs={{0,1},{1,2},{2,3},{3,0},{4,5},{5,6},{6,7},{7,4},{8,9},{9,10},{10,1... | collective-permute-start | bytes 1179656 | tf_op jit(solution)/shard_map/ppermute | solution.py:438
  123.5 10.5 %collective-permute-start.21 = (bf16[40,4096]{1,0:T(8,128)(2,1)S(1)}, bf16[40,4096]{1,0:T(8,128)(2,1)S(1)}, u32[]{:S(2)}, u32[]{:S(2)}) collective-permute-start(bf16[40,4096]{1,0:T(8,128)(2,1)S(1)} %get-tuple-element.83.refs_1_), channel_id=1, source_target_pairs={{0,3},{1,0},{2,1},{3,2},{4,7},{5,4},{6,5},{7,6},{8,11},{9,8},{10,9... | collective-permute-start | bytes 983048 | tf_op jit(solution)/shard_map/ppermute | solution.py:438
  134.0 9.9 %collective-permute-start.22 = (bf16[48,4096]{1,0:T(8,128)(2,1)S(1)}, bf16[48,4096]{1,0:T(8,128)(2,1)S(1)}, u32[]{:S(2)}, u32[]{:S(2)}) collective-permute-start(bf16[48,4096]{1,0:T(8,128)(2,1)S(1)} %collective-permute-done.18.refs_0_), channel_id=1, source_target_pairs={{0,1},{1,2},{2,3},{3,0},{4,5},{5,6},{6,7},{7,4},{8,9},{9,10},{10,1... | collective-permute-start | bytes 1179656 | tf_op jit(solution)/shard_map/ppermute | solution.py:438
  134.0 7.5 %collective-permute-start.23 = (bf16[40,4096]{1,0:T(8,128)(2,1)S(1)}, bf16[40,4096]{1,0:T(8,128)(2,1)S(1)}, u32[]{:S(2)}, u32[]{:S(2)}) collective-permute-start(bf16[40,4096]{1,0:T(8,128)(2,1)S(1)} %collective-permute-done.21.refs_3_), channel_id=1, source_target_pairs={{0,3},{1,0},{2,1},{3,2},{4,7},{5,4},{6,5},{7,6},{8,11},{9,8},{10,9... | collective-permute-start | bytes 983048 | tf_op jit(solution)/shard_map/ppermute | solution.py:438
  136.6 14.2 %collective-permute-start.20 = (bf16[48,4096]{1,0:T(8,128)(2,1)S(1)}, bf16[48,4096]{1,0:T(8,128)(2,1)S(1)}, u32[]{:S(2)}, u32[]{:S(2)}) collective-permute-start(bf16[48,4096]{1,0:T(8,128)(2,1)S(1)} %get-tuple-element.82.refs_0_), channel_id=1, source_target_pairs={{0,3},{1,0},{2,1},{3,2},{4,7},{5,4},{6,5},{7,6},{8,11},{9,8},{10,9... | collective-permute-start | bytes 1179656 | tf_op jit(solution)/shard_map/ppermute | solution.py:438
  136.7 14.2 %collective-permute-start.19 = (bf16[40,4096]{1,0:T(8,128)(2,1)S(1)}, bf16[40,4096]{1,0:T(8,128)(2,1)S(1)}, u32[]{:S(2)}, u32[]{:S(2)}) collective-permute-start(bf16[40,4096]{1,0:T(8,128)(2,1)S(1)} %get-tuple-element.83.refs_1_), channel_id=1, source_target_pairs={{0,1},{1,2},{2,3},{3,0},{4,5},{5,6},{6,7},{7,4},{8,9},{9,10},{10,1... | collective-permute-start | bytes 983048 | tf_op jit(solution)/shard_map/ppermute | solution.py:438
  146.1 13.1 %collective-permute-start.24 = (bf16[48,4096]{1,0:T(8,128)(2,1)S(1)}, bf16[48,4096]{1,0:T(8,128)(2,1)S(1)}, u32[]{:S(2)}, u32[]{:S(2)}) collective-permute-start(bf16[48,4096]{1,0:T(8,128)(2,1)S(1)} %get-tuple-element.86), channel_id=1, source_target_pairs={{0,1},{1,2},{2,3},{3,0},{4,5},{5,6},{6,7},{7,4},{8,9},{9,10},{10,1... | collective-permute-start | bytes 1179656 | tf_op jit(solution)/shard_map/ppermute | solution.py:438
  146.2 10.6 %collective-permute-start.25 = (bf16[40,4096]{1,0:T(8,128)(2,1)S(1)}, bf16[40,4096]{1,0:T(8,128)(2,1)S(1)}, u32[]{:S(2)}, u32[]{:S(2)}) collective-permute-start(bf16[40,4096]{1,0:T(8,128)(2,1)S(1)} %get-tuple-element.88), channel_id=1, source_target_pairs={{0,3},{1,0},{2,1},{3,2},{4,7},{5,4},{6,5},{7,6},{8,11},{9,8},{10,9... | collective-permute-start | bytes 983048 | tf_op jit(solution)/shard_map/ppermute | solution.py:438
  154.3 21.1 %collective-permute-start.27 = (bf16[48,4096]{1,0:T(8,128)(2,1)S(1)}, bf16[48,4096]{1,0:T(8,128)(2,1)S(1)}, u32[]{:S(2)}, u32[]{:S(2)}) collective-permute-start(bf16[48,4096]{1,0:T(8,128)(2,1)S(1)} %get-tuple-element.90), channel_id=1, source_target_pairs={{0,3},{1,0},{2,1},{3,2},{4,7},{5,4},{6,5},{7,6},{8,11},{9,8},{10,9... | collective-permute-start | bytes 1179656 | tf_op jit(solution)/shard_map/ppermute | solution.py:438
  160.2 15.2 %collective-permute-start.26 = (bf16[48,4096]{1,0:T(8,128)(2,1)S(1)}, bf16[48,4096]{1,0:T(8,128)(2,1)S(1)}, u32[]{:S(2)}, u32[]{:S(2)}) collective-permute-start(bf16[48,4096]{1,0:T(8,128)(2,1)S(1)} %get-tuple-element.89), channel_id=1, source_target_pairs={{0,1},{1,2},{2,3},{3,0},{4,5},{5,6},{6,7},{7,4},{8,9},{9,10},{10,1... | collective-permute-start | bytes 1179656 | tf_op jit(solution)/shard_map/ppermute | solution.py:438
  160.2 15.2 %collective-permute-start.28 = (bf16[40,4096]{1,0:T(8,128)(2,1)}, bf16[40,4096]{1,0:T(8,128)(2,1)S(1)}, u32[]{:S(2)}, u32[]{:S(2)}) collective-permute-start(bf16[40,4096]{1,0:T(8,128)(2,1)} %get-tuple-element.92), channel_id=1, source_target_pairs={{0,1},{1,2},{2,3},{3,0},{4,5},{5,6},{6,7},{7,4},{8,9},{9,10},{10,1... | collective-permute-start | bytes 983048 | tf_op jit(solution)/shard_map/ppermute | solution.py:438
  160.2 15.2 %collective-permute-start.29 = (bf16[40,4096]{1,0:T(8,128)(2,1)}, bf16[40,4096]{1,0:T(8,128)(2,1)S(1)}, u32[]{:S(2)}, u32[]{:S(2)}) collective-permute-start(bf16[40,4096]{1,0:T(8,128)(2,1)} %get-tuple-element.93), channel_id=1, source_target_pairs={{0,3},{1,0},{2,1},{3,2},{4,7},{5,4},{6,5},{7,6},{8,11},{9,8},{10,9... | collective-permute-start | bytes 983048 | tf_op jit(solution)/shard_map/ppermute | solution.py:438
  (18 other events, 376.4 us)
